TPU v7x, 512 devices: a whole 4x4x16 slice. The times are simulated.
512 devices in a mesh: fs: 64 (over z, y), tp: 8 (over x, core).
Axes of the slice: x: 4, y: 4, z: 16, core: 2. Of those that a mesh axis runs over, the one named last changes fastest.
Arguments:
- tokens: bfloat16 [16384, 2048], P('fs'), may hold values from -6 to 6
- recurrent_input_gain: bfloat16 [2048], replicated, may hold values from 0.099609375 to 1.8984375
- recurrent_branch_weight: bfloat16 [2048, 1024], P('fs', 'tp'), may hold values from -0.125 to 0.125
- output_gate_weight: bfloat16 [2048, 1024], P('fs', 'tp'), may hold values from -0.125 to 0.125
- filter_taps: bfloat16 [4, 1024], P(None, 'tp'), may hold values from -3 to 3
- retention_gate_blocks: bfloat16 [2, 8, 128, 128], P(None, 'tp'), may hold values from -0.5 to 0.5
- input_gate_blocks: bfloat16 [2, 8, 128, 128], P(None, 'tp'), may hold values from -0.5 to 0.5
- channel_decay_rate: float32 [2, 1024], P(None, 'tp'), may hold values from 0 to 0.008, as said below
- position_log_decay: float32 [2, 16384, 1024], P(None, 'fs', 'tp'), may hold values from -0.7 to 0, as said below
- recurrent_output_weight: bfloat16 [1024, 2048], P('tp', 'fs'), may hold values from -0.1875 to 0.1875
- recurrent_output_gain: bfloat16 [2048], replicated, may hold values from 0.099609375 to 1.8984375
- feedforward_norm_gain: bfloat16 [2048], replicated, may hold values from 0.099609375 to 1.8984375
- feedforward_up_weight: bfloat16 [2048, 8192], P('fs', 'tp'), may hold values from -0.125 to 0.125
- feedforward_down_weight: bfloat16 [8192, 2048], P('tp', 'fs'), may hold values from -0.0625 to 0.0625
- feedforward_output_gain: bfloat16 [2048], replicated, may hold values from 0.099609375 to 1.8984375
Outputs:
- layer_out: bfloat16 [16384, 2048], P('fs')
Inputs may be any that keep to these rules, and one draw needn't show every extreme that they name: `channel_decay_rate`: positive rates, one for each channel and direction. `position_log_decay`: zero except at a few positions of each sequence and channel.
All inputs are finite; a program needn't handle non-finite values.
Results may differ from a plain program's by a relative error of at most 0.02.
Values may be sent and summed in bfloat16 or wider, within the bound.
No kernel may reach another device: no remote copies, remote signals or barrier semaphores. Data moves between devices by JAX's collectives and lax.ppermute only.
A program may use at most 128 MiB of HBM per device.

v0:
```python
import jax
import jax.numpy as jnp
from jax import lax
from jax.experimental import pallas as pl
from jax.experimental.pallas import tpu as pltpu
from jax.sharding import Mesh
from jax.sharding import PartitionSpec as P

FS = ("zh", "zl", "y")
Z = ("zh", "zl")
TP = ("x", "c")


EPS = 1e-06
GATE_STEEPNESS = 8.0


def spread(array, axis):
    copies = jnp.broadcast_to(array, (lax.axis_size(axis), *array.shape))
    return lax.all_to_all(copies, axis, split_axis=0, concat_axis=0, tiled=True)


def in_order(pieces, rows):
    width = pieces.shape[-1]
    pieces = pieces.reshape(pieces.shape[0], -1, rows, width)
    return jnp.transpose(pieces, (1, 0, 2, 3)).reshape(-1, width)


def sent_round(array, axis):
    size = lax.axis_size(axis)
    pieces = [array]
    for step in range(1, size):
        ring = [(i, (i + step) % size) for i in range(size)]
        pieces.append(lax.ppermute(array, axis, ring))
    return pieces


def set_in_order(pieces, axis, rows):
    size, here = lax.axis_size(axis), lax.axis_index(axis)
    deep, width = pieces[0].shape[0] // rows, pieces[0].shape[1]
    out = jnp.zeros((deep, size, rows, width), pieces[0].dtype)
    for step, piece in enumerate(pieces):
        block = piece.reshape(deep, 1, rows, width)
        out = lax.dynamic_update_slice(out, block, (0, (here - step) % size, 0, 0))
    return out.reshape(-1, width)


def feedforward_weights(array):
    near = spread(array, "y").reshape(-1, array.shape[-1])
    return lax.all_gather(near, Z, axis=0, tiled=True)


def summed_rows(partial):
    cores, wide = lax.axis_size("c"), lax.axis_size("x")
    rows, width = partial.shape
    halves = partial.astype(jnp.bfloat16).reshape(cores, rows // cores, width)
    pair = lax.all_to_all(halves, "c", split_axis=0, concat_axis=0, tiled=True)
    half = jnp.sum(pair.astype(jnp.float32), axis=0).astype(jnp.bfloat16)
    quarters = half.reshape(wide, rows // (cores * wide), width)
    several = lax.all_to_all(quarters, "x", split_axis=0, concat_axis=0, tiled=True)
    return jnp.sum(several.astype(jnp.float32), axis=0)


def all_rows(part):
    return spread(spread(part, "x"), "c").reshape(-1, part.shape[-1])


def root_norm(values, gain):
    return (
        values
        * lax.rsqrt(jnp.mean(values * values, axis=-1, keepdims=True) + EPS)
        * gain.astype(jnp.float32)
    )


def swept(decay, drive, backward):
    length = decay.shape[0]
    place = lax.broadcasted_iota(jnp.int32, decay.shape, 0)
    step = 1
    while step < length:
        if step % 8:
            turn = length - step if backward else step
            inside = place < length - step if backward else place >= step
            far_decay = jnp.where(inside, pltpu.roll(decay, turn, 0), 1.0)
            far_drive = jnp.where(inside, pltpu.roll(drive, turn, 0), 0.0)
        else:
            one = jnp.ones((step, decay.shape[1]), jnp.float32)
            if backward:
                far_decay = jnp.concatenate((decay[step:], one), axis=0)
                far_drive = jnp.concatenate((drive[step:], 0.0 * one), axis=0)
            else:
                far_decay = jnp.concatenate((one, decay[:-step]), axis=0)
                far_drive = jnp.concatenate((0.0 * one, drive[:-step]), axis=0)
        drive = drive + decay * far_drive
        decay = decay * far_decay
        step *= 2
    return drive


def shifted(values, by):
    if by == 0:
        return values
    length = values.shape[0]
    place = lax.broadcasted_iota(jnp.int32, values.shape, 0)
    inside = place >= by if by > 0 else place < length + by
    return jnp.where(inside, pltpu.roll(values, by % length, 0), 0.0)


def one_less_exp(x):
    series = jnp.ones(x.shape, jnp.float32)
    for degree in range(8, 1, -1):
        series = 1.0 + x * series * (1.0 / degree)
    return jnp.where(jnp.abs(x) < 0.4, -x * series, 1.0 - jnp.exp(x))


def hidden_kernel(both, taps, retention, admission, rate, extra, out):
    channels = out.shape[1]
    signal = both[:, :channels].astype(jnp.float32)
    width_taps = taps.shape[0]
    total = jnp.zeros(signal.shape, jnp.float32)
    for offset in range(width_taps):
        total = total + shifted(signal, width_taps // 2 - offset) * taps[offset : offset + 1, :]
    conv_out = total.astype(jnp.bfloat16)
    wide = conv_out.astype(jnp.float32)
    state = jnp.zeros(signal.shape, jnp.float32)
    for way in range(2):
        retain = jax.nn.sigmoid(
            jnp.dot(conv_out, retention[way], preferred_element_type=jnp.float32)
        )
        admit = jax.nn.sigmoid(
            jnp.dot(conv_out, admission[way], preferred_element_type=jnp.float32)
        )
        log_decay = -GATE_STEEPNESS * retain * rate[way : way + 1, :] + extra[way]
        drive = jnp.sqrt(one_less_exp(2.0 * log_decay)) * (admit * wide)
        state = state + swept(jnp.exp(log_decay), drive, way == 1)
    out[...] = (state * jax.nn.gelu(both[:, channels:].astype(jnp.float32))).astype(out.dtype)


def per_device(
    tokens,
    recurrent_input_gain,
    recurrent_branch_weight,
    output_gate_weight,
    filter_taps,
    retention_gate_blocks,
    input_gate_blocks,
    channel_decay_rate,
    position_log_decay,
    recurrent_output_weight,
    recurrent_output_gain,
    feedforward_norm_gain,
    feedforward_up_weight,
    feedforward_down_weight,
    feedforward_output_gain,
):
    channels = recurrent_branch_weight.shape[1]
    hidden_units = feedforward_up_weight.shape[1]
    rows = recurrent_branch_weight.shape[0]
    early = hidden_units - 2 * channels
    forward = feedforward_weights(
        jnp.concatenate((feedforward_up_weight[:, :early], feedforward_down_weight.T), axis=1)
    )
    column = lax.all_gather(
        jnp.concatenate(
            (
                recurrent_branch_weight,
                output_gate_weight,
                recurrent_output_weight.T,
                feedforward_up_weight[:, early:],
            ),
            axis=1,
        ),
        Z,
        axis=0,
        tiled=True,
    )
    mixer = spread(column[:, : 3 * channels], "y")
    late, mixer = lax.optimization_barrier((column[:, 3 * channels :], mixer))
    late = sent_round(late, "y")
    mixer = in_order(mixer, rows)
    normed = root_norm(tokens.astype(jnp.float32), recurrent_input_gain).astype(jnp.bfloat16)
    both = jnp.dot(
        normed, mixer[:, : 2 * channels], preferred_element_type=jnp.float32
    ).astype(jnp.bfloat16)
    hidden = pl.pallas_call(
        hidden_kernel, out_shape=jax.ShapeDtypeStruct((both.shape[0], channels), jnp.bfloat16)
    )(
        both,
        filter_taps.astype(jnp.float32),
        retention_gate_blocks.reshape(2, channels, channels),
        input_gate_blocks.reshape(2, channels, channels),
        channel_decay_rate,
        position_log_decay,
    )
    across = (((1,), (1,)), ((), ()))
    partial_value = lax.dot_general(
        hidden, mixer[:, 2 * channels :], across, preferred_element_type=jnp.float32
    )
    share = tokens.shape[0] // lax.axis_size(TP)
    place = lax.axis_index("c") * lax.axis_size("x") + lax.axis_index("x")
    own = lax.dynamic_slice_in_dim(tokens, place * share, share, axis=0)
    own, partial_value, mixer_gain, norm_gain, out_gain = lax.optimization_barrier(
        (
            own,
            partial_value.astype(jnp.bfloat16),
            recurrent_output_gain.astype(jnp.float32),
            feedforward_norm_gain.astype(jnp.float32),
            feedforward_output_gain.astype(jnp.float32),
        )
    )
    mixed = summed_rows(partial_value)
    stream = lax.optimization_barrier(
        (own.astype(jnp.float32) + root_norm(mixed, mixer_gain)).astype(jnp.bfloat16)
    )
    normed_ff = all_rows(
        root_norm(stream.astype(jnp.float32), norm_gain).astype(jnp.bfloat16)
    )
    late, normed_ff = lax.optimization_barrier((late, normed_ff))
    lifted = [
        jnp.square(
            jax.nn.relu(jnp.dot(normed_ff, weight, preferred_element_type=jnp.float32))
        ).astype(jnp.bfloat16)
        for weight in (forward[:, :early], set_in_order(late, "y", rows))
    ]
    lowered_part = lax.dot_general(
        jnp.concatenate(lifted, axis=1), forward[:, early:], across, preferred_element_type=jnp.float32
    )
    lowered = summed_rows(lowered_part)
    return all_rows(
        (stream.astype(jnp.float32) + root_norm(lowered, out_gain)).astype(
            jnp.bfloat16
        )
    )


def solution(mesh):
    split = Mesh(mesh.devices.reshape(4, 4, 4, 4, 2), ("zh", "zl", "y", "x", "c"))
    placed = (
        P(FS, None),
        P(),
        P(FS, TP),
        P(FS, TP),
        P(None, TP),
        P(None, TP, None, None),
        P(None, TP, None, None),
        P(None, TP),
        P(None, FS, TP),
        P(TP, FS),
        P(),
        P(),
        P(FS, TP),
        P(TP, FS),
        P(),
    )
    return jax.shard_map(
        per_device, mesh=split, in_specs=placed, out_specs=P(FS, None), check_vma=False
    )
```

profile of v0, /device:TPU:1, one launch (start us, length us, event | category | flops | bytes accessed | tf_op | source)
XLA Modules:
  0.0 184.0 jit_solution(14267748032177936983)
XLA Ops:
  8.3 11.5 %all_to_all.50 = bf16[4,32,1792]{2,1,0:T(8,128)(2,1)} all-to-all(bf16[4,32,1792]{2,1,0:T(8,128)(2,1)S(1)} %broadcast_in_dim.32), channel_id=1, replica_groups=mesh['zh'=4,'zl'=4,'y'=4,'x'=4,'c'=2] {'y'}, dimensions={0} | all-to-all | bytes 917504 | tf_op jit(solution)/shard_map/all_to_all | solution.py:20
  19.9 38.9 %all_gather.6 = bf16[512,640]{1,0:T(8,128)(2,1)S(1)} all-gather(bf16[32,640]{1,0:T(8,128)(2,1)S(1)} %pad_maximum_fusion.1), channel_id=1, replica_groups=mesh['zh'=4,'zl'=4,'y'=4,'x'=4,'c'=2] {'zh','zl'}, dimensions={0}, use_global_device_ids=true | all-gather | bytes 696320 | tf_op jit(solution)/shard_map/all_gather | solution.py:163
  58.7 1.4 broadcast_in_dim.14
  60.1 3.7 %all-to-all-start = ((bf16[4,512,384]{2,1,0:T(8,128)(2,1)}), bf16[4,512,384]{2,1,0:T(8,128)(2,1)S(1)}, u32[]{:S(2)}, u32[]{:S(2)}) async-start(bf16[4,512,384]{2,1,0:T(8,128)(2,1)} %broadcast_in_dim.14), calls=%async_computation | async-start | bytes 3145728 | tf_op jit(solution)/shard_map/all_to_all | solution.py:20
  65.1 1.3 convert_element_type.69
  68.6 8.1 %all-to-all-done = bf16[4,512,384]{2,1,0:T(8,128)(2,1)S(1)} async-done(((bf16[4,512,384]{2,1,0:T(8,128)(2,1)}), bf16[4,512,384]{2,1,0:T(8,128)(2,1)S(1)}, u32[]{:S(2)}, u32[]{:S(2)}) %all-to-all-start) | async-done | bytes 1572896 | tf_op jit(solution)/shard_map/all_to_all | solution.py:20
  77.9 1.9 %convolution_convert_fusion.1.both = bf16[256,256]{1,0:T(8,128)(2,1)} fusion(bf16[256,2048]{1,0:T(8,128)(2,1)S(1)} %copy-done.1, bf16[2048,384]{1,0:T(8,128)(2,1)S(1)} %bitcast.27, f32[2048]{0:T(1024)} %convert_element_type.63, f32[256]{0:T(256)S(1)} %copy-done.10), kind=kOutput, calls=%fused_computation.17 | convolution fusion | flops 270598144 | bytes 2237440 | tf_op jit(solution)/shard_map/dot_general | solution.py:182
  79.8 2.7 %shard_map.145 = bf16[256,128]{1,0:T(8,128)(2,1)} custom-call(bf16[256,256]{1,0:T(8,128)(2,1)} %convolution_convert_fusion.1.both, f32[4,128]{1,0:T(4,128)} %convert_element_type.66.taps, bf16[2,128,128]{2,1,0:T(8,128)(2,1)} %bitcast.41, bf16[2,128,128]{2,1,0:T(8,128)(2,1)} %bitcast.42, f32[2,128]{1,0:T(2,128)} %rate.1, f32[2,256,128]{2,1,0:T(8,128)} %extra.1), custom_call_target="tpu_custom_call" | custom-call | tf_op jit(solution)/shard_map/pallas_call | solution.py:185
  82.5 1.3 convolution_convert_fusion
  83.8 13.0 %all_to_all.51 = bf16[2,128,2048]{2,1,0:T(8,128)(2,1)S(1)} all-to-all(bf16[2,128,2048]{2,1,0:T(8,128)(2,1)S(1)} %bitcast.25), channel_id=1, replica_groups=mesh['zh'=4,'zl'=4,'y'=4,'x'=4,'c'=2] {'c'}, dimensions={0} | all-to-all | bytes 2097152 | tf_op jit(solution)/shard_map/all_to_all | solution.py:57
  97.1 12.5 %all_to_all.52 = bf16[4,32,2048]{2,1,0:T(8,128)(2,1)S(1)} all-to-all(bf16[4,32,2048]{2,1,0:T(8,128)(2,1)S(1)} %bitcast.30), channel_id=1, replica_groups=mesh['zh'=4,'zl'=4,'y'=4,'x'=4,'c'=2] {'x'}, dimensions={0} | all-to-all | bytes 1048576 | tf_op jit(solution)/shard_map/all_to_all | solution.py:60
  111.0 3.5 %all-to-all-start.3 = ((bf16[4,32,2048]{2,1,0:T(8,128)(2,1)}), bf16[4,32,2048]{2,1,0:T(8,128)(2,1)S(1)}, u32[]{:S(2)}, u32[]{:S(2)}) async-start(bf16[4,32,2048]{2,1,0:T(8,128)(2,1)} %broadcast_in_dim.30), calls=%async_computation.3 | async-start | bytes 1048576 | tf_op jit(solution)/shard_map/all_to_all | solution.py:20
  114.5 2.2 %collective-permute-start = (bf16[512,256]{1,0:T(8,128)(2,1)S(1)}, bf16[512,256]{1,0:T(8,128)(2,1)S(1)}, u32[]{:S(2)}, u32[]{:S(2)}) collective-permute-start(bf16[512,256]{1,0:T(8,128)(2,1)S(1)} %slice.32), channel_id=1, source_target_pairs={{0,8},{8,16},{16,24},{24,0},{1,9},{9,17},{17,25},{25,1},{2,10},{10... | collective-permute-start | bytes 786440 | tf_op jit(solution)/shard_map/ppermute | solution.py:34
  116.7 3.7 %collective-permute-start.1 = (bf16[512,256]{1,0:T(8,128)(2,1)S(1)}, bf16[512,256]{1,0:T(8,128)(2,1)S(1)}, u32[]{:S(2)}, u32[]{:S(2)}) collective-permute-start(bf16[512,256]{1,0:T(8,128)(2,1)S(1)} %slice.32), channel_id=1, source_target_pairs={{0,16},{8,24},{16,0},{24,8},{1,17},{9,25},{17,1},{25,9},{2,18},{10... | collective-permute-start | bytes 786440 | tf_op jit(solution)/shard_map/ppermute | solution.py:34
  120.4 2.5 %collective-permute-start.2 = (bf16[512,256]{1,0:T(8,128)(2,1)S(1)}, bf16[512,256]{1,0:T(8,128)(2,1)S(1)}, u32[]{:S(2)}, u32[]{:S(2)}) collective-permute-start(bf16[512,256]{1,0:T(8,128)(2,1)S(1)} %slice.32), channel_id=1, source_target_pairs={{0,24},{8,0},{16,8},{24,16},{1,25},{9,1},{17,9},{25,17},{2,26},{10... | collective-permute-start | bytes 786440 | tf_op jit(solution)/shard_map/ppermute | solution.py:34
  123.0 1.1 broadcast_in_dim.31
  124.1 5.9 %all-to-all-start.4 = ((bf16[2,4,32,2048]{3,2,1,0:T(8,128)(2,1)}), bf16[2,4,32,2048]{3,2,1,0:T(8,128)(2,1)S(1)}, u32[]{:S(2)}, u32[]{:S(2)}) async-start(bf16[2,4,32,2048]{3,2,1,0:T(8,128)(2,1)} %broadcast_in_dim.31), calls=%async_computation.4 | async-start | bytes 2097152 | tf_op jit(solution)/shard_map/all_to_all | solution.py:20
  130.0 2.5 %collective-permute-done.2 = bf16[512,256]{1,0:T(8,128)(2,1)S(1)} collective-permute-done((bf16[512,256]{1,0:T(8,128)(2,1)S(1)}, bf16[512,256]{1,0:T(8,128)(2,1)S(1)}, u32[]{:S(2)}, u32[]{:S(2)}) %collective-permute-start.2) | collective-permute-done | bytes 262176 | tf_op jit(solution)/shard_map/ppermute | solution.py:34
  133.3 2.9 %fusion.16 = bf16[256,768]{1,0:T(8,128)(2,1)S(1)} fusion(bf16[256,2048]{1,0:T(8,128)(2,1)S(1)} %bitcast.34, bf16[2048,1792]{1,0:T(8,128)(2,1)} %all-gather.2.cloned.1.call-done), kind=kOutput, calls=%fused_computation.13 | convolution fusion | flops 805896192 | bytes 4587520 | tf_op jit(solution)/shard_map/dot_general | solution.py:221
  136.1 3.5 %fusion.4 = bf16[256,2048]{1,0:T(8,128)(2,1)S(1)} fusion(bf16[2048,1792]{1,0:T(8,128)(2,1)} %all-gather.2.cloned.1.call-done, bf16[256,256]{1,0:T(8,128)(2,1)S(1)} %fusion.20, bf16[256,768]{1,0:T(8,128)(2,1)S(1)} %fusion.16), kind=kOutput, calls=%fused_computation.7 | convolution fusion | flops 1075314688 | bytes 5767168 | tf_op jit(solution)/shard_map/dot_general | solution.py:225
  139.6 6.1 %all_to_all.53 = bf16[2,128,2048]{2,1,0:T(8,128)(2,1)S(1)} all-to-all(bf16[2,128,2048]{2,1,0:T(8,128)(2,1)S(1)} %bitcast.35), channel_id=1, replica_groups=mesh['zh'=4,'zl'=4,'y'=4,'x'=4,'c'=2] {'c'}, dimensions={0} | all-to-all | bytes 2097152 | tf_op jit(solution)/shard_map/all_to_all | solution.py:57
  146.1 12.6 %all_to_all.54 = bf16[4,32,2048]{2,1,0:T(8,128)(2,1)S(1)} all-to-all(bf16[4,32,2048]{2,1,0:T(8,128)(2,1)S(1)} %bitcast.29), channel_id=1, replica_groups=mesh['zh'=4,'zl'=4,'y'=4,'x'=4,'c'=2] {'x'}, dimensions={0} | all-to-all | bytes 1048576 | tf_op jit(solution)/shard_map/all_to_all | solution.py:60
  159.1 10.2 %all_to_all.55 = bf16[4,32,2048]{2,1,0:T(8,128)(2,1)S(1)} all-to-all(bf16[4,32,2048]{2,1,0:T(8,128)(2,1)S(1)} %broadcast_in_dim.34), channel_id=1, replica_groups=mesh['zh'=4,'zl'=4,'y'=4,'x'=4,'c'=2] {'x'}, dimensions={0} | all-to-all | bytes 1048576 | tf_op jit(solution)/shard_map/all_to_all | solution.py:20
  169.4 6.9 %all_to_all.56 = bf16[2,4,32,2048]{3,2,1,0:T(8,128)(2,1)S(1)} all-to-all(bf16[2,4,32,2048]{3,2,1,0:T(8,128)(2,1)S(1)} %broadcast_in_dim.35), channel_id=1, replica_groups=mesh['zh'=4,'zl'=4,'y'=4,'x'=4,'c'=2] {'c'}, dimensions={0} | all-to-all | bytes 2097152 | tf_op jit(solution)/shard_map/all_to_all | solution.py:20
  (68 shorter events, 10.7 us)
Async XLA Ops:
  6.5 13.3 %slice-start = ((bf16[32,1024]{1,0:T(8,128)(2,1)}), bf16[32,256]{1,0:T(8,128)(2,1)S(1)}, s32[]{:S(2)}) async-start(bf16[32,1024]{1,0:T(8,128)(2,1)} %param.27), calls=%async_computation.11 | async-start | bytes 32768 | tf_op jit(solution)/shard_map/slice | solution.py:169
  6.5 13.3 %copy-start.4 = (bf16[128,32]{0,1:T(8,128)(2,1)S(1)}, bf16[128,32]{0,1:T(8,128)(2,1)}, u32[]{:S(2)}) copy-start(bf16[128,32]{0,1:T(8,128)(2,1)} %param.24) | copy-start | bytes 24580
  6.5 13.3 %copy-start.6 = (bf16[32,128]{1,0:T(8,128)(2,1)S(1)}, bf16[32,128]{1,0:T(8,128)(2,1)}, u32[]{:S(2)}) copy-start(bf16[32,128]{1,0:T(8,128)(2,1)} %param.17) | copy-start | bytes 24580
  6.5 13.3 %copy-start.5 = (bf16[32,128]{1,0:T(8,128)(2,1)S(1)}, bf16[32,128]{1,0:T(8,128)(2,1)}, u32[]{:S(2)}) copy-start(bf16[32,128]{1,0:T(8,128)(2,1)} %param.18) | copy-start | bytes 24580
  6.5 126.7 %all-gather.2.cloned.1.call-start = ((), (), s32[]{:S(2)}) async-start(), calls=%async_computation.10 | async-start | bytes 7798784 | tf_op jit(solution)/shard_map/all_gather | solution.py:50
  60.1 3.8 %copy-start.7 = (bf16[2048]{0:T(1024)(128)(2,1)S(1)}, bf16[2048]{0:T(1024)(128)(2,1)}, u32[]{:S(2)}) copy-start(bf16[2048]{0:T(1024)(128)(2,1)} %param.16) | copy-start | bytes 12292
  60.1 4.4 %copy-start.9 = (bf16[4,128]{1,0:T(4,128)(2,1)S(1)}, bf16[4,128]{1,0:T(4,128)(2,1)}, u32[]{:S(2)}) copy-start(bf16[4,128]{1,0:T(4,128)(2,1)} %param.19) | copy-start | bytes 3076
  60.1 5.0 %copy-start.8 = (bf16[2048]{0:T(1024)(128)(2,1)S(1)}, bf16[2048]{0:T(1024)(128)(2,1)}, u32[]{:S(2)}) copy-start(bf16[2048]{0:T(1024)(128)(2,1)} %param.25) | copy-start | bytes 12292
  60.1 6.9 %copy-start = (bf16[256,2048]{1,0:T(8,128)(2,1)S(1)}, bf16[256,2048]{1,0:T(8,128)(2,1)}, u32[]{:S(2)}) copy-start(bf16[256,2048]{1,0:T(8,128)(2,1)} %param.15) | copy-start | bytes 3145732
  60.1 16.5 %all-to-all-start = ((bf16[4,512,384]{2,1,0:T(8,128)(2,1)}), bf16[4,512,384]{2,1,0:T(8,128)(2,1)S(1)}, u32[]{:S(2)}, u32[]{:S(2)}) async-start(bf16[4,512,384]{2,1,0:T(8,128)(2,1)} %broadcast_in_dim.14), calls=%async_computation | async-start | bytes 3145728 | tf_op jit(solution)/shard_map/all_to_all | solution.py:20
  68.6 8.3 %copy-start.10 = (f32[256]{0:T(256)S(1)}, f32[256]{0:T(256)}, u32[]{:S(2)}) copy-start(f32[256]{0:T(256)} %add_rsqrt_fusion) | copy-start | bytes 3076
  76.7 1.2 copy-start.1
  96.8 13.0 %copy-start.2 = (bf16[32,2048]{1,0:T(8,128)(2,1)S(1)}, bf16[32,2048]{1,0:T(8,128)(2,1)}, u32[]{:S(2)}) copy-start(bf16[32,2048]{1,0:T(8,128)(2,1)} %constant_dynamic-slice_fusion) | copy-start | bytes 393220
  96.8 13.3 %copy-start.3 = (f32[2048]{0:T(1024)S(1)}, f32[2048]{0:T(1024)}, u32[]{:S(2)}) copy-start(f32[2048]{0:T(1024)} %convert_element_type.69) | copy-start | bytes 24580
  111.0 12.0 %all-to-all-start.3 = ((bf16[4,32,2048]{2,1,0:T(8,128)(2,1)}), bf16[4,32,2048]{2,1,0:T(8,128)(2,1)S(1)}, u32[]{:S(2)}, u32[]{:S(2)}) async-start(bf16[4,32,2048]{2,1,0:T(8,128)(2,1)} %broadcast_in_dim.30), calls=%async_computation.3 | async-start | bytes 1048576 | tf_op jit(solution)/shard_map/all_to_all | solution.py:20
  114.5 15.5 %collective-permute-start = (bf16[512,256]{1,0:T(8,128)(2,1)S(1)}, bf16[512,256]{1,0:T(8,128)(2,1)S(1)}, u32[]{:S(2)}, u32[]{:S(2)}) collective-permute-start(bf16[512,256]{1,0:T(8,128)(2,1)S(1)} %slice.32), channel_id=1, source_target_pairs={{0,8},{8,16},{16,24},{24,0},{1,9},{9,17},{17,25},{25,1},{2,10},{10... | collective-permute-start | bytes 786440 | tf_op jit(solution)/shard_map/ppermute | solution.py:34
  116.7 13.3 %collective-permute-start.1 = (bf16[512,256]{1,0:T(8,128)(2,1)S(1)}, bf16[512,256]{1,0:T(8,128)(2,1)S(1)}, u32[]{:S(2)}, u32[]{:S(2)}) collective-permute-start(bf16[512,256]{1,0:T(8,128)(2,1)S(1)} %slice.32), channel_id=1, source_target_pairs={{0,16},{8,24},{16,0},{24,8},{1,17},{9,25},{17,1},{25,9},{2,18},{10... | collective-permute-start | bytes 786440 | tf_op jit(solution)/shard_map/ppermute | solution.py:34
  120.4 12.1 %collective-permute-start.2 = (bf16[512,256]{1,0:T(8,128)(2,1)S(1)}, bf16[512,256]{1,0:T(8,128)(2,1)S(1)}, u32[]{:S(2)}, u32[]{:S(2)}) collective-permute-start(bf16[512,256]{1,0:T(8,128)(2,1)S(1)} %slice.32), channel_id=1, source_target_pairs={{0,24},{8,0},{16,8},{24,16},{1,25},{9,1},{17,9},{25,17},{2,26},{10... | collective-permute-start | bytes 786440 | tf_op jit(solution)/shard_map/ppermute | solution.py:34
  124.1 8.4 %all-to-all-start.4 = ((bf16[2,4,32,2048]{3,2,1,0:T(8,128)(2,1)}), bf16[2,4,32,2048]{3,2,1,0:T(8,128)(2,1)S(1)}, u32[]{:S(2)}, u32[]{:S(2)}) async-start(bf16[2,4,32,2048]{3,2,1,0:T(8,128)(2,1)} %broadcast_in_dim.31), calls=%async_computation.4 | async-start | bytes 2097152 | tf_op jit(solution)/shard_map/all_to_all | solution.py:20
Sparse Core Ops, SparseCore 0:
  19.9 103.5 all-gather.1
where the time goes:
time: 185 us; the launch traced here: 184 us
  blocking collectives  112 us (61%)
  starting transfers between devices  21.5 us (12%)
  between operations  13.8 us (7%)
  waiting for transfers between devices  10.6 us (6%)
  matrix products  9.92 us (5%)
  local copies, waits for them, and re-layouts  7.49 us (4%)
  other arithmetic  6.41 us (3%)
  Pallas kernels  2.73 us (1%)
    all_gather x1, blocking collectives, per_device(): lax.all_gather(jnp.concatenate((recurrent_branch_weight, output_gate_weig...  38.9 us
    all_to_all x3, blocking collectives, spread(): return lax.all_to_all(copies, axis, split_axis=0, concat_axis=0, tiled=True)  28.5 us
    all_to_all x2, blocking collectives, summed_rows(): lax.all_to_all(quarters, 'x', split_axis=0, concat_axis=0, tiled=True)  25.1 us
    all_to_all x2, blocking collectives, summed_rows(): pair = lax.all_to_all(halves, 'c', split_axis=0, concat_axis=0, tiled=True)  19.1 us
    all_to_all x3, starting transfers between devices, spread(): return lax.all_to_all(copies, axis, split_axis=0, concat_axis=0, tiled=True)  13.1 us
    ppermute x3, starting transfers between devices, sent_round(): pieces.append(lax.ppermute(array, axis, ring))  8.41 us
    all_to_all x3, waiting for transfers between devices, spread(): return lax.all_to_all(copies, axis, split_axis=0, concat_axis=0, tiled=True)  8.07 us
  transfers between devices with their start and end apart: 7, of which 2 were waited for; matrix products, arithmetic and copies ran while one was open for 7% of the time, Pallas kernels for 1%

commit v1 on v0

--- a/solution.py
+++ b/solution.py
@@ -35,13 +35,14 @@
     return pieces
 
 
-def set_in_order(pieces, axis, rows):
-    size, here = lax.axis_size(axis), lax.axis_index(axis)
+def set_in_order(pieces, places, rows):
+    size = len(pieces)
     deep, width = pieces[0].shape[0] // rows, pieces[0].shape[1]
     out = jnp.zeros((deep, size, rows, width), pieces[0].dtype)
-    for step, piece in enumerate(pieces):
+    nought = jnp.uint32(0)
+    for place, piece in zip(places, pieces):
         block = piece.reshape(deep, 1, rows, width)
-        out = lax.dynamic_update_slice(out, block, (0, (here - step) % size, 0, 0))
+        out = lax.dynamic_update_slice(out, block, (nought, place, nought, nought))
     return out.reshape(-1, width)
 
 
@@ -178,7 +179,9 @@
     late, mixer = lax.optimization_barrier((column[:, 3 * channels :], mixer))
     late = sent_round(late, "y")
     mixer = in_order(mixer, rows)
-    normed = root_norm(tokens.astype(jnp.float32), recurrent_input_gain).astype(jnp.bfloat16)
+    normed = lax.optimization_barrier(
+        root_norm(tokens.astype(jnp.float32), recurrent_input_gain).astype(jnp.bfloat16)
+    )
     both = jnp.dot(
         normed, mixer[:, : 2 * channels], preferred_element_type=jnp.float32
     ).astype(jnp.bfloat16)
@@ -199,8 +202,12 @@
     share = tokens.shape[0] // lax.axis_size(TP)
     place = lax.axis_index("c") * lax.axis_size("x") + lax.axis_index("x")
     own = lax.dynamic_slice_in_dim(tokens, place * share, share, axis=0)
-    own, partial_value, mixer_gain, norm_gain, out_gain = lax.optimization_barrier(
+    span = lax.axis_size("y")
+    turn = lax.axis_index("y").astype(jnp.uint32)
+    places = [(turn + (span - step)) % span for step in range(span)]
+    places, own, partial_value, mixer_gain, norm_gain, out_gain = lax.optimization_barrier(
         (
+            places,
             own,
             partial_value.astype(jnp.bfloat16),
             recurrent_output_gain.astype(jnp.float32),
@@ -212,15 +219,14 @@
     stream = lax.optimization_barrier(
         (own.astype(jnp.float32) + root_norm(mixed, mixer_gain)).astype(jnp.bfloat16)
     )
-    normed_ff = all_rows(
-        root_norm(stream.astype(jnp.float32), norm_gain).astype(jnp.bfloat16)
-    )
-    late, normed_ff = lax.optimization_barrier((late, normed_ff))
+    half = spread(root_norm(stream.astype(jnp.float32), norm_gain).astype(jnp.bfloat16), "x")
+    half = lax.optimization_barrier(half)
+    normed_ff = spread(half, "c").reshape(tokens.shape)
     lifted = [
         jnp.square(
             jax.nn.relu(jnp.dot(normed_ff, weight, preferred_element_type=jnp.float32))
         ).astype(jnp.bfloat16)
-        for weight in (forward[:, :early], set_in_order(late, "y", rows))
+        for weight in (forward[:, :early], set_in_order(late, places, rows))
     ]
     lowered_part = lax.dot_general(
         jnp.concatenate(lifted, axis=1), forward[:, early:], across, preferred_element_type=jnp.float32

time: 185 us -> 180 us (0.973)
  blocking collectives: 112 us -> 104 us
  waiting for transfers between devices: 10.6 us -> 16.4 us
    all_to_all x2 -> x1, blocking collectives: 25.1 us -> 11.6 us  [summed_rows(): lax.all_to_all(quarters, 'x', split_axis=0, concat_axis=0, tiled=True)]
    all_to_all x3 -> x4, blocking collectives: 28.5 us -> 35.6 us  [spread(): return lax.all_to_all(copies, axis, split_axis=0, concat_axis=0, tiled=True)]
    all_to_all x3 -> x2, starting transfers between devices: 13.1 us -> 7.45 us  [spread(): return lax.all_to_all(copies, axis, split_axis=0, concat_axis=0, tiled=True)]
    all_to_all x0 -> x1, starting transfers between devices: none -> 3.98 us  [summed_rows(): lax.all_to_all(quarters, 'x', split_axis=0, concat_axis=0, tiled=True)]
    all_to_all x3 -> x2, waiting for transfers between devices: 8.07 us -> 11.8 us  [spread(): return lax.all_to_all(copies, axis, split_axis=0, concat_axis=0, tiled=True)]
  transfers between devices with their start and end apart: 7 -> 7, of which waited for: 2 -> 5; matrix products, arithmetic and copies ran while one was open for 7% -> 6% of each run, Pallas kernels for 1% -> 2%
where the time goes in v1:
time: 180 us; the launch traced here: 179 us
  blocking collectives  104 us (58%)
  starting transfers between devices  19.9 us (11%)
  waiting for transfers between devices  16.4 us (9%)
  between operations  13.7 us (8%)
  matrix products  9.17 us (5%)
  other arithmetic  7.33 us (4%)
  local copies, waits for them, and re-layouts  5.85 us (3%)
  Pallas kernels  2.75 us (2%)
    all_gather x1, blocking collectives, per_device(): lax.all_gather(jnp.concatenate((recurrent_branch_weight, output_gate_weig...  38.9 us
    all_to_all x4, blocking collectives, spread(): return lax.all_to_all(copies, axis, split_axis=0, concat_axis=0, tiled=True)  35.6 us
    all_to_all x2, blocking collectives, summed_rows(): pair = lax.all_to_all(halves, 'c', split_axis=0, concat_axis=0, tiled=True)  17.6 us
    all_to_all x2, waiting for transfers between devices, spread(): return lax.all_to_all(copies, axis, split_axis=0, concat_axis=0, tiled=True)  11.8 us
    all_to_all x1, blocking collectives, summed_rows(): lax.all_to_all(quarters, 'x', split_axis=0, concat_axis=0, tiled=True)  11.6 us
    ppermute x3, starting transfers between devices, sent_round(): pieces.append(lax.ppermute(array, axis, ring))  8.4 us
    all_to_all x2, starting transfers between devices, spread(): return lax.all_to_all(copies, axis, split_axis=0, concat_axis=0, tiled=True)  7.45 us
    ppermute x3, waiting for transfers between devices, sent_round(): pieces.append(lax.ppermute(array, axis, ring))  4.07 us
  transfers between devices with their start and end apart: 7, of which 5 were waited for; matrix products, arithmetic and copies ran while one was open for 6% of the time, Pallas kernels for 2%

profile of v1, /device:TPU:1, one launch (start us, length us, event | category | flops | bytes accessed | tf_op | source)
XLA Modules:
  0.0 178.7 jit_solution(12207303571954360608)
XLA Ops:
  8.3 11.5 %all_to_all.50 = bf16[4,32,1792]{2,1,0:T(8,128)(2,1)} all-to-all(bf16[4,32,1792]{2,1,0:T(8,128)(2,1)S(1)} %broadcast_in_dim.32), channel_id=1, replica_groups=mesh['zh'=4,'zl'=4,'y'=4,'x'=4,'c'=2] {'y'}, dimensions={0} | all-to-all | bytes 917504 | tf_op jit(solution)/shard_map/all_to_all | solution.py:20
  19.9 38.9 %all_gather.6 = bf16[512,640]{1,0:T(8,128)(2,1)S(1)} all-gather(bf16[32,640]{1,0:T(8,128)(2,1)S(1)} %pad_maximum_fusion.1), channel_id=1, replica_groups=mesh['zh'=4,'zl'=4,'y'=4,'x'=4,'c'=2] {'zh','zl'}, dimensions={0}, use_global_device_ids=true | all-gather | bytes 696320 | tf_op jit(solution)/shard_map/all_gather | solution.py:164
  58.7 1.4 broadcast_in_dim.14
  60.1 3.7 %all-to-all-start = ((bf16[4,512,384]{2,1,0:T(8,128)(2,1)}), bf16[4,512,384]{2,1,0:T(8,128)(2,1)S(1)}, u32[]{:S(2)}, u32[]{:S(2)}) async-start(bf16[4,512,384]{2,1,0:T(8,128)(2,1)} %broadcast_in_dim.14), calls=%async_computation | async-start | bytes 3145728 | tf_op jit(solution)/shard_map/all_to_all | solution.py:20
  64.2 1.3 fusion.9
  66.1 1.3 convert_element_type.78
  68.1 8.6 %all-to-all-done = bf16[4,512,384]{2,1,0:T(8,128)(2,1)S(1)} async-done(((bf16[4,512,384]{2,1,0:T(8,128)(2,1)}), bf16[4,512,384]{2,1,0:T(8,128)(2,1)S(1)}, u32[]{:S(2)}, u32[]{:S(2)}) %all-to-all-start) | async-done | bytes 1572896 | tf_op jit(solution)/shard_map/all_to_all | solution.py:20
  79.0 2.7 %shard_map.145 = bf16[256,128]{1,0:T(8,128)(2,1)} custom-call(bf16[256,256]{1,0:T(8,128)(2,1)} %convolution_convert_fusion.1.both, f32[4,128]{1,0:T(4,128)} %convert_element_type.75.taps, bf16[2,128,128]{2,1,0:T(8,128)(2,1)} %bitcast.41, bf16[2,128,128]{2,1,0:T(8,128)(2,1)} %bitcast.42, f32[2,128]{1,0:T(2,128)} %rate.1, f32[2,256,128]{2,1,0:T(8,128)} %extra.1), custom_call_target="tpu_custom_call" | custom-call | tf_op jit(solution)/shard_map/pallas_call | solution.py:188
  81.7 1.3 convolution_convert_fusion
  83.0 13.0 %all_to_all.51 = bf16[2,128,2048]{2,1,0:T(8,128)(2,1)S(1)} all-to-all(bf16[2,128,2048]{2,1,0:T(8,128)(2,1)S(1)} %bitcast.26), channel_id=1, replica_groups=mesh['zh'=4,'zl'=4,'y'=4,'x'=4,'c'=2] {'c'}, dimensions={0} | all-to-all | bytes 2097152 | tf_op jit(solution)/shard_map/all_to_all | solution.py:58
  97.1 4.0 %all-to-all-start.2 = ((bf16[4,32,2048]{2,1,0:T(8,128)(2,1)}), bf16[4,32,2048]{2,1,0:T(8,128)(2,1)S(1)}, u32[]{:S(2)}, u32[]{:S(2)}) async-start(bf16[4,32,2048]{2,1,0:T(8,128)(2,1)} %bitcast.7), calls=%async_computation.2 | async-start | bytes 1048576 | tf_op jit(solution)/shard_map/all_to_all | solution.py:61
  101.1 2.2 %collective-permute-start = (bf16[512,256]{1,0:T(8,128)(2,1)S(1)}, bf16[512,256]{1,0:T(8,128)(2,1)S(1)}, u32[]{:S(2)}, u32[]{:S(2)}) collective-permute-start(bf16[512,256]{1,0:T(8,128)(2,1)S(1)} %slice.32), channel_id=1, source_target_pairs={{0,8},{8,16},{16,24},{24,0},{1,9},{9,17},{17,25},{25,1},{2,10},{10... | collective-permute-start | bytes 786440 | tf_op jit(solution)/shard_map/ppermute | solution.py:34
  103.3 3.7 %collective-permute-start.1 = (bf16[512,256]{1,0:T(8,128)(2,1)S(1)}, bf16[512,256]{1,0:T(8,128)(2,1)S(1)}, u32[]{:S(2)}, u32[]{:S(2)}) collective-permute-start(bf16[512,256]{1,0:T(8,128)(2,1)S(1)} %slice.32), channel_id=1, source_target_pairs={{0,16},{8,24},{16,0},{24,8},{1,17},{9,25},{17,1},{25,9},{2,18},{10... | collective-permute-start | bytes 786440 | tf_op jit(solution)/shard_map/ppermute | solution.py:34
  107.0 2.5 %collective-permute-start.2 = (bf16[512,256]{1,0:T(8,128)(2,1)S(1)}, bf16[512,256]{1,0:T(8,128)(2,1)S(1)}, u32[]{:S(2)}, u32[]{:S(2)}) collective-permute-start(bf16[512,256]{1,0:T(8,128)(2,1)S(1)} %slice.32), channel_id=1, source_target_pairs={{0,24},{8,0},{16,8},{24,16},{1,25},{9,1},{17,9},{25,17},{2,26},{10... | collective-permute-start | bytes 786440 | tf_op jit(solution)/shard_map/ppermute | solution.py:34
  111.5 3.8 %all-to-all-start.3 = ((bf16[4,32,2048]{2,1,0:T(8,128)(2,1)}), bf16[4,32,2048]{2,1,0:T(8,128)(2,1)S(1)}, u32[]{:S(2)}, u32[]{:S(2)}) async-start(bf16[4,32,2048]{2,1,0:T(8,128)(2,1)} %broadcast_in_dim.30), calls=%async_computation.3 | async-start | bytes 1048576 | tf_op jit(solution)/shard_map/all_to_all | solution.py:20
  116.5 3.0 %collective-permute-done.2 = bf16[512,256]{1,0:T(8,128)(2,1)S(1)} collective-permute-done((bf16[512,256]{1,0:T(8,128)(2,1)S(1)}, bf16[512,256]{1,0:T(8,128)(2,1)S(1)}, u32[]{:S(2)}, u32[]{:S(2)}) %collective-permute-start.2) | collective-permute-done | bytes 262176 | tf_op jit(solution)/shard_map/ppermute | solution.py:34
  119.6 3.2 %all-to-all-done.3 = bf16[4,32,2048]{2,1,0:T(8,128)(2,1)S(1)} async-done(((bf16[4,32,2048]{2,1,0:T(8,128)(2,1)}), bf16[4,32,2048]{2,1,0:T(8,128)(2,1)S(1)}, u32[]{:S(2)}, u32[]{:S(2)}) %all-to-all-start.3) | async-done | bytes 524320 | tf_op jit(solution)/shard_map/all_to_all | solution.py:20
  122.9 7.1 %all_to_all.52 = bf16[2,4,32,2048]{3,2,1,0:T(8,128)(2,1)S(1)} all-to-all(bf16[2,4,32,2048]{3,2,1,0:T(8,128)(2,1)S(1)} %broadcast_in_dim.31), channel_id=1, replica_groups=mesh['zh'=4,'zl'=4,'y'=4,'x'=4,'c'=2] {'c'}, dimensions={0} | all-to-all | bytes 2097152 | tf_op jit(solution)/shard_map/all_to_all | solution.py:20
  130.5 2.9 %fusion.16 = bf16[256,768]{1,0:T(8,128)(2,1)S(1)} fusion(bf16[256,2048]{1,0:T(8,128)(2,1)S(1)} %bitcast.34, bf16[2048,1792]{1,0:T(8,128)(2,1)} %all-gather.2.cloned.1.call-done), kind=kOutput, calls=%fused_computation.13 | convolution fusion | flops 805896192 | bytes 4587520 | tf_op jit(solution)/shard_map/dot_general | solution.py:227
  133.4 3.5 %fusion.4 = bf16[256,2048]{1,0:T(8,128)(2,1)S(1)} fusion(bf16[2048,1792]{1,0:T(8,128)(2,1)} %all-gather.2.cloned.1.call-done, bf16[256,256]{1,0:T(8,128)(2,1)S(1)} %fusion.20, bf16[256,768]{1,0:T(8,128)(2,1)S(1)} %fusion.16), kind=kOutput, calls=%fused_computation.7 | convolution fusion | flops 1075314688 | bytes 5767168 | tf_op jit(solution)/shard_map/dot_general | solution.py:231
  136.8 4.6 %all_to_all.53 = bf16[2,128,2048]{2,1,0:T(8,128)(2,1)S(1)} all-to-all(bf16[2,128,2048]{2,1,0:T(8,128)(2,1)S(1)} %bitcast.35), channel_id=1, replica_groups=mesh['zh'=4,'zl'=4,'y'=4,'x'=4,'c'=2] {'c'}, dimensions={0} | all-to-all | bytes 2097152 | tf_op jit(solution)/shard_map/all_to_all | solution.py:58
  141.7 11.6 %all_to_all.54 = bf16[4,32,2048]{2,1,0:T(8,128)(2,1)S(1)} all-to-all(bf16[4,32,2048]{2,1,0:T(8,128)(2,1)S(1)} %bitcast.30), channel_id=1, replica_groups=mesh['zh'=4,'zl'=4,'y'=4,'x'=4,'c'=2] {'x'}, dimensions={0} | all-to-all | bytes 1048576 | tf_op jit(solution)/shard_map/all_to_all | solution.py:61
  153.7 10.7 %all_to_all.55 = bf16[4,32,2048]{2,1,0:T(8,128)(2,1)S(1)} all-to-all(bf16[4,32,2048]{2,1,0:T(8,128)(2,1)S(1)} %broadcast_in_dim.34), channel_id=1, replica_groups=mesh['zh'=4,'zl'=4,'y'=4,'x'=4,'c'=2] {'x'}, dimensions={0} | all-to-all | bytes 1048576 | tf_op jit(solution)/shard_map/all_to_all | solution.py:20
  164.6 6.3 %all_to_all.56 = bf16[2,4,32,2048]{3,2,1,0:T(8,128)(2,1)S(1)} all-to-all(bf16[2,4,32,2048]{3,2,1,0:T(8,128)(2,1)S(1)} %broadcast_in_dim.35), channel_id=1, replica_groups=mesh['zh'=4,'zl'=4,'y'=4,'x'=4,'c'=2] {'c'}, dimensions={0} | all-to-all | bytes 2097152 | tf_op jit(solution)/shard_map/all_to_all | solution.py:20
  (65 shorter events, 12.4 us)
Async XLA Ops:
  6.5 13.3 %slice-start = ((bf16[32,1024]{1,0:T(8,128)(2,1)}), bf16[32,256]{1,0:T(8,128)(2,1)S(1)}, s32[]{:S(2)}) async-start(bf16[32,1024]{1,0:T(8,128)(2,1)} %param.27), calls=%async_computation.11 | async-start | bytes 32768 | tf_op jit(solution)/shard_map/slice | solution.py:170
  6.5 13.3 %copy-start.3 = (bf16[128,32]{0,1:T(8,128)(2,1)S(1)}, bf16[128,32]{0,1:T(8,128)(2,1)}, u32[]{:S(2)}) copy-start(bf16[128,32]{0,1:T(8,128)(2,1)} %param.24) | copy-start | bytes 24580
  6.5 13.3 %copy-start.5 = (bf16[32,128]{1,0:T(8,128)(2,1)S(1)}, bf16[32,128]{1,0:T(8,128)(2,1)}, u32[]{:S(2)}) copy-start(bf16[32,128]{1,0:T(8,128)(2,1)} %param.17) | copy-start | bytes 24580
  6.5 13.3 %copy-start.4 = (bf16[32,128]{1,0:T(8,128)(2,1)S(1)}, bf16[32,128]{1,0:T(8,128)(2,1)}, u32[]{:S(2)}) copy-start(bf16[32,128]{1,0:T(8,128)(2,1)} %param.18) | copy-start | bytes 24580
  6.5 123.9 %all-gather.2.cloned.1.call-start = ((), (), s32[]{:S(2)}) async-start(), calls=%async_computation.10 | async-start | bytes 7798784 | tf_op jit(solution)/shard_map/all_gather | solution.py:51
  60.1 3.8 %copy-start.6 = (bf16[2048]{0:T(1024)(128)(2,1)S(1)}, bf16[2048]{0:T(1024)(128)(2,1)}, u32[]{:S(2)}) copy-start(bf16[2048]{0:T(1024)(128)(2,1)} %param.16) | copy-start | bytes 12292
  60.1 3.8 %copy-start = (bf16[256,2048]{1,0:T(8,128)(2,1)S(1)}, bf16[256,2048]{1,0:T(8,128)(2,1)}, u32[]{:S(2)}) copy-start(bf16[256,2048]{1,0:T(8,128)(2,1)} %param.15) | copy-start | bytes 3145732
  60.1 16.5 %all-to-all-start = ((bf16[4,512,384]{2,1,0:T(8,128)(2,1)}), bf16[4,512,384]{2,1,0:T(8,128)(2,1)S(1)}, u32[]{:S(2)}, u32[]{:S(2)}) async-start(bf16[4,512,384]{2,1,0:T(8,128)(2,1)} %broadcast_in_dim.14), calls=%async_computation | async-start | bytes 3145728 | tf_op jit(solution)/shard_map/all_to_all | solution.py:20
  63.8 1.7 copy-start.8
  63.8 2.3 %copy-start.7 = (bf16[2048]{0:T(1024)(128)(2,1)S(1)}, bf16[2048]{0:T(1024)(128)(2,1)}, u32[]{:S(2)}) copy-start(bf16[2048]{0:T(1024)(128)(2,1)} %param.25) | copy-start | bytes 12292
  76.6 1.2 copy-start.1
  96.0 14.5 %copy-start.2 = (f32[2048]{0:T(1024)S(1)}, f32[2048]{0:T(1024)}, u32[]{:S(2)}) copy-start(f32[2048]{0:T(1024)} %convert_element_type.78) | copy-start | bytes 24580
  97.1 12.9 %all-to-all-start.2 = ((bf16[4,32,2048]{2,1,0:T(8,128)(2,1)}), bf16[4,32,2048]{2,1,0:T(8,128)(2,1)S(1)}, u32[]{:S(2)}, u32[]{:S(2)}) async-start(bf16[4,32,2048]{2,1,0:T(8,128)(2,1)} %bitcast.7), calls=%async_computation.2 | async-start | bytes 1048576 | tf_op jit(solution)/shard_map/all_to_all | solution.py:61
  101.1 14.3 %collective-permute-start = (bf16[512,256]{1,0:T(8,128)(2,1)S(1)}, bf16[512,256]{1,0:T(8,128)(2,1)S(1)}, u32[]{:S(2)}, u32[]{:S(2)}) collective-permute-start(bf16[512,256]{1,0:T(8,128)(2,1)S(1)} %slice.32), channel_id=1, source_target_pairs={{0,8},{8,16},{16,24},{24,0},{1,9},{9,17},{17,25},{25,1},{2,10},{10... | collective-permute-start | bytes 786440 | tf_op jit(solution)/shard_map/ppermute | solution.py:34
  103.3 13.2 %collective-permute-start.1 = (bf16[512,256]{1,0:T(8,128)(2,1)S(1)}, bf16[512,256]{1,0:T(8,128)(2,1)S(1)}, u32[]{:S(2)}, u32[]{:S(2)}) collective-permute-start(bf16[512,256]{1,0:T(8,128)(2,1)S(1)} %slice.32), channel_id=1, source_target_pairs={{0,16},{8,24},{16,0},{24,8},{1,17},{9,25},{17,1},{25,9},{2,18},{10... | collective-permute-start | bytes 786440 | tf_op jit(solution)/shard_map/ppermute | solution.py:34
  107.0 12.5 %collective-permute-start.2 = (bf16[512,256]{1,0:T(8,128)(2,1)S(1)}, bf16[512,256]{1,0:T(8,128)(2,1)S(1)}, u32[]{:S(2)}, u32[]{:S(2)}) collective-permute-start(bf16[512,256]{1,0:T(8,128)(2,1)S(1)} %slice.32), channel_id=1, source_target_pairs={{0,24},{8,0},{16,8},{24,16},{1,25},{9,1},{17,9},{25,17},{2,26},{10... | collective-permute-start | bytes 786440 | tf_op jit(solution)/shard_map/ppermute | solution.py:34
  111.5 11.3 %all-to-all-start.3 = ((bf16[4,32,2048]{2,1,0:T(8,128)(2,1)}), bf16[4,32,2048]{2,1,0:T(8,128)(2,1)S(1)}, u32[]{:S(2)}, u32[]{:S(2)}) async-start(bf16[4,32,2048]{2,1,0:T(8,128)(2,1)} %broadcast_in_dim.30), calls=%async_computation.3 | async-start | bytes 1048576 | tf_op jit(solution)/shard_map/all_to_all | solution.py:20
Sparse Core Ops, SparseCore 0:
  19.9 103.5 all-gather.1

commit v2 on v1

--- a/solution.py
+++ b/solution.py
@@ -35,15 +35,11 @@
     return pieces
 
 
-def set_in_order(pieces, places, rows):
-    size = len(pieces)
-    deep, width = pieces[0].shape[0] // rows, pieces[0].shape[1]
-    out = jnp.zeros((deep, size, rows, width), pieces[0].dtype)
+def set_in(out, piece, place):
+    deep, _, rows, width = out.shape
     nought = jnp.uint32(0)
-    for place, piece in zip(places, pieces):
-        block = piece.reshape(deep, 1, rows, width)
-        out = lax.dynamic_update_slice(out, block, (nought, place, nought, nought))
-    return out.reshape(-1, width)
+    block = piece.reshape(deep, 1, rows, width)
+    return lax.dynamic_update_slice(out, block, (nought, place, nought, nought))
 
 
 def feedforward_weights(array):
@@ -63,7 +59,10 @@
 
 
 def all_rows(part):
-    return spread(spread(part, "x"), "c").reshape(-1, part.shape[-1])
+    half = spread(part, "x").reshape(-1, part.shape[-1])
+    other = lax.ppermute(half, "c", [(0, 1), (1, 0)])
+    mine = lax.broadcasted_iota(jnp.int32, (2, 1, 1), 0) == lax.axis_index("c")
+    return jnp.where(mine, half[None], other[None]).reshape(-1, part.shape[-1])
 
 
 def root_norm(values, gain):
@@ -157,7 +156,7 @@
     channels = recurrent_branch_weight.shape[1]
     hidden_units = feedforward_up_weight.shape[1]
     rows = recurrent_branch_weight.shape[0]
-    early = hidden_units - 2 * channels
+    early = hidden_units - channels
     forward = feedforward_weights(
         jnp.concatenate((feedforward_up_weight[:, :early], feedforward_down_weight.T), axis=1)
     )
@@ -205,8 +204,12 @@
     span = lax.axis_size("y")
     turn = lax.axis_index("y").astype(jnp.uint32)
     places = [(turn + (span - step)) % span for step in range(span)]
-    places, own, partial_value, mixer_gain, norm_gain, out_gain = lax.optimization_barrier(
+    late_width = late[0].shape[1]
+    late_up = jnp.zeros((late[0].shape[0] // rows, span, rows, late_width), jnp.bfloat16)
+    late_up = set_in(late_up, late[0], places[0])
+    late_up, places, own, partial_value, mixer_gain, norm_gain, out_gain = lax.optimization_barrier(
         (
+            late_up,
             places,
             own,
             partial_value.astype(jnp.bfloat16),
@@ -222,11 +225,13 @@
     half = spread(root_norm(stream.astype(jnp.float32), norm_gain).astype(jnp.bfloat16), "x")
     half = lax.optimization_barrier(half)
     normed_ff = spread(half, "c").reshape(tokens.shape)
+    for piece, spot in zip(late[1:], places[1:]):
+        late_up = set_in(late_up, piece, spot)
     lifted = [
         jnp.square(
             jax.nn.relu(jnp.dot(normed_ff, weight, preferred_element_type=jnp.float32))
         ).astype(jnp.bfloat16)
-        for weight in (forward[:, :early], set_in_order(late, places, rows))
+        for weight in (forward[:, :early], late_up.reshape(-1, late_width))
     ]
     lowered_part = lax.dot_general(
         jnp.concatenate(lifted, axis=1), forward[:, early:], across, preferred_element_type=jnp.float32

time: 180 us -> 179 us (level)
  blocking collectives: 104 us -> 94.6 us
  waiting for transfers between devices: 16.4 us -> 22.4 us
  starting transfers between devices: 19.9 us -> 24.5 us
    all_to_all x4 -> x3, blocking collectives: 35.6 us -> 27.5 us  [spread(): return lax.all_to_all(copies, axis, split_axis=0, concat_axis=0, tiled=True)]
    all_to_all x1, waiting for transfers between devices: 0.49 us -> 6.7 us  [summed_rows(): lax.all_to_all(quarters, 'x', split_axis=0, concat_axis=0, tiled=True)]
    ppermute x0 -> x1, starting transfers between devices: none -> 4.56 us  [all_rows(): other = lax.ppermute(half, 'c', [(0, 1), (1, 0)])]
    dot_general x1, matrix products: 3.48 us -> 1.28 us  [per_device(): lax.dot_general(jnp.concatenate(lifted, axis=1), forward[:, early:], acro...]
  transfers between devices with their start and end apart: 7 -> 8, of which waited for: 5 -> 5; matrix products, arithmetic and copies ran while one was open for 6% -> 5% of each run, Pallas kernels for 2% -> 2%
where the time goes in v2:
time: 179 us; the launch traced here: 178 us
  blocking collectives  94.6 us (53%)
  starting transfers between devices  24.5 us (14%)
  waiting for transfers between devices  22.4 us (13%)
  between operations  13.8 us (8%)
  matrix products  7.53 us (4%)
  other arithmetic  6.53 us (4%)
  local copies, waits for them, and re-layouts  5.73 us (3%)
  Pallas kernels  2.75 us (2%)
    all_gather x1, blocking collectives, per_device(): lax.all_gather(jnp.concatenate((recurrent_branch_weight, output_gate_weig...  37.3 us
    all_to_all x3, blocking collectives, spread(): return lax.all_to_all(copies, axis, split_axis=0, concat_axis=0, tiled=True)  27.5 us
    all_to_all x2, blocking collectives, summed_rows(): pair = lax.all_to_all(halves, 'c', split_axis=0, concat_axis=0, tiled=True)  16.9 us
    all_to_all x1, blocking collectives, summed_rows(): lax.all_to_all(quarters, 'x', split_axis=0, concat_axis=0, tiled=True)  12.9 us
    all_to_all x2, waiting for transfers between devices, spread(): return lax.all_to_all(copies, axis, split_axis=0, concat_axis=0, tiled=True)  11.1 us
    ppermute x3, starting transfers between devices, sent_round(): pieces.append(lax.ppermute(array, axis, ring))  8.75 us
    all_to_all x2, starting transfers between devices, spread(): return lax.all_to_all(copies, axis, split_axis=0, concat_axis=0, tiled=True)  7.17 us
    all_to_all x1, waiting for transfers between devices, summed_rows(): lax.all_to_all(quarters, 'x', split_axis=0, concat_axis=0, tiled=True)  6.7 us
  transfers between devices with their start and end apart: 8, of which 5 were waited for; matrix products, arithmetic and copies ran while one was open for 5% of the time, Pallas kernels for 2%

profile of v2, /device:TPU:1, one launch (start us, length us, event | category | flops | bytes accessed | tf_op | source)
XLA Modules:
  0.0 177.8 jit_solution(14949958088759216166)
XLA Ops:
  8.3 11.7 %all_to_all.45 = bf16[4,32,1920]{2,1,0:T(8,128)(2,1)} all-to-all(bf16[4,32,1920]{2,1,0:T(8,128)(2,1)S(1)} %broadcast_in_dim.68), channel_id=1, replica_groups=mesh['zh'=4,'zl'=4,'y'=4,'x'=4,'c'=2] {'y'}, dimensions={0} | all-to-all | bytes 983040 | tf_op jit(solution)/shard_map/all_to_all | solution.py:20
  20.1 37.3 %all_gather.6 = bf16[512,512]{1,0:T(8,128)(2,1)S(1)} all-gather(bf16[32,512]{1,0:T(8,128)(2,1)S(1)} %pad_maximum_fusion.1), channel_id=1, replica_groups=mesh['zh'=4,'zl'=4,'y'=4,'x'=4,'c'=2] {'zh','zl'}, dimensions={0}, use_global_device_ids=true | all-gather | bytes 557056 | tf_op jit(solution)/shard_map/all_gather | solution.py:163
  57.4 1.4 broadcast_in_dim.65
  58.8 3.7 %all-to-all-start = ((bf16[4,512,384]{2,1,0:T(8,128)(2,1)}), bf16[4,512,384]{2,1,0:T(8,128)(2,1)S(1)}, u32[]{:S(2)}, u32[]{:S(2)}) async-start(bf16[4,512,384]{2,1,0:T(8,128)(2,1)} %broadcast_in_dim.65), calls=%async_computation | async-start | bytes 3145728 | tf_op jit(solution)/shard_map/all_to_all | solution.py:20
  62.9 1.3 fusion.9
  64.8 11.1 %all-to-all-done = bf16[4,512,384]{2,1,0:T(8,128)(2,1)S(1)} async-done(((bf16[4,512,384]{2,1,0:T(8,128)(2,1)}), bf16[4,512,384]{2,1,0:T(8,128)(2,1)S(1)}, u32[]{:S(2)}, u32[]{:S(2)}) %all-to-all-start) | async-done | bytes 1572896 | tf_op jit(solution)/shard_map/all_to_all | solution.py:20
  78.3 2.8 %shard_map.145 = bf16[256,128]{1,0:T(8,128)(2,1)} custom-call(bf16[256,256]{1,0:T(8,128)(2,1)} %convolution_convert_fusion.1.both, f32[4,128]{1,0:T(4,128)} %convert_element_type.75.taps, bf16[2,128,128]{2,1,0:T(8,128)(2,1)} %bitcast.47, bf16[2,128,128]{2,1,0:T(8,128)(2,1)} %bitcast.48, f32[2,128]{1,0:T(2,128)} %rate.1, f32[2,256,128]{2,1,0:T(8,128)} %extra.1), custom_call_target="tpu_custom_call" | custom-call | tf_op jit(solution)/shard_map/pallas_call | solution.py:187
  81.2 1.3 convolution_convert_fusion
  82.5 12.3 %all_to_all.46 = bf16[2,128,2048]{2,1,0:T(8,128)(2,1)S(1)} all-to-all(bf16[2,128,2048]{2,1,0:T(8,128)(2,1)S(1)} %bitcast.34), channel_id=1, replica_groups=mesh['zh'=4,'zl'=4,'y'=4,'x'=4,'c'=2] {'c'}, dimensions={0} | all-to-all | bytes 2097152 | tf_op jit(solution)/shard_map/all_to_all | solution.py:54
  95.9 4.0 %all-to-all-start.2 = ((bf16[4,32,2048]{2,1,0:T(8,128)(2,1)}), bf16[4,32,2048]{2,1,0:T(8,128)(2,1)S(1)}, u32[]{:S(2)}, u32[]{:S(2)}) async-start(bf16[4,32,2048]{2,1,0:T(8,128)(2,1)} %bitcast.9), calls=%async_computation.2 | async-start | bytes 1048576 | tf_op jit(solution)/shard_map/all_to_all | solution.py:57
  99.9 2.2 %collective-permute-start = (bf16[512,128]{1,0:T(8,128)(2,1)S(1)}, bf16[512,128]{1,0:T(8,128)(2,1)S(1)}, u32[]{:S(2)}, u32[]{:S(2)}) collective-permute-start(bf16[512,128]{1,0:T(8,128)(2,1)S(1)} %slice.32), channel_id=1, source_target_pairs={{0,8},{8,16},{16,24},{24,0},{1,9},{9,17},{17,25},{25,1},{2,10},{10... | collective-permute-start | bytes 393224 | tf_op jit(solution)/shard_map/ppermute | solution.py:34
  102.1 6.7 %all-to-all-done.2 = bf16[4,32,2048]{2,1,0:T(8,128)(2,1)S(1)} async-done(((bf16[4,32,2048]{2,1,0:T(8,128)(2,1)}), bf16[4,32,2048]{2,1,0:T(8,128)(2,1)S(1)}, u32[]{:S(2)}, u32[]{:S(2)}) %all-to-all-start.2) | async-done | bytes 524320 | tf_op jit(solution)/shard_map/all_to_all | solution.py:57
  110.3 3.5 %all-to-all-start.3 = ((bf16[4,32,2048]{2,1,0:T(8,128)(2,1)}), bf16[4,32,2048]{2,1,0:T(8,128)(2,1)S(1)}, u32[]{:S(2)}, u32[]{:S(2)}) async-start(bf16[4,32,2048]{2,1,0:T(8,128)(2,1)} %broadcast_in_dim.66), calls=%async_computation.3 | async-start | bytes 1048576 | tf_op jit(solution)/shard_map/all_to_all | solution.py:20
  113.7 2.3 %collective-permute-start.1 = (bf16[512,128]{1,0:T(8,128)(2,1)S(1)}, bf16[512,128]{1,0:T(8,128)(2,1)S(1)}, u32[]{:S(2)}, u32[]{:S(2)}) collective-permute-start(bf16[512,128]{1,0:T(8,128)(2,1)S(1)} %slice.32), channel_id=1, source_target_pairs={{0,16},{8,24},{16,0},{24,8},{1,17},{9,25},{17,1},{25,9},{2,18},{10... | collective-permute-start | bytes 393224 | tf_op jit(solution)/shard_map/ppermute | solution.py:34
  116.0 4.3 %collective-permute-start.2 = (bf16[512,128]{1,0:T(8,128)(2,1)S(1)}, bf16[512,128]{1,0:T(8,128)(2,1)S(1)}, u32[]{:S(2)}, u32[]{:S(2)}) collective-permute-start(bf16[512,128]{1,0:T(8,128)(2,1)S(1)} %slice.32), channel_id=1, source_target_pairs={{0,24},{8,0},{16,8},{24,16},{1,25},{9,1},{17,9},{25,17},{2,26},{10... | collective-permute-start | bytes 393224 | tf_op jit(solution)/shard_map/ppermute | solution.py:34
  121.0 2.5 %collective-permute-done.2 = bf16[512,128]{1,0:T(8,128)(2,1)S(1)} collective-permute-done((bf16[512,128]{1,0:T(8,128)(2,1)S(1)}, bf16[512,128]{1,0:T(8,128)(2,1)S(1)}, u32[]{:S(2)}, u32[]{:S(2)}) %collective-permute-start.2) | collective-permute-done | bytes 131104 | tf_op jit(solution)/shard_map/ppermute | solution.py:34
  123.7 5.6 %all_to_all.47 = bf16[2,4,32,2048]{3,2,1,0:T(8,128)(2,1)S(1)} all-to-all(bf16[2,4,32,2048]{3,2,1,0:T(8,128)(2,1)S(1)} %broadcast_in_dim.67), channel_id=1, replica_groups=mesh['zh'=4,'zl'=4,'y'=4,'x'=4,'c'=2] {'c'}, dimensions={0} | all-to-all | bytes 2097152 | tf_op jit(solution)/shard_map/all_to_all | solution.py:20
  129.8 3.4 %fusion.16 = bf16[256,896]{1,0:T(8,128)(2,1)S(1)} fusion(bf16[256,2048]{1,0:T(8,128)(2,1)S(1)} %bitcast.33, bf16[2048,1920]{1,0:T(8,128)(2,1)} %all-gather.2.cloned.1.call-done), kind=kOutput, calls=%fused_computation.13 | convolution fusion | flops 940212224 | bytes 5177344 | tf_op jit(solution)/shard_map/dot_general | solution.py:232
  134.1 1.3 fusion.4
  135.4 4.6 %all_to_all.48 = bf16[2,128,2048]{2,1,0:T(8,128)(2,1)S(1)} all-to-all(bf16[2,128,2048]{2,1,0:T(8,128)(2,1)S(1)} %bitcast.42), channel_id=1, replica_groups=mesh['zh'=4,'zl'=4,'y'=4,'x'=4,'c'=2] {'c'}, dimensions={0} | all-to-all | bytes 2097152 | tf_op jit(solution)/shard_map/all_to_all | solution.py:54
  140.3 12.9 %all_to_all.49 = bf16[4,32,2048]{2,1,0:T(8,128)(2,1)S(1)} all-to-all(bf16[4,32,2048]{2,1,0:T(8,128)(2,1)S(1)} %bitcast.40), channel_id=1, replica_groups=mesh['zh'=4,'zl'=4,'y'=4,'x'=4,'c'=2] {'x'}, dimensions={0} | all-to-all | bytes 1048576 | tf_op jit(solution)/shard_map/all_to_all | solution.py:57
  153.6 10.2 %all_to_all.50 = bf16[4,32,2048]{2,1,0:T(8,128)(2,1)S(1)} all-to-all(bf16[4,32,2048]{2,1,0:T(8,128)(2,1)S(1)} %broadcast_in_dim.69), channel_id=1, replica_groups=mesh['zh'=4,'zl'=4,'y'=4,'x'=4,'c'=2] {'x'}, dimensions={0} | all-to-all | bytes 1048576 | tf_op jit(solution)/shard_map/all_to_all | solution.py:20
  163.7 4.6 %collective-permute-start.3 = (bf16[128,2048]{1,0:T(8,128)(2,1)S(1)}, bf16[128,2048]{1,0:T(8,128)(2,1)S(1)}, u32[]{:S(2)}, u32[]{:S(2)}) collective-permute-start(bf16[128,2048]{1,0:T(8,128)(2,1)S(1)} %bitcast.37), channel_id=1, source_target_pairs={{0,1},{1,0},{2,3},{3,2},{4,5},{5,4},{6,7},{7,6},{8,9},{9,8},{10,11... | collective-permute-start | bytes 1572872 | tf_op jit(solution)/shard_map/ppermute | solution.py:63
  168.4 1.4 collective-permute-done.3
  (71 shorter events, 11.9 us)
Async XLA Ops:
  6.5 13.5 %slice-start = ((bf16[32,1024]{1,0:T(8,128)(2,1)}), bf16[32,128]{1,0:T(8,128)(2,1)S(1)}, s32[]{:S(2)}) async-start(bf16[32,1024]{1,0:T(8,128)(2,1)} %param.27), calls=%async_computation.10 | async-start | bytes 16384 | tf_op jit(solution)/shard_map/slice | solution.py:169
  6.5 13.5 %copy-start.2 = (bf16[128,32]{0,1:T(8,128)(2,1)S(1)}, bf16[128,32]{0,1:T(8,128)(2,1)}, u32[]{:S(2)}) copy-start(bf16[128,32]{0,1:T(8,128)(2,1)} %param.24) | copy-start | bytes 24580
  6.5 13.5 %copy-start.4 = (bf16[32,128]{1,0:T(8,128)(2,1)S(1)}, bf16[32,128]{1,0:T(8,128)(2,1)}, u32[]{:S(2)}) copy-start(bf16[32,128]{1,0:T(8,128)(2,1)} %param.17) | copy-start | bytes 24580
  6.5 13.5 %copy-start.3 = (bf16[32,128]{1,0:T(8,128)(2,1)S(1)}, bf16[32,128]{1,0:T(8,128)(2,1)}, u32[]{:S(2)}) copy-start(bf16[32,128]{1,0:T(8,128)(2,1)} %param.18) | copy-start | bytes 24580
  6.5 123.2 %all-gather.2.cloned.1.call-start = ((), (), s32[]{:S(2)}) async-start(), calls=%async_computation.9 | async-start | bytes 8355840 | tf_op jit(solution)/shard_map/all_gather | solution.py:47
  58.8 3.8 %copy-start.5 = (bf16[2048]{0:T(1024)(128)(2,1)S(1)}, bf16[2048]{0:T(1024)(128)(2,1)}, u32[]{:S(2)}) copy-start(bf16[2048]{0:T(1024)(128)(2,1)} %param.16) | copy-start | bytes 12292
  58.8 3.8 %copy-start = (bf16[256,2048]{1,0:T(8,128)(2,1)S(1)}, bf16[256,2048]{1,0:T(8,128)(2,1)}, u32[]{:S(2)}) copy-start(bf16[256,2048]{1,0:T(8,128)(2,1)} %param.15) | copy-start | bytes 3145732
  58.8 17.2 %all-to-all-start = ((bf16[4,512,384]{2,1,0:T(8,128)(2,1)}), bf16[4,512,384]{2,1,0:T(8,128)(2,1)S(1)}, u32[]{:S(2)}, u32[]{:S(2)}) async-start(bf16[4,512,384]{2,1,0:T(8,128)(2,1)} %broadcast_in_dim.65), calls=%async_computation | async-start | bytes 3145728 | tf_op jit(solution)/shard_map/all_to_all | solution.py:20
  62.5 1.7 copy-start.9
  62.5 2.3 %copy-start.6 = (bf16[2048]{0:T(1024)(128)(2,1)S(1)}, bf16[2048]{0:T(1024)(128)(2,1)}, u32[]{:S(2)}) copy-start(bf16[2048]{0:T(1024)(128)(2,1)} %param.25) | copy-start | bytes 12292
  62.5 2.3 %copy-start.7 = (bf16[2048]{0:T(1024)(128)(2,1)S(1)}, bf16[2048]{0:T(1024)(128)(2,1)}, u32[]{:S(2)}) copy-start(bf16[2048]{0:T(1024)(128)(2,1)} %param.26) | copy-start | bytes 12292
  62.5 2.3 %copy-start.8 = (bf16[2048]{0:T(1024)(128)(2,1)S(1)}, bf16[2048]{0:T(1024)(128)(2,1)}, u32[]{:S(2)}) copy-start(bf16[2048]{0:T(1024)(128)(2,1)} %param.29) | copy-start | bytes 12292
  76.0 1.2 copy-start.1
  95.9 12.9 %all-to-all-start.2 = ((bf16[4,32,2048]{2,1,0:T(8,128)(2,1)}), bf16[4,32,2048]{2,1,0:T(8,128)(2,1)S(1)}, u32[]{:S(2)}, u32[]{:S(2)}) async-start(bf16[4,32,2048]{2,1,0:T(8,128)(2,1)} %bitcast.9), calls=%async_computation.2 | async-start | bytes 1048576 | tf_op jit(solution)/shard_map/all_to_all | solution.py:57
  99.9 20.4 %collective-permute-start = (bf16[512,128]{1,0:T(8,128)(2,1)S(1)}, bf16[512,128]{1,0:T(8,128)(2,1)S(1)}, u32[]{:S(2)}, u32[]{:S(2)}) collective-permute-start(bf16[512,128]{1,0:T(8,128)(2,1)S(1)} %slice.32), channel_id=1, source_target_pairs={{0,8},{8,16},{16,24},{24,0},{1,9},{9,17},{17,25},{25,1},{2,10},{10... | collective-permute-start | bytes 393224 | tf_op jit(solution)/shard_map/ppermute | solution.py:34
  110.3 13.3 %all-to-all-start.3 = ((bf16[4,32,2048]{2,1,0:T(8,128)(2,1)}), bf16[4,32,2048]{2,1,0:T(8,128)(2,1)S(1)}, u32[]{:S(2)}, u32[]{:S(2)}) async-start(bf16[4,32,2048]{2,1,0:T(8,128)(2,1)} %broadcast_in_dim.66), calls=%async_computation.3 | async-start | bytes 1048576 | tf_op jit(solution)/shard_map/all_to_all | solution.py:20
  113.7 7.3 %collective-permute-start.1 = (bf16[512,128]{1,0:T(8,128)(2,1)S(1)}, bf16[512,128]{1,0:T(8,128)(2,1)S(1)}, u32[]{:S(2)}, u32[]{:S(2)}) collective-permute-start(bf16[512,128]{1,0:T(8,128)(2,1)S(1)} %slice.32), channel_id=1, source_target_pairs={{0,16},{8,24},{16,0},{24,8},{1,17},{9,25},{17,1},{25,9},{2,18},{10... | collective-permute-start | bytes 393224 | tf_op jit(solution)/shard_map/ppermute | solution.py:34
  116.0 7.5 %collective-permute-start.2 = (bf16[512,128]{1,0:T(8,128)(2,1)S(1)}, bf16[512,128]{1,0:T(8,128)(2,1)S(1)}, u32[]{:S(2)}, u32[]{:S(2)}) collective-permute-start(bf16[512,128]{1,0:T(8,128)(2,1)S(1)} %slice.32), channel_id=1, source_target_pairs={{0,24},{8,0},{16,8},{24,16},{1,25},{9,1},{17,9},{25,17},{2,26},{10... | collective-permute-start | bytes 393224 | tf_op jit(solution)/shard_map/ppermute | solution.py:34
  129.8 4.4 %copy-start.10 = (bf16[2048,1920]{1,0:T(8,128)(2,1)S(1)}, bf16[2048,1920]{1,0:T(8,128)(2,1)}, u32[]{:S(2)}) copy-start(bf16[2048,1920]{1,0:T(8,128)(2,1)} %all-gather.2.cloned.1.call-done) | copy-start | bytes 23592964
  163.7 6.1 %collective-permute-start.3 = (bf16[128,2048]{1,0:T(8,128)(2,1)S(1)}, bf16[128,2048]{1,0:T(8,128)(2,1)S(1)}, u32[]{:S(2)}, u32[]{:S(2)}) collective-permute-start(bf16[128,2048]{1,0:T(8,128)(2,1)S(1)} %bitcast.37), channel_id=1, source_target_pairs={{0,1},{1,0},{2,3},{3,2},{4,5},{5,4},{6,7},{7,6},{8,9},{9,8},{10,11... | collective-permute-start | bytes 1572872 | tf_op jit(solution)/shard_map/ppermute | solution.py:63
Sparse Core Ops, SparseCore 0:
  20.1 108.3 all-gather.1

commit v3 on v2

--- a/solution.py
+++ b/solution.py
@@ -47,20 +47,22 @@
     return lax.all_gather(near, Z, axis=0, tiled=True)
 
 
-def summed_rows(partial):
-    cores, wide = lax.axis_size("c"), lax.axis_size("x")
-    rows, width = partial.shape
-    halves = partial.astype(jnp.bfloat16).reshape(cores, rows // cores, width)
-    pair = lax.all_to_all(halves, "c", split_axis=0, concat_axis=0, tiled=True)
-    half = jnp.sum(pair.astype(jnp.float32), axis=0).astype(jnp.bfloat16)
-    quarters = half.reshape(wide, rows // (cores * wide), width)
+CORES = [(0, 1), (1, 0)]
+
+
+def summed_rows(rows_of, mine, others):
+    sent = lax.ppermute(rows_of(others).astype(jnp.bfloat16), "c", CORES)
+    kept = lax.optimization_barrier(rows_of(mine))
+    half = (kept + sent.astype(jnp.float32)).astype(jnp.bfloat16)
+    wide = lax.axis_size("x")
+    quarters = half.reshape(wide, half.shape[0] // wide, half.shape[1])
     several = lax.all_to_all(quarters, "x", split_axis=0, concat_axis=0, tiled=True)
     return jnp.sum(several.astype(jnp.float32), axis=0)
 
 
 def all_rows(part):
     half = spread(part, "x").reshape(-1, part.shape[-1])
-    other = lax.ppermute(half, "c", [(0, 1), (1, 0)])
+    other = lax.ppermute(half, "c", CORES)
     mine = lax.broadcasted_iota(jnp.int32, (2, 1, 1), 0) == lax.axis_index("c")
     return jnp.where(mine, half[None], other[None]).reshape(-1, part.shape[-1])
 
@@ -157,9 +159,13 @@
     hidden_units = feedforward_up_weight.shape[1]
     rows = recurrent_branch_weight.shape[0]
     early = hidden_units - channels
-    forward = feedforward_weights(
-        jnp.concatenate((feedforward_up_weight[:, :early], feedforward_down_weight.T), axis=1)
-    )
+    lowest = jnp.array(-jnp.inf, jnp.bfloat16)
+    down_rows = feedforward_down_weight.T
+    fed = jnp.maximum(
+        lax.pad(down_rows, lowest, ((0, 0, 0), (0, early, 0))),
+        lax.pad(feedforward_up_weight, lowest, ((0, 0, 0), (hidden_units, early - hidden_units, 0))),
+    )
+    forward = feedforward_weights(fed)
     column = lax.all_gather(
         jnp.concatenate(
             (
@@ -195,9 +201,7 @@
         position_log_decay,
     )
     across = (((1,), (1,)), ((), ()))
-    partial_value = lax.dot_general(
-        hidden, mixer[:, 2 * channels :], across, preferred_element_type=jnp.float32
-    )
+
     share = tokens.shape[0] // lax.axis_size(TP)
     place = lax.axis_index("c") * lax.axis_size("x") + lax.axis_index("x")
     own = lax.dynamic_slice_in_dim(tokens, place * share, share, axis=0)
@@ -207,36 +211,49 @@
     late_width = late[0].shape[1]
     late_up = jnp.zeros((late[0].shape[0] // rows, span, rows, late_width), jnp.bfloat16)
     late_up = set_in(late_up, late[0], places[0])
-    late_up, places, own, partial_value, mixer_gain, norm_gain, out_gain = lax.optimization_barrier(
+    late_up, places, own, hidden, mixer_gain, norm_gain, out_gain = lax.optimization_barrier(
         (
             late_up,
             places,
             own,
-            partial_value.astype(jnp.bfloat16),
+            hidden,
             recurrent_output_gain.astype(jnp.float32),
             feedforward_norm_gain.astype(jnp.float32),
             feedforward_output_gain.astype(jnp.float32),
         )
     )
-    mixed = summed_rows(partial_value)
+    part_rows = tokens.shape[0] // 2
+    core = lax.axis_index("c").astype(jnp.uint32)
+    mixed = summed_rows(
+        lambda these: lax.dot_general(
+            these, mixer[:, 2 * channels :], across, preferred_element_type=jnp.float32
+        ),
+        lax.dynamic_slice_in_dim(hidden, core * part_rows, part_rows, axis=0),
+        lax.dynamic_slice_in_dim(hidden, (1 - core) * part_rows, part_rows, axis=0),
+    )
     stream = lax.optimization_barrier(
         (own.astype(jnp.float32) + root_norm(mixed, mixer_gain)).astype(jnp.bfloat16)
     )
     half = spread(root_norm(stream.astype(jnp.float32), norm_gain).astype(jnp.bfloat16), "x")
     half = lax.optimization_barrier(half)
-    normed_ff = spread(half, "c").reshape(tokens.shape)
+    half = half.reshape(part_rows, -1)
+    normed_ff = jnp.concatenate((half, lax.ppermute(half, "c", CORES)), axis=0)
     for piece, spot in zip(late[1:], places[1:]):
         late_up = set_in(late_up, piece, spot)
     lifted = [
         jnp.square(
             jax.nn.relu(jnp.dot(normed_ff, weight, preferred_element_type=jnp.float32))
         ).astype(jnp.bfloat16)
-        for weight in (forward[:, :early], late_up.reshape(-1, late_width))
+        for weight in (forward[:, hidden_units:], late_up.reshape(-1, late_width))
     ]
-    lowered_part = lax.dot_general(
-        jnp.concatenate(lifted, axis=1), forward[:, early:], across, preferred_element_type=jnp.float32
-    )
-    lowered = summed_rows(lowered_part)
+    lifted = jnp.concatenate(lifted, axis=1)
+    lowered = summed_rows(
+        lambda these: lax.dot_general(
+            these, forward[:, :hidden_units], across, preferred_element_type=jnp.float32
+        ),
+        lifted[:part_rows],
+        lifted[part_rows:],
+    )
     return all_rows(
         (stream.astype(jnp.float32) + root_norm(lowered, out_gain)).astype(
             jnp.bfloat16

time: 179 us -> 183 us (1.022)
  starting transfers between devices: 24.5 us -> 33.6 us
  waiting for transfers between devices: 22.4 us -> 18 us
  matrix products: 7.53 us -> 10.1 us
    all_to_all x2 -> x0, blocking collectives: 16.9 us -> none  [summed_rows(): pair = lax.all_to_all(halves, 'c', split_axis=0, concat_axis=0, tiled=True)]
    ppermute x1 -> x4, starting transfers between devices: 4.56 us -> 21.4 us  [the longest x2 12.9 us: summed_rows(): sent = lax.ppermute(rows_of(others).astype(jnp.bfloat16), 'c', CORES)]
    all_to_all x1 -> x2, blocking collectives: 12.9 us -> 24.1 us  [summed_rows(): lax.all_to_all(quarters, 'x', split_axis=0, concat_axis=0, tiled=True)]
    all_to_all x1 -> x0, waiting for transfers between devices: 6.7 us -> none  [summed_rows(): lax.all_to_all(quarters, 'x', split_axis=0, concat_axis=0, tiled=True)]
    all_to_all x3, blocking collectives: 27.5 us -> 32.6 us  [spread(): return lax.all_to_all(copies, axis, split_axis=0, concat_axis=0, tiled=True)]
    all_to_all x1 -> x0, starting transfers between devices: 3.97 us -> none  [summed_rows(): lax.all_to_all(quarters, 'x', split_axis=0, concat_axis=0, tiled=True)]
    all_to_all x2 -> x1, starting transfers between devices: 7.17 us -> 3.7 us  [spread(): return lax.all_to_all(copies, axis, split_axis=0, concat_axis=0, tiled=True)]
    dot_general x2 -> x4, matrix products: 2.55 us -> 5.08 us  [the longest x2 2.97 us: per_device(): lax.dot_general(these, forward[:, :hidden_units], across, preferred_eleme...]
  transfers between devices with their start and end apart: 8 -> 9, of which waited for: 5 -> 5; matrix products, arithmetic and copies ran while one was open for 5% -> 6% of each run, Pallas kernels for 2% -> 2%
where the time goes in v3:
time: 183 us
  blocking collectives  94 us (51%)
  starting transfers between devices  33.6 us (18%)
  waiting for transfers between devices  18 us (10%)
  between operations  13.8 us (8%)
  matrix products  10.1 us (6%)
  other arithmetic  6.39 us (3%)
  local copies, waits for them, and re-layouts  3.98 us (2%)
  Pallas kernels  2.74 us (1%)
    all_gather x1, blocking collectives, per_device(): lax.all_gather(jnp.concatenate((recurrent_branch_weight, output_gate_weig...  37.3 us
    all_to_all x3, blocking collectives, spread(): return lax.all_to_all(copies, axis, split_axis=0, concat_axis=0, tiled=True)  32.6 us
    all_to_all x2, blocking collectives, summed_rows(): lax.all_to_all(quarters, 'x', split_axis=0, concat_axis=0, tiled=True)  24.1 us
    ppermute x2, starting transfers between devices, summed_rows(): sent = lax.ppermute(rows_of(others).astype(jnp.bfloat16), 'c', CORES)  12.9 us
    all_to_all x1, waiting for transfers between devices, spread(): return lax.all_to_all(copies, axis, split_axis=0, concat_axis=0, tiled=True)  11.1 us
    ppermute x3, starting transfers between devices, sent_round(): pieces.append(lax.ppermute(array, axis, ring))  8.41 us
    ppermute x3, waiting for transfers between devices, sent_round(): pieces.append(lax.ppermute(array, axis, ring))  4.83 us
    ppermute x1, starting transfers between devices, per_device(): normed_ff = jnp.concatenate((half, lax.ppermute(half, 'c', CORES)), axis=0)  4.5 us
  transfers between devices with their start and end apart: 9, of which 5 were waited for; matrix products, arithmetic and copies ran while one was open for 6% of the time, Pallas kernels for 2%

profile of v3, /device:TPU:1, one launch (start us, length us, event | category | flops | bytes accessed | tf_op | source)
XLA Modules:
  0.0 182.6 jit_solution(1515364840292070651)
XLA Ops:
  7.5 11.7 %all_to_all.30 = bf16[4,32,1920]{2,1,0:T(8,128)(2,1)} all-to-all(bf16[4,32,1920]{2,1,0:T(8,128)(2,1)S(1)} %broadcast_in_dim.64), channel_id=1, replica_groups=mesh['zh'=4,'zl'=4,'y'=4,'x'=4,'c'=2] {'y'}, dimensions={0} | all-to-all | bytes 983040 | tf_op jit(solution)/shard_map/all_to_all | solution.py:20
  19.3 37.3 %all_gather.6 = bf16[512,512]{1,0:T(8,128)(2,1)S(1)} all-gather(bf16[32,512]{1,0:T(8,128)(2,1)S(1)} %pad_maximum_fusion.5), channel_id=1, replica_groups=mesh['zh'=4,'zl'=4,'y'=4,'x'=4,'c'=2] {'zh','zl'}, dimensions={0}, use_global_device_ids=true | all-gather | bytes 557056 | tf_op jit(solution)/shard_map/all_gather | solution.py:169
  56.6 1.4 broadcast_in_dim.62
  58.0 3.7 %all-to-all-start = ((bf16[4,512,384]{2,1,0:T(8,128)(2,1)}), bf16[4,512,384]{2,1,0:T(8,128)(2,1)S(1)}, u32[]{:S(2)}, u32[]{:S(2)}) async-start(bf16[4,512,384]{2,1,0:T(8,128)(2,1)} %broadcast_in_dim.62), calls=%async_computation | async-start | bytes 3145728 | tf_op jit(solution)/shard_map/all_to_all | solution.py:20
  62.1 1.3 fusion.11
  64.0 11.1 %all-to-all-done = bf16[4,512,384]{2,1,0:T(8,128)(2,1)S(1)} async-done(((bf16[4,512,384]{2,1,0:T(8,128)(2,1)}), bf16[4,512,384]{2,1,0:T(8,128)(2,1)S(1)}, u32[]{:S(2)}, u32[]{:S(2)}) %all-to-all-start) | async-done | bytes 1572896 | tf_op jit(solution)/shard_map/all_to_all | solution.py:20
  77.5 2.7 %shard_map.145 = bf16[256,128]{1,0:T(8,128)(2,1)} custom-call(bf16[256,256]{1,0:T(8,128)(2,1)} %convolution_convert_fusion.1.both, f32[4,128]{1,0:T(4,128)} %convert_element_type.86.taps, bf16[2,128,128]{2,1,0:T(8,128)(2,1)} %bitcast.43, bf16[2,128,128]{2,1,0:T(8,128)(2,1)} %bitcast.44, f32[2,128]{1,0:T(2,128)} %rate.1, f32[2,256,128]{2,1,0:T(8,128)} %extra.1), custom_call_target="tpu_custom_call" | custom-call | tf_op jit(solution)/shard_map/pallas_call | solution.py:193
  81.4 10.0 %collective-permute-start = (bf16[128,2048]{1,0:T(8,128)(2,1)S(1)}, bf16[128,2048]{1,0:T(8,128)(2,1)}, u32[]{:S(2)}, u32[]{:S(2)}) collective-permute-start(bf16[128,2048]{1,0:T(8,128)(2,1)S(1)} %convolution_convert_fusion), channel_id=1, source_target_pairs={{0,1},{1,0},{2,3},{3,2},{4,5},{5,4},{6,7},{7,6},{8,9},{9,8},{10,11... | collective-permute-start | bytes 1572872 | tf_op jit(solution)/shard_map/ppermute | solution.py:54
  94.3 12.5 %all_to_all.31 = bf16[4,32,2048]{2,1,0:T(8,128)(2,1)S(1)} all-to-all(bf16[4,32,2048]{2,1,0:T(8,128)(2,1)S(1)} %bitcast.32), channel_id=1, replica_groups=mesh['zh'=4,'zl'=4,'y'=4,'x'=4,'c'=2] {'x'}, dimensions={0} | all-to-all | bytes 1048576 | tf_op jit(solution)/shard_map/all_to_all | solution.py:59
  107.4 10.2 %all_to_all.32 = bf16[4,32,2048]{2,1,0:T(8,128)(2,1)S(1)} all-to-all(bf16[4,32,2048]{2,1,0:T(8,128)(2,1)S(1)} %broadcast_in_dim.63), channel_id=1, replica_groups=mesh['zh'=4,'zl'=4,'y'=4,'x'=4,'c'=2] {'x'}, dimensions={0} | all-to-all | bytes 1048576 | tf_op jit(solution)/shard_map/all_to_all | solution.py:20
  117.7 4.5 %collective-permute-start.1 = (bf16[128,2048]{1,0:T(8,128)(2,1)S(1)}, bf16[128,2048]{1,0:T(8,128)(2,1)S(1)}, u32[]{:S(2)}, u32[]{:S(2)}) collective-permute-start(bf16[128,2048]{1,0:T(8,128)(2,1)S(1)} %bitcast.36), channel_id=1, source_target_pairs={{0,1},{1,0},{2,3},{3,2},{4,5},{5,4},{6,7},{7,6},{8,9},{9,8},{10,11... | collective-permute-start | bytes 1572872 | tf_op jit(solution)/shard_map/ppermute | solution.py:240
  122.2 2.2 %collective-permute-start.2 = (bf16[512,128]{1,0:T(8,128)(2,1)S(1)}, bf16[512,128]{1,0:T(8,128)(2,1)S(1)}, u32[]{:S(2)}, u32[]{:S(2)}) collective-permute-start(bf16[512,128]{1,0:T(8,128)(2,1)S(1)} %slice.39), channel_id=1, source_target_pairs={{0,8},{8,16},{16,24},{24,0},{1,9},{9,17},{17,25},{25,1},{2,10},{10... | collective-permute-start | bytes 393224 | tf_op jit(solution)/shard_map/ppermute | solution.py:34
  124.4 3.7 %collective-permute-start.3 = (bf16[512,128]{1,0:T(8,128)(2,1)S(1)}, bf16[512,128]{1,0:T(8,128)(2,1)S(1)}, u32[]{:S(2)}, u32[]{:S(2)}) collective-permute-start(bf16[512,128]{1,0:T(8,128)(2,1)S(1)} %slice.39), channel_id=1, source_target_pairs={{0,16},{8,24},{16,0},{24,8},{1,17},{9,25},{17,1},{25,9},{2,18},{10... | collective-permute-start | bytes 393224 | tf_op jit(solution)/shard_map/ppermute | solution.py:34
  128.1 2.5 %collective-permute-start.4 = (bf16[512,128]{1,0:T(8,128)(2,1)S(1)}, bf16[512,128]{1,0:T(8,128)(2,1)S(1)}, u32[]{:S(2)}, u32[]{:S(2)}) collective-permute-start(bf16[512,128]{1,0:T(8,128)(2,1)S(1)} %slice.39), channel_id=1, source_target_pairs={{0,24},{8,0},{16,8},{24,16},{1,25},{9,1},{17,9},{25,17},{2,26},{10... | collective-permute-start | bytes 393224 | tf_op jit(solution)/shard_map/ppermute | solution.py:34
  130.6 1.9 %collective-permute-done.3 = bf16[512,128]{1,0:T(8,128)(2,1)S(1)} collective-permute-done((bf16[512,128]{1,0:T(8,128)(2,1)S(1)}, bf16[512,128]{1,0:T(8,128)(2,1)S(1)}, u32[]{:S(2)}, u32[]{:S(2)}) %collective-permute-start.3) | collective-permute-done | bytes 131104 | tf_op jit(solution)/shard_map/ppermute | solution.py:34
  132.6 2.9 %collective-permute-done.4 = bf16[512,128]{1,0:T(8,128)(2,1)S(1)} collective-permute-done((bf16[512,128]{1,0:T(8,128)(2,1)S(1)}, bf16[512,128]{1,0:T(8,128)(2,1)S(1)}, u32[]{:S(2)}, u32[]{:S(2)}) %collective-permute-start.4) | collective-permute-done | bytes 131104 | tf_op jit(solution)/shard_map/ppermute | solution.py:34
  136.0 3.4 %fusion.18 = bf16[256,896]{1,0:T(8,128)(2,1)S(1)} fusion(bf16[2048,1920]{1,0:T(8,128)(2,1)} %all-gather.2.cloned.1.call-done, bf16[128,2048]{1,0:T(8,128)(2,1)S(1)} %collective-permute-done.1, bf16[128,2048]{1,0:T(8,128)(2,1)S(1)} %bitcast.38), kind=kOutput, calls=%fused_computation.15 | convolution fusion | flops 942309376 | bytes 5177344 | tf_op jit(solution)/shard_map/dot_general | solution.py:245
  140.3 1.5 fusion.6
  141.8 2.9 %collective-permute-start.5 = (bf16[128,2048]{1,0:T(8,128)(2,1)S(1)}, bf16[128,2048]{1,0:T(8,128)(2,1)S(1)}, u32[]{:S(2)}, u32[]{:S(2)}) collective-permute-start(bf16[128,2048]{1,0:T(8,128)(2,1)S(1)} %fusion.6), channel_id=1, source_target_pairs={{0,1},{1,0},{2,3},{3,2},{4,5},{5,4},{6,7},{7,6},{8,9},{9,8},{10,11... | collective-permute-start | bytes 1572872 | tf_op jit(solution)/shard_map/ppermute | solution.py:54
  144.7 1.5 fusion.2
  146.4 11.6 %all_to_all.33 = bf16[4,32,2048]{2,1,0:T(8,128)(2,1)S(1)} all-to-all(bf16[4,32,2048]{2,1,0:T(8,128)(2,1)S(1)} %bitcast.33), channel_id=1, replica_groups=mesh['zh'=4,'zl'=4,'y'=4,'x'=4,'c'=2] {'x'}, dimensions={0} | all-to-all | bytes 1048576 | tf_op jit(solution)/shard_map/all_to_all | solution.py:59
  158.4 10.7 %all_to_all.34 = bf16[4,32,2048]{2,1,0:T(8,128)(2,1)S(1)} all-to-all(bf16[4,32,2048]{2,1,0:T(8,128)(2,1)S(1)} %broadcast_in_dim.65), channel_id=1, replica_groups=mesh['zh'=4,'zl'=4,'y'=4,'x'=4,'c'=2] {'x'}, dimensions={0} | all-to-all | bytes 1048576 | tf_op jit(solution)/shard_map/all_to_all | solution.py:20
  169.1 4.0 %collective-permute-start.6 = (bf16[128,2048]{1,0:T(8,128)(2,1)S(1)}, bf16[128,2048]{1,0:T(8,128)(2,1)S(1)}, u32[]{:S(2)}, u32[]{:S(2)}) collective-permute-start(bf16[128,2048]{1,0:T(8,128)(2,1)S(1)} %bitcast.30), channel_id=1, source_target_pairs={{0,1},{1,0},{2,3},{3,2},{4,5},{5,4},{6,7},{7,6},{8,9},{9,8},{10,11... | collective-permute-start | bytes 1572872 | tf_op jit(solution)/shard_map/ppermute | solution.py:65
  173.2 1.4 collective-permute-done.6
  (72 shorter events, 12.1 us)
Async XLA Ops:
  6.5 12.7 %slice-start = ((bf16[32,1024]{1,0:T(8,128)(2,1)}), bf16[32,128]{1,0:T(8,128)(2,1)S(1)}, s32[]{:S(2)}) async-start(bf16[32,1024]{1,0:T(8,128)(2,1)} %param.27), calls=%async_computation.7 | async-start | bytes 16384 | tf_op jit(solution)/shard_map/slice | solution.py:175
  6.5 12.7 %copy-start.2 = (bf16[128,32]{0,1:T(8,128)(2,1)S(1)}, bf16[128,32]{0,1:T(8,128)(2,1)}, u32[]{:S(2)}) copy-start(bf16[128,32]{0,1:T(8,128)(2,1)} %param.24) | copy-start | bytes 24580
  6.5 12.7 %copy-start.4 = (bf16[32,128]{1,0:T(8,128)(2,1)S(1)}, bf16[32,128]{1,0:T(8,128)(2,1)}, u32[]{:S(2)}) copy-start(bf16[32,128]{1,0:T(8,128)(2,1)} %param.17) | copy-start | bytes 24580
  6.5 12.7 %copy-start.3 = (bf16[32,128]{1,0:T(8,128)(2,1)S(1)}, bf16[32,128]{1,0:T(8,128)(2,1)}, u32[]{:S(2)}) copy-start(bf16[32,128]{1,0:T(8,128)(2,1)} %param.18) | copy-start | bytes 24580
  6.5 129.4 %all-gather.2.cloned.1.call-start = ((), (), s32[]{:S(2)}) async-start(), calls=%async_computation.6 | async-start | bytes 8355840 | tf_op jit(solution)/shard_map/all_gather | solution.py:47
  58.0 3.8 %copy-start.5 = (bf16[2048]{0:T(1024)(128)(2,1)S(1)}, bf16[2048]{0:T(1024)(128)(2,1)}, u32[]{:S(2)}) copy-start(bf16[2048]{0:T(1024)(128)(2,1)} %param.16) | copy-start | bytes 12292
  58.0 3.8 %copy-start = (bf16[256,2048]{1,0:T(8,128)(2,1)S(1)}, bf16[256,2048]{1,0:T(8,128)(2,1)}, u32[]{:S(2)}) copy-start(bf16[256,2048]{1,0:T(8,128)(2,1)} %param.15) | copy-start | bytes 3145732
  58.0 17.2 %all-to-all-start = ((bf16[4,512,384]{2,1,0:T(8,128)(2,1)}), bf16[4,512,384]{2,1,0:T(8,128)(2,1)S(1)}, u32[]{:S(2)}, u32[]{:S(2)}) async-start(bf16[4,512,384]{2,1,0:T(8,128)(2,1)} %broadcast_in_dim.62), calls=%async_computation | async-start | bytes 3145728 | tf_op jit(solution)/shard_map/all_to_all | solution.py:20
  61.7 1.7 copy-start.9
  61.7 2.3 %copy-start.6 = (bf16[2048]{0:T(1024)(128)(2,1)S(1)}, bf16[2048]{0:T(1024)(128)(2,1)}, u32[]{:S(2)}) copy-start(bf16[2048]{0:T(1024)(128)(2,1)} %param.25) | copy-start | bytes 12292
  61.7 2.3 %copy-start.7 = (bf16[2048]{0:T(1024)(128)(2,1)S(1)}, bf16[2048]{0:T(1024)(128)(2,1)}, u32[]{:S(2)}) copy-start(bf16[2048]{0:T(1024)(128)(2,1)} %param.26) | copy-start | bytes 12292
  61.7 2.3 %copy-start.8 = (bf16[2048]{0:T(1024)(128)(2,1)S(1)}, bf16[2048]{0:T(1024)(128)(2,1)}, u32[]{:S(2)}) copy-start(bf16[2048]{0:T(1024)(128)(2,1)} %param.29) | copy-start | bytes 12292
  75.2 1.2 copy-start.1
  81.4 11.7 %collective-permute-start = (bf16[128,2048]{1,0:T(8,128)(2,1)S(1)}, bf16[128,2048]{1,0:T(8,128)(2,1)}, u32[]{:S(2)}, u32[]{:S(2)}) collective-permute-start(bf16[128,2048]{1,0:T(8,128)(2,1)S(1)} %convolution_convert_fusion), channel_id=1, source_target_pairs={{0,1},{1,0},{2,3},{3,2},{4,5},{5,4},{6,7},{7,6},{8,9},{9,8},{10,11... | collective-permute-start | bytes 1572872 | tf_op jit(solution)/shard_map/ppermute | solution.py:54
  117.7 17.9 %collective-permute-start.1 = (bf16[128,2048]{1,0:T(8,128)(2,1)S(1)}, bf16[128,2048]{1,0:T(8,128)(2,1)S(1)}, u32[]{:S(2)}, u32[]{:S(2)}) collective-permute-start(bf16[128,2048]{1,0:T(8,128)(2,1)S(1)} %bitcast.36), channel_id=1, source_target_pairs={{0,1},{1,0},{2,3},{3,2},{4,5},{5,4},{6,7},{7,6},{8,9},{9,8},{10,11... | collective-permute-start | bytes 1572872 | tf_op jit(solution)/shard_map/ppermute | solution.py:240
  122.2 8.4 %collective-permute-start.2 = (bf16[512,128]{1,0:T(8,128)(2,1)S(1)}, bf16[512,128]{1,0:T(8,128)(2,1)S(1)}, u32[]{:S(2)}, u32[]{:S(2)}) collective-permute-start(bf16[512,128]{1,0:T(8,128)(2,1)S(1)} %slice.39), channel_id=1, source_target_pairs={{0,8},{8,16},{16,24},{24,0},{1,9},{9,17},{17,25},{25,1},{2,10},{10... | collective-permute-start | bytes 393224 | tf_op jit(solution)/shard_map/ppermute | solution.py:34
  124.4 8.2 %collective-permute-start.3 = (bf16[512,128]{1,0:T(8,128)(2,1)S(1)}, bf16[512,128]{1,0:T(8,128)(2,1)S(1)}, u32[]{:S(2)}, u32[]{:S(2)}) collective-permute-start(bf16[512,128]{1,0:T(8,128)(2,1)S(1)} %slice.39), channel_id=1, source_target_pairs={{0,16},{8,24},{16,0},{24,8},{1,17},{9,25},{17,1},{25,9},{2,18},{10... | collective-permute-start | bytes 393224 | tf_op jit(solution)/shard_map/ppermute | solution.py:34
  128.1 7.4 %collective-permute-start.4 = (bf16[512,128]{1,0:T(8,128)(2,1)S(1)}, bf16[512,128]{1,0:T(8,128)(2,1)S(1)}, u32[]{:S(2)}, u32[]{:S(2)}) collective-permute-start(bf16[512,128]{1,0:T(8,128)(2,1)S(1)} %slice.39), channel_id=1, source_target_pairs={{0,24},{8,0},{16,8},{24,16},{1,25},{9,1},{17,9},{25,17},{2,26},{10... | collective-permute-start | bytes 393224 | tf_op jit(solution)/shard_map/ppermute | solution.py:34
  136.0 4.4 %copy-start.10 = (bf16[2048,1920]{1,0:T(8,128)(2,1)S(1)}, bf16[2048,1920]{1,0:T(8,128)(2,1)}, u32[]{:S(2)}) copy-start(bf16[2048,1920]{1,0:T(8,128)(2,1)} %all-gather.2.cloned.1.call-done) | copy-start | bytes 23592964
  141.8 4.4 %collective-permute-start.5 = (bf16[128,2048]{1,0:T(8,128)(2,1)S(1)}, bf16[128,2048]{1,0:T(8,128)(2,1)S(1)}, u32[]{:S(2)}, u32[]{:S(2)}) collective-permute-start(bf16[128,2048]{1,0:T(8,128)(2,1)S(1)} %fusion.6), channel_id=1, source_target_pairs={{0,1},{1,0},{2,3},{3,2},{4,5},{5,4},{6,7},{7,6},{8,9},{9,8},{10,11... | collective-permute-start | bytes 1572872 | tf_op jit(solution)/shard_map/ppermute | solution.py:54
  169.1 5.5 %collective-permute-start.6 = (bf16[128,2048]{1,0:T(8,128)(2,1)S(1)}, bf16[128,2048]{1,0:T(8,128)(2,1)S(1)}, u32[]{:S(2)}, u32[]{:S(2)}) collective-permute-start(bf16[128,2048]{1,0:T(8,128)(2,1)S(1)} %bitcast.30), channel_id=1, source_target_pairs={{0,1},{1,0},{2,3},{3,2},{4,5},{5,4},{6,7},{7,6},{8,9},{9,8},{10,11... | collective-permute-start | bytes 1572872 | tf_op jit(solution)/shard_map/ppermute | solution.py:65
Sparse Core Ops, SparseCore 0:
  19.3 108.3 all-gather.1

commit v4 on v3

--- a/solution.py
+++ b/solution.py
@@ -158,7 +158,7 @@
     channels = recurrent_branch_weight.shape[1]
     hidden_units = feedforward_up_weight.shape[1]
     rows = recurrent_branch_weight.shape[0]
-    early = hidden_units - channels
+    early = hidden_units - 2 * channels
     lowest = jnp.array(-jnp.inf, jnp.bfloat16)
     down_rows = feedforward_down_weight.T
     fed = jnp.maximum(
@@ -210,10 +210,8 @@
     places = [(turn + (span - step)) % span for step in range(span)]
     late_width = late[0].shape[1]
     late_up = jnp.zeros((late[0].shape[0] // rows, span, rows, late_width), jnp.bfloat16)
-    late_up = set_in(late_up, late[0], places[0])
-    late_up, places, own, hidden, mixer_gain, norm_gain, out_gain = lax.optimization_barrier(
+    places, own, hidden, mixer_gain, norm_gain, out_gain = lax.optimization_barrier(
         (
-            late_up,
             places,
             own,
             hidden,
@@ -238,7 +236,7 @@
     half = lax.optimization_barrier(half)
     half = half.reshape(part_rows, -1)
     normed_ff = jnp.concatenate((half, lax.ppermute(half, "c", CORES)), axis=0)
-    for piece, spot in zip(late[1:], places[1:]):
+    for piece, spot in zip(late, places):
         late_up = set_in(late_up, piece, spot)
     lifted = [
         jnp.square(

time: 183 us -> 187 us (1.022)
  blocking collectives: 94 us -> 85.2 us
  waiting for transfers between devices: 18 us -> 24.5 us
  starting transfers between devices: 33.6 us -> 38.1 us
    all_to_all x3 -> x2, blocking collectives: 32.6 us -> 22.2 us  [spread(): return lax.all_to_all(copies, axis, split_axis=0, concat_axis=0, tiled=True)]
    ppermute x3, waiting for transfers between devices: 4.83 us -> 8.64 us  [sent_round(): pieces.append(lax.ppermute(array, axis, ring))]
    all_to_all x1 -> x2, starting transfers between devices: 3.7 us -> 7.17 us  [spread(): return lax.all_to_all(copies, axis, split_axis=0, concat_axis=0, tiled=True)]
    all_to_all x1 -> x2, waiting for transfers between devices: 11.1 us -> 13.9 us  [spread(): return lax.all_to_all(copies, axis, split_axis=0, concat_axis=0, tiled=True)]
  transfers between devices with their start and end apart: 9 -> 10, of which waited for: 5 -> 6; matrix products, arithmetic and copies ran while one was open for 6% -> 7% of each run, Pallas kernels for 2% -> 1%
where the time goes in v4:
time: 187 us; the launch traced here: 186 us
  blocking collectives  85.2 us (46%)
  starting transfers between devices  38.1 us (20%)
  waiting for transfers between devices  24.5 us (13%)
  between operations  13.8 us (7%)
  matrix products  9.64 us (5%)
  other arithmetic  7.31 us (4%)
  local copies, waits for them, and re-layouts  4.94 us (3%)
  Pallas kernels  2.75 us (1%)
    all_gather x1, blocking collectives, per_device(): lax.all_gather(jnp.concatenate((recurrent_branch_weight, output_gate_weig...  38.9 us
    all_to_all x2, blocking collectives, summed_rows(): lax.all_to_all(quarters, 'x', split_axis=0, concat_axis=0, tiled=True)  24.1 us
    all_to_all x2, blocking collectives, spread(): return lax.all_to_all(copies, axis, split_axis=0, concat_axis=0, tiled=True)  22.2 us
    all_to_all x2, waiting for transfers between devices, spread(): return lax.all_to_all(copies, axis, split_axis=0, concat_axis=0, tiled=True)  13.9 us
    ppermute x2, starting transfers between devices, summed_rows(): sent = lax.ppermute(rows_of(others).astype(jnp.bfloat16), 'c', CORES)  13.5 us
    ppermute x3, starting transfers between devices, sent_round(): pieces.append(lax.ppermute(array, axis, ring))  8.71 us
    ppermute x3, waiting for transfers between devices, sent_round(): pieces.append(lax.ppermute(array, axis, ring))  8.64 us
    all_to_all x2, starting transfers between devices, spread(): return lax.all_to_all(copies, axis, split_axis=0, concat_axis=0, tiled=True)  7.17 us
  transfers between devices with their start and end apart: 10, of which 6 were waited for; matrix products, arithmetic and copies ran while one was open for 7% of the time, Pallas kernels for 1%

profile of v4, /device:TPU:1, one launch (start us, length us, event | category | flops | bytes accessed | tf_op | source)
XLA Modules:
  0.0 186.1 jit_solution(8792367461709052050)
XLA Ops:
  7.5 11.5 %all_to_all.30 = bf16[4,32,1792]{2,1,0:T(8,128)(2,1)} all-to-all(bf16[4,32,1792]{2,1,0:T(8,128)(2,1)S(1)} %broadcast_in_dim.63), channel_id=1, replica_groups=mesh['zh'=4,'zl'=4,'y'=4,'x'=4,'c'=2] {'y'}, dimensions={0} | all-to-all | bytes 917504 | tf_op jit(solution)/shard_map/all_to_all | solution.py:20
  19.1 38.9 %all_gather.6 = bf16[512,640]{1,0:T(8,128)(2,1)S(1)} all-gather(bf16[32,640]{1,0:T(8,128)(2,1)S(1)} %pad_maximum_fusion.5), channel_id=1, replica_groups=mesh['zh'=4,'zl'=4,'y'=4,'x'=4,'c'=2] {'zh','zl'}, dimensions={0}, use_global_device_ids=true | all-gather | bytes 696320 | tf_op jit(solution)/shard_map/all_gather | solution.py:169
  58.0 1.4 broadcast_in_dim.61
  59.4 3.7 %all-to-all-start = ((bf16[4,512,384]{2,1,0:T(8,128)(2,1)}), bf16[4,512,384]{2,1,0:T(8,128)(2,1)S(1)}, u32[]{:S(2)}, u32[]{:S(2)}) async-start(bf16[4,512,384]{2,1,0:T(8,128)(2,1)} %broadcast_in_dim.61), calls=%async_computation | async-start | bytes 3145728 | tf_op jit(solution)/shard_map/all_to_all | solution.py:20
  67.3 8.6 %all-to-all-done = bf16[4,512,384]{2,1,0:T(8,128)(2,1)S(1)} async-done(((bf16[4,512,384]{2,1,0:T(8,128)(2,1)}), bf16[4,512,384]{2,1,0:T(8,128)(2,1)S(1)}, u32[]{:S(2)}, u32[]{:S(2)}) %all-to-all-start) | async-done | bytes 1572896 | tf_op jit(solution)/shard_map/all_to_all | solution.py:20
  78.2 2.7 %shard_map.145 = bf16[256,128]{1,0:T(8,128)(2,1)} custom-call(bf16[256,256]{1,0:T(8,128)(2,1)} %convolution_convert_fusion.1.both, f32[4,128]{1,0:T(4,128)} %convert_element_type.86.taps, bf16[2,128,128]{2,1,0:T(8,128)(2,1)} %bitcast.43, bf16[2,128,128]{2,1,0:T(8,128)(2,1)} %bitcast.44, f32[2,128]{1,0:T(2,128)} %rate.1, f32[2,256,128]{2,1,0:T(8,128)} %extra.1), custom_call_target="tpu_custom_call" | custom-call | tf_op jit(solution)/shard_map/pallas_call | solution.py:193
  82.0 10.7 %collective-permute-start = (bf16[128,2048]{1,0:T(8,128)(2,1)S(1)}, bf16[128,2048]{1,0:T(8,128)(2,1)S(1)}, u32[]{:S(2)}, u32[]{:S(2)}) collective-permute-start(bf16[128,2048]{1,0:T(8,128)(2,1)S(1)} %convolution_convert_fusion), channel_id=1, source_target_pairs={{0,1},{1,0},{2,3},{3,2},{4,5},{5,4},{6,7},{7,6},{8,9},{9,8},{10,11... | collective-permute-start | bytes 1572872 | tf_op jit(solution)/shard_map/ppermute | solution.py:54
  94.4 12.5 %all_to_all.31 = bf16[4,32,2048]{2,1,0:T(8,128)(2,1)S(1)} all-to-all(bf16[4,32,2048]{2,1,0:T(8,128)(2,1)S(1)} %bitcast.32), channel_id=1, replica_groups=mesh['zh'=4,'zl'=4,'y'=4,'x'=4,'c'=2] {'x'}, dimensions={0} | all-to-all | bytes 1048576 | tf_op jit(solution)/shard_map/all_to_all | solution.py:59
  108.3 3.5 %all-to-all-start.2 = ((bf16[4,32,2048]{2,1,0:T(8,128)(2,1)}), bf16[4,32,2048]{2,1,0:T(8,128)(2,1)S(1)}, u32[]{:S(2)}, u32[]{:S(2)}) async-start(bf16[4,32,2048]{2,1,0:T(8,128)(2,1)} %broadcast_in_dim.62), calls=%async_computation.2 | async-start | bytes 1048576 | tf_op jit(solution)/shard_map/all_to_all | solution.py:20
  111.8 2.2 %collective-permute-start.2 = (bf16[512,256]{1,0:T(8,128)(2,1)S(1)}, bf16[512,256]{1,0:T(8,128)(2,1)S(1)}, u32[]{:S(2)}, u32[]{:S(2)}) collective-permute-start(bf16[512,256]{1,0:T(8,128)(2,1)S(1)} %slice.39), channel_id=1, source_target_pairs={{0,8},{8,16},{16,24},{24,0},{1,9},{9,17},{17,25},{25,1},{2,10},{10... | collective-permute-start | bytes 786440 | tf_op jit(solution)/shard_map/ppermute | solution.py:34
  114.0 5.3 %all-to-all-done.2 = bf16[4,32,2048]{2,1,0:T(8,128)(2,1)S(1)} async-done(((bf16[4,32,2048]{2,1,0:T(8,128)(2,1)}), bf16[4,32,2048]{2,1,0:T(8,128)(2,1)S(1)}, u32[]{:S(2)}, u32[]{:S(2)}) %all-to-all-start.2) | async-done | bytes 524320 | tf_op jit(solution)/shard_map/all_to_all | solution.py:20
  119.3 4.7 %collective-permute-start.1 = (bf16[128,2048]{1,0:T(8,128)(2,1)S(1)}, bf16[128,2048]{1,0:T(8,128)(2,1)S(1)}, u32[]{:S(2)}, u32[]{:S(2)}) collective-permute-start(bf16[128,2048]{1,0:T(8,128)(2,1)S(1)} %bitcast.37), channel_id=1, source_target_pairs={{0,1},{1,0},{2,3},{3,2},{4,5},{5,4},{6,7},{7,6},{8,9},{9,8},{10,11... | collective-permute-start | bytes 1572872 | tf_op jit(solution)/shard_map/ppermute | solution.py:238
  124.1 2.3 %collective-permute-start.3 = (bf16[512,256]{1,0:T(8,128)(2,1)S(1)}, bf16[512,256]{1,0:T(8,128)(2,1)S(1)}, u32[]{:S(2)}, u32[]{:S(2)}) collective-permute-start(bf16[512,256]{1,0:T(8,128)(2,1)S(1)} %slice.39), channel_id=1, source_target_pairs={{0,16},{8,24},{16,0},{24,8},{1,17},{9,25},{17,1},{25,9},{2,18},{10... | collective-permute-start | bytes 786440 | tf_op jit(solution)/shard_map/ppermute | solution.py:34
  126.4 4.2 %collective-permute-start.4 = (bf16[512,256]{1,0:T(8,128)(2,1)S(1)}, bf16[512,256]{1,0:T(8,128)(2,1)S(1)}, u32[]{:S(2)}, u32[]{:S(2)}) collective-permute-start(bf16[512,256]{1,0:T(8,128)(2,1)S(1)} %slice.39), channel_id=1, source_target_pairs={{0,24},{8,0},{16,8},{24,16},{1,25},{9,1},{17,9},{25,17},{2,26},{10... | collective-permute-start | bytes 786440 | tf_op jit(solution)/shard_map/ppermute | solution.py:34
  130.8 4.5 %collective-permute-done.3 = bf16[512,256]{1,0:T(8,128)(2,1)S(1)} collective-permute-done((bf16[512,256]{1,0:T(8,128)(2,1)S(1)}, bf16[512,256]{1,0:T(8,128)(2,1)S(1)}, u32[]{:S(2)}, u32[]{:S(2)}) %collective-permute-start.3) | collective-permute-done | bytes 262176 | tf_op jit(solution)/shard_map/ppermute | solution.py:34
  135.4 4.1 %collective-permute-done.4 = bf16[512,256]{1,0:T(8,128)(2,1)S(1)} collective-permute-done((bf16[512,256]{1,0:T(8,128)(2,1)S(1)}, bf16[512,256]{1,0:T(8,128)(2,1)S(1)}, u32[]{:S(2)}, u32[]{:S(2)}) %collective-permute-start.4) | collective-permute-done | bytes 262176 | tf_op jit(solution)/shard_map/ppermute | solution.py:34
  140.0 3.0 %fusion.18 = bf16[256,768]{1,0:T(8,128)(2,1)S(1)} fusion(bf16[2048,1792]{1,0:T(8,128)(2,1)} %all-gather.2.cloned.1.call-done, bf16[128,2048]{1,0:T(8,128)(2,1)S(1)} %collective-permute-done.1, bf16[128,2048]{1,0:T(8,128)(2,1)S(1)} %bitcast.39), kind=kOutput, calls=%fused_computation.15 | convolution fusion | flops 807993344 | bytes 4587520 | tf_op jit(solution)/shard_map/dot_general | solution.py:243
  144.0 1.5 fusion.6
  145.5 2.8 %collective-permute-start.5 = (bf16[128,2048]{1,0:T(8,128)(2,1)S(1)}, bf16[128,2048]{1,0:T(8,128)(2,1)S(1)}, u32[]{:S(2)}, u32[]{:S(2)}) collective-permute-start(bf16[128,2048]{1,0:T(8,128)(2,1)S(1)} %fusion.6), channel_id=1, source_target_pairs={{0,1},{1,0},{2,3},{3,2},{4,5},{5,4},{6,7},{7,6},{8,9},{9,8},{10,11... | collective-permute-start | bytes 1572872 | tf_op jit(solution)/shard_map/ppermute | solution.py:54
  148.3 1.5 fusion.2
  149.9 11.6 %all_to_all.32 = bf16[4,32,2048]{2,1,0:T(8,128)(2,1)S(1)} all-to-all(bf16[4,32,2048]{2,1,0:T(8,128)(2,1)S(1)} %bitcast.33), channel_id=1, replica_groups=mesh['zh'=4,'zl'=4,'y'=4,'x'=4,'c'=2] {'x'}, dimensions={0} | all-to-all | bytes 1048576 | tf_op jit(solution)/shard_map/all_to_all | solution.py:59
  161.9 10.7 %all_to_all.33 = bf16[4,32,2048]{2,1,0:T(8,128)(2,1)S(1)} all-to-all(bf16[4,32,2048]{2,1,0:T(8,128)(2,1)S(1)} %broadcast_in_dim.65), channel_id=1, replica_groups=mesh['zh'=4,'zl'=4,'y'=4,'x'=4,'c'=2] {'x'}, dimensions={0} | all-to-all | bytes 1048576 | tf_op jit(solution)/shard_map/all_to_all | solution.py:20
  172.6 4.0 %collective-permute-start.6 = (bf16[128,2048]{1,0:T(8,128)(2,1)S(1)}, bf16[128,2048]{1,0:T(8,128)(2,1)S(1)}, u32[]{:S(2)}, u32[]{:S(2)}) collective-permute-start(bf16[128,2048]{1,0:T(8,128)(2,1)S(1)} %bitcast.30), channel_id=1, source_target_pairs={{0,1},{1,0},{2,3},{3,2},{4,5},{5,4},{6,7},{7,6},{8,9},{9,8},{10,11... | collective-permute-start | bytes 1572872 | tf_op jit(solution)/shard_map/ppermute | solution.py:65
  176.7 1.4 collective-permute-done.6
  (71 shorter events, 15.1 us)
Async XLA Ops:
  6.5 12.5 %slice-start = ((bf16[32,1024]{1,0:T(8,128)(2,1)}), bf16[32,256]{1,0:T(8,128)(2,1)S(1)}, s32[]{:S(2)}) async-start(bf16[32,1024]{1,0:T(8,128)(2,1)} %param.27), calls=%async_computation.7 | async-start | bytes 32768 | tf_op jit(solution)/shard_map/slice | solution.py:175
  6.5 12.5 %copy-start.3 = (bf16[128,32]{0,1:T(8,128)(2,1)S(1)}, bf16[128,32]{0,1:T(8,128)(2,1)}, u32[]{:S(2)}) copy-start(bf16[128,32]{0,1:T(8,128)(2,1)} %param.24) | copy-start | bytes 24580
  6.5 12.5 %copy-start.5 = (bf16[32,128]{1,0:T(8,128)(2,1)S(1)}, bf16[32,128]{1,0:T(8,128)(2,1)}, u32[]{:S(2)}) copy-start(bf16[32,128]{1,0:T(8,128)(2,1)} %param.17) | copy-start | bytes 24580
  6.5 12.5 %copy-start.4 = (bf16[32,128]{1,0:T(8,128)(2,1)S(1)}, bf16[32,128]{1,0:T(8,128)(2,1)}, u32[]{:S(2)}) copy-start(bf16[32,128]{1,0:T(8,128)(2,1)} %param.18) | copy-start | bytes 24580
  6.5 133.4 %all-gather.2.cloned.1.call-start = ((), (), s32[]{:S(2)}) async-start(), calls=%async_computation.6 | async-start | bytes 7798784 | tf_op jit(solution)/shard_map/all_gather | solution.py:47
  59.4 3.8 %copy-start.6 = (bf16[2048]{0:T(1024)(128)(2,1)S(1)}, bf16[2048]{0:T(1024)(128)(2,1)}, u32[]{:S(2)}) copy-start(bf16[2048]{0:T(1024)(128)(2,1)} %param.16) | copy-start | bytes 12292
  59.4 3.8 %copy-start = (bf16[256,2048]{1,0:T(8,128)(2,1)S(1)}, bf16[256,2048]{1,0:T(8,128)(2,1)}, u32[]{:S(2)}) copy-start(bf16[256,2048]{1,0:T(8,128)(2,1)} %param.15) | copy-start | bytes 3145732
  59.4 16.5 %all-to-all-start = ((bf16[4,512,384]{2,1,0:T(8,128)(2,1)}), bf16[4,512,384]{2,1,0:T(8,128)(2,1)S(1)}, u32[]{:S(2)}, u32[]{:S(2)}) async-start(bf16[4,512,384]{2,1,0:T(8,128)(2,1)} %broadcast_in_dim.61), calls=%async_computation | async-start | bytes 3145728 | tf_op jit(solution)/shard_map/all_to_all | solution.py:20
  63.1 1.7 copy-start.8
  63.1 2.3 %copy-start.7 = (bf16[2048]{0:T(1024)(128)(2,1)S(1)}, bf16[2048]{0:T(1024)(128)(2,1)}, u32[]{:S(2)}) copy-start(bf16[2048]{0:T(1024)(128)(2,1)} %param.25) | copy-start | bytes 12292
  75.9 1.2 copy-start.1
  82.0 12.2 %collective-permute-start = (bf16[128,2048]{1,0:T(8,128)(2,1)S(1)}, bf16[128,2048]{1,0:T(8,128)(2,1)S(1)}, u32[]{:S(2)}, u32[]{:S(2)}) collective-permute-start(bf16[128,2048]{1,0:T(8,128)(2,1)S(1)} %convolution_convert_fusion), channel_id=1, source_target_pairs={{0,1},{1,0},{2,3},{3,2},{4,5},{5,4},{6,7},{7,6},{8,9},{9,8},{10,11... | collective-permute-start | bytes 1572872 | tf_op jit(solution)/shard_map/ppermute | solution.py:54
  93.8 13.5 %copy-start.2 = (f32[2048]{0:T(1024)S(1)}, f32[2048]{0:T(1024)}, u32[]{:S(2)}) copy-start(f32[2048]{0:T(1024)} %convert_element_type.88) | copy-start | bytes 24580
  108.3 11.0 %all-to-all-start.2 = ((bf16[4,32,2048]{2,1,0:T(8,128)(2,1)}), bf16[4,32,2048]{2,1,0:T(8,128)(2,1)S(1)}, u32[]{:S(2)}, u32[]{:S(2)}) async-start(bf16[4,32,2048]{2,1,0:T(8,128)(2,1)} %broadcast_in_dim.62), calls=%async_computation.2 | async-start | bytes 1048576 | tf_op jit(solution)/shard_map/all_to_all | solution.py:20
  111.8 19.0 %collective-permute-start.2 = (bf16[512,256]{1,0:T(8,128)(2,1)S(1)}, bf16[512,256]{1,0:T(8,128)(2,1)S(1)}, u32[]{:S(2)}, u32[]{:S(2)}) collective-permute-start(bf16[512,256]{1,0:T(8,128)(2,1)S(1)} %slice.39), channel_id=1, source_target_pairs={{0,8},{8,16},{16,24},{24,0},{1,9},{9,17},{17,25},{25,1},{2,10},{10... | collective-permute-start | bytes 786440 | tf_op jit(solution)/shard_map/ppermute | solution.py:34
  119.3 20.1 %collective-permute-start.1 = (bf16[128,2048]{1,0:T(8,128)(2,1)S(1)}, bf16[128,2048]{1,0:T(8,128)(2,1)S(1)}, u32[]{:S(2)}, u32[]{:S(2)}) collective-permute-start(bf16[128,2048]{1,0:T(8,128)(2,1)S(1)} %bitcast.37), channel_id=1, source_target_pairs={{0,1},{1,0},{2,3},{3,2},{4,5},{5,4},{6,7},{7,6},{8,9},{9,8},{10,11... | collective-permute-start | bytes 1572872 | tf_op jit(solution)/shard_map/ppermute | solution.py:238
  124.1 11.2 %collective-permute-start.3 = (bf16[512,256]{1,0:T(8,128)(2,1)S(1)}, bf16[512,256]{1,0:T(8,128)(2,1)S(1)}, u32[]{:S(2)}, u32[]{:S(2)}) collective-permute-start(bf16[512,256]{1,0:T(8,128)(2,1)S(1)} %slice.39), channel_id=1, source_target_pairs={{0,16},{8,24},{16,0},{24,8},{1,17},{9,25},{17,1},{25,9},{2,18},{10... | collective-permute-start | bytes 786440 | tf_op jit(solution)/shard_map/ppermute | solution.py:34
  126.4 13.1 %collective-permute-start.4 = (bf16[512,256]{1,0:T(8,128)(2,1)S(1)}, bf16[512,256]{1,0:T(8,128)(2,1)S(1)}, u32[]{:S(2)}, u32[]{:S(2)}) collective-permute-start(bf16[512,256]{1,0:T(8,128)(2,1)S(1)} %slice.39), channel_id=1, source_target_pairs={{0,24},{8,0},{16,8},{24,16},{1,25},{9,1},{17,9},{25,17},{2,26},{10... | collective-permute-start | bytes 786440 | tf_op jit(solution)/shard_map/ppermute | solution.py:34
  140.0 4.0 %copy-start.9 = (bf16[2048,1792]{1,0:T(8,128)(2,1)S(1)}, bf16[2048,1792]{1,0:T(8,128)(2,1)}, u32[]{:S(2)}) copy-start(bf16[2048,1792]{1,0:T(8,128)(2,1)} %all-gather.2.cloned.1.call-done) | copy-start | bytes 22020100
  145.5 4.3 %collective-permute-start.5 = (bf16[128,2048]{1,0:T(8,128)(2,1)S(1)}, bf16[128,2048]{1,0:T(8,128)(2,1)S(1)}, u32[]{:S(2)}, u32[]{:S(2)}) collective-permute-start(bf16[128,2048]{1,0:T(8,128)(2,1)S(1)} %fusion.6), channel_id=1, source_target_pairs={{0,1},{1,0},{2,3},{3,2},{4,5},{5,4},{6,7},{7,6},{8,9},{9,8},{10,11... | collective-permute-start | bytes 1572872 | tf_op jit(solution)/shard_map/ppermute | solution.py:54
  172.6 5.5 %collective-permute-start.6 = (bf16[128,2048]{1,0:T(8,128)(2,1)S(1)}, bf16[128,2048]{1,0:T(8,128)(2,1)S(1)}, u32[]{:S(2)}, u32[]{:S(2)}) collective-permute-start(bf16[128,2048]{1,0:T(8,128)(2,1)S(1)} %bitcast.30), channel_id=1, source_target_pairs={{0,1},{1,0},{2,3},{3,2},{4,5},{5,4},{6,7},{7,6},{8,9},{9,8},{10,11... | collective-permute-start | bytes 1572872 | tf_op jit(solution)/shard_map/ppermute | solution.py:65
Sparse Core Ops, SparseCore 0:
  19.1 103.5 all-gather.1

commit v5 on v4

--- a/solution.py
+++ b/solution.py
@@ -180,7 +180,11 @@
         axis=0,
         tiled=True,
     )
-    mixer = spread(column[:, : 3 * channels], "y")
+    span = lax.axis_size("y")
+    turn = lax.axis_index("y").astype(jnp.uint32)
+    places = [(turn + (span - step)) % span for step in range(span)]
+    mixer = spread(column[:, : 2 * channels], "y")
+    out_pieces = sent_round(column[:, 2 * channels : 3 * channels], "y")
     late, mixer = lax.optimization_barrier((column[:, 3 * channels :], mixer))
     late = sent_round(late, "y")
     mixer = in_order(mixer, rows)
@@ -188,7 +192,7 @@
         root_norm(tokens.astype(jnp.float32), recurrent_input_gain).astype(jnp.bfloat16)
     )
     both = jnp.dot(
-        normed, mixer[:, : 2 * channels], preferred_element_type=jnp.float32
+        normed, mixer, preferred_element_type=jnp.float32
     ).astype(jnp.bfloat16)
     hidden = pl.pallas_call(
         hidden_kernel, out_shape=jax.ShapeDtypeStruct((both.shape[0], channels), jnp.bfloat16)
@@ -200,14 +204,15 @@
         channel_decay_rate,
         position_log_decay,
     )
+    out_rows = jnp.zeros((out_pieces[0].shape[0] // rows, span, rows, channels), jnp.bfloat16)
+    for piece, spot in zip(out_pieces, places):
+        out_rows = set_in(out_rows, piece, spot)
+    out_rows = out_rows.reshape(-1, channels)
     across = (((1,), (1,)), ((), ()))
 
     share = tokens.shape[0] // lax.axis_size(TP)
     place = lax.axis_index("c") * lax.axis_size("x") + lax.axis_index("x")
     own = lax.dynamic_slice_in_dim(tokens, place * share, share, axis=0)
-    span = lax.axis_size("y")
-    turn = lax.axis_index("y").astype(jnp.uint32)
-    places = [(turn + (span - step)) % span for step in range(span)]
     late_width = late[0].shape[1]
     late_up = jnp.zeros((late[0].shape[0] // rows, span, rows, late_width), jnp.bfloat16)
     places, own, hidden, mixer_gain, norm_gain, out_gain = lax.optimization_barrier(
@@ -224,7 +229,7 @@
     core = lax.axis_index("c").astype(jnp.uint32)
     mixed = summed_rows(
         lambda these: lax.dot_general(
-            these, mixer[:, 2 * channels :], across, preferred_element_type=jnp.float32
+            these, out_rows, across, preferred_element_type=jnp.float32
         ),
         lax.dynamic_slice_in_dim(hidden, core * part_rows, part_rows, axis=0),
         lax.dynamic_slice_in_dim(hidden, (1 - core) * part_rows, part_rows, axis=0),

time: 187 us -> 195 us (1.043)
  starting transfers between devices: 38.1 us -> 46.9 us
  local copies, waits for them, and re-layouts: 4.94 us -> 8.65 us
  waiting for transfers between devices: 24.5 us -> 21.3 us
    ppermute x3 -> x6, starting transfers between devices: 8.71 us -> 17.4 us  [sent_round(): pieces.append(lax.ppermute(array, axis, ring))]
    dynamic_update_slice x4 -> x8, local copies, waits for them, and re-layouts: 0.08 us -> 3.8 us  [set_in(): return lax.dynamic_update_slice(out, block, (nought, place, nought, nought))]
    all_to_all x2, waiting for transfers between devices: 13.9 us -> 10.7 us  [spread(): return lax.all_to_all(copies, axis, split_axis=0, concat_axis=0, tiled=True)]
    ppermute x3 -> x6, waiting for transfers between devices: 8.64 us -> 8.65 us  [sent_round(): pieces.append(lax.ppermute(array, axis, ring))]
  transfers between devices with their start and end apart: 10 -> 13, of which waited for: 6 -> 6; matrix products, arithmetic and copies ran while one was open for 7% -> 8% of each run, Pallas kernels for 1% -> 1%
where the time goes in v5:
time: 195 us; the launch traced here: 194 us
  blocking collectives  84.9 us (44%)
  starting transfers between devices  46.9 us (24%)
  waiting for transfers between devices  21.3 us (11%)
  between operations  13.8 us (7%)
  matrix products  9.69 us (5%)
  local copies, waits for them, and re-layouts  8.65 us (4%)
  other arithmetic  5.69 us (3%)
  Pallas kernels  2.75 us (1%)
    all_gather x1, blocking collectives, per_device(): lax.all_gather(jnp.concatenate((recurrent_branch_weight, output_gate_weig...  38.7 us
    all_to_all x2, blocking collectives, summed_rows(): lax.all_to_all(quarters, 'x', split_axis=0, concat_axis=0, tiled=True)  24 us
    all_to_all x2, blocking collectives, spread(): return lax.all_to_all(copies, axis, split_axis=0, concat_axis=0, tiled=True)  22.2 us
    ppermute x6, starting transfers between devices, sent_round(): pieces.append(lax.ppermute(array, axis, ring))  17.4 us
    ppermute x2, starting transfers between devices, summed_rows(): sent = lax.ppermute(rows_of(others).astype(jnp.bfloat16), 'c', CORES)  13.6 us
    all_to_all x2, waiting for transfers between devices, spread(): return lax.all_to_all(copies, axis, split_axis=0, concat_axis=0, tiled=True)  10.7 us
    ppermute x6, waiting for transfers between devices, sent_round(): pieces.append(lax.ppermute(array, axis, ring))  8.65 us
    all_to_all x2, starting transfers between devices, spread(): return lax.all_to_all(copies, axis, split_axis=0, concat_axis=0, tiled=True)  7.14 us
  transfers between devices with their start and end apart: 13, of which 6 were waited for; matrix products, arithmetic and copies ran while one was open for 8% of the time, Pallas kernels for 1%

profile of v5, /device:TPU:1, one launch (start us, length us, event | category | flops | bytes accessed | tf_op | source)
XLA Modules:
  0.0 193.7 jit_solution(12461636331637390916)
XLA Ops:
  7.5 11.5 %all_to_all.30 = bf16[4,32,1792]{2,1,0:T(8,128)(2,1)} all-to-all(bf16[4,32,1792]{2,1,0:T(8,128)(2,1)S(1)} %broadcast_in_dim.67), channel_id=1, replica_groups=mesh['zh'=4,'zl'=4,'y'=4,'x'=4,'c'=2] {'y'}, dimensions={0} | all-to-all | bytes 917504 | tf_op jit(solution)/shard_map/all_to_all | solution.py:20
  20.5 38.7 %all_gather.6 = bf16[512,640]{1,0:T(8,128)(2,1)S(1)} all-gather(bf16[32,640]{1,0:T(8,128)(2,1)S(1)} %pad_maximum_fusion.5), channel_id=1, replica_groups=mesh['zh'=4,'zl'=4,'y'=4,'x'=4,'c'=2] {'zh','zl'}, dimensions={0}, use_global_device_ids=true | all-gather | bytes 696320 | tf_op jit(solution)/shard_map/all_gather | solution.py:169
  59.8 2.4 %collective-permute-start = (bf16[512,128]{1,0:T(8,128)(2,1)}, bf16[512,128]{1,0:T(8,128)(2,1)}, u32[]{:S(2)}, u32[]{:S(2)}) collective-permute-start(bf16[512,128]{1,0:T(8,128)(2,1)} %slice.36), channel_id=1, source_target_pairs={{0,8},{8,16},{16,24},{24,0},{1,9},{9,17},{17,25},{25,1},{2,10},{10... | collective-permute-start | bytes 393224 | tf_op jit(solution)/shard_map/ppermute | solution.py:34
  62.3 3.3 %collective-permute-start.1 = (bf16[512,128]{1,0:T(8,128)(2,1)}, bf16[512,128]{1,0:T(8,128)(2,1)}, u32[]{:S(2)}, u32[]{:S(2)}) collective-permute-start(bf16[512,128]{1,0:T(8,128)(2,1)} %slice.36), channel_id=1, source_target_pairs={{0,16},{8,24},{16,0},{24,8},{1,17},{9,25},{17,1},{25,9},{2,18},{10... | collective-permute-start | bytes 393224 | tf_op jit(solution)/shard_map/ppermute | solution.py:34
  65.6 2.9 %collective-permute-start.2 = (bf16[512,128]{1,0:T(8,128)(2,1)}, bf16[512,128]{1,0:T(8,128)(2,1)}, u32[]{:S(2)}, u32[]{:S(2)}) collective-permute-start(bf16[512,128]{1,0:T(8,128)(2,1)} %slice.36), channel_id=1, source_target_pairs={{0,24},{8,0},{16,8},{24,16},{1,25},{9,1},{17,9},{25,17},{2,26},{10... | collective-permute-start | bytes 393224 | tf_op jit(solution)/shard_map/ppermute | solution.py:34
  69.6 3.7 %all-to-all-start = ((bf16[4,512,256]{2,1,0:T(8,128)(2,1)}), bf16[4,512,256]{2,1,0:T(8,128)(2,1)S(1)}, u32[]{:S(2)}, u32[]{:S(2)}) async-start(bf16[4,512,256]{2,1,0:T(8,128)(2,1)} %broadcast_in_dim.64), calls=%async_computation | async-start | bytes 2097152 | tf_op jit(solution)/shard_map/all_to_all | solution.py:20
  79.1 5.4 %all-to-all-done = bf16[4,512,256]{2,1,0:T(8,128)(2,1)S(1)} async-done(((bf16[4,512,256]{2,1,0:T(8,128)(2,1)}), bf16[4,512,256]{2,1,0:T(8,128)(2,1)S(1)}, u32[]{:S(2)}, u32[]{:S(2)}) %all-to-all-start) | async-done | bytes 1048608 | tf_op jit(solution)/shard_map/all_to_all | solution.py:20
  85.6 2.7 %shard_map.145 = bf16[256,128]{1,0:T(8,128)(2,1)} custom-call(bf16[256,256]{1,0:T(8,128)(2,1)} %convolution_convert_fusion.1.both, f32[4,128]{1,0:T(4,128)} %convert_element_type.86.taps, bf16[2,128,128]{2,1,0:T(8,128)(2,1)} %bitcast.51, bf16[2,128,128]{2,1,0:T(8,128)(2,1)} %bitcast.52, f32[2,128]{1,0:T(2,128)} %rate.1, f32[2,256,128]{2,1,0:T(8,128)} %extra.1), custom_call_target="tpu_custom_call" | custom-call | tf_op jit(solution)/shard_map/pallas_call | solution.py:197
  89.4 10.9 %collective-permute-start.3 = (bf16[128,2048]{1,0:T(8,128)(2,1)S(1)}, bf16[128,2048]{1,0:T(8,128)(2,1)S(1)}, u32[]{:S(2)}, u32[]{:S(2)}) collective-permute-start(bf16[128,2048]{1,0:T(8,128)(2,1)S(1)} %convolution_convert_fusion), channel_id=1, source_target_pairs={{0,1},{1,0},{2,3},{3,2},{4,5},{5,4},{6,7},{7,6},{8,9},{9,8},{10,11... | collective-permute-start | bytes 1572872 | tf_op jit(solution)/shard_map/ppermute | solution.py:54
  101.9 12.4 %all_to_all.31 = bf16[4,32,2048]{2,1,0:T(8,128)(2,1)S(1)} all-to-all(bf16[4,32,2048]{2,1,0:T(8,128)(2,1)S(1)} %bitcast.40), channel_id=1, replica_groups=mesh['zh'=4,'zl'=4,'y'=4,'x'=4,'c'=2] {'x'}, dimensions={0} | all-to-all | bytes 1048576 | tf_op jit(solution)/shard_map/all_to_all | solution.py:59
  115.8 3.5 %all-to-all-start.2 = ((bf16[4,32,2048]{2,1,0:T(8,128)(2,1)}), bf16[4,32,2048]{2,1,0:T(8,128)(2,1)S(1)}, u32[]{:S(2)}, u32[]{:S(2)}) async-start(bf16[4,32,2048]{2,1,0:T(8,128)(2,1)} %broadcast_in_dim.66), calls=%async_computation.2 | async-start | bytes 1048576 | tf_op jit(solution)/shard_map/all_to_all | solution.py:20
  119.3 2.2 %collective-permute-start.5 = (bf16[512,256]{1,0:T(8,128)(2,1)S(1)}, bf16[512,256]{1,0:T(8,128)(2,1)S(1)}, u32[]{:S(2)}, u32[]{:S(2)}) collective-permute-start(bf16[512,256]{1,0:T(8,128)(2,1)S(1)} %get-tuple-element.21), channel_id=1, source_target_pairs={{0,8},{8,16},{16,24},{24,0},{1,9},{9,17},{17,25},{25,1},{2,10},{10... | collective-permute-start | bytes 786440 | tf_op jit(solution)/shard_map/ppermute | solution.py:34
  121.5 5.3 %all-to-all-done.2 = bf16[4,32,2048]{2,1,0:T(8,128)(2,1)S(1)} async-done(((bf16[4,32,2048]{2,1,0:T(8,128)(2,1)}), bf16[4,32,2048]{2,1,0:T(8,128)(2,1)S(1)}, u32[]{:S(2)}, u32[]{:S(2)}) %all-to-all-start.2) | async-done | bytes 524320 | tf_op jit(solution)/shard_map/all_to_all | solution.py:20
  126.8 4.8 %collective-permute-start.4 = (bf16[128,2048]{1,0:T(8,128)(2,1)S(1)}, bf16[128,2048]{1,0:T(8,128)(2,1)S(1)}, u32[]{:S(2)}, u32[]{:S(2)}) collective-permute-start(bf16[128,2048]{1,0:T(8,128)(2,1)S(1)} %bitcast.45), channel_id=1, source_target_pairs={{0,1},{1,0},{2,3},{3,2},{4,5},{5,4},{6,7},{7,6},{8,9},{9,8},{10,11... | collective-permute-start | bytes 1572872 | tf_op jit(solution)/shard_map/ppermute | solution.py:243
  131.6 2.2 %collective-permute-start.6 = (bf16[512,256]{1,0:T(8,128)(2,1)S(1)}, bf16[512,256]{1,0:T(8,128)(2,1)S(1)}, u32[]{:S(2)}, u32[]{:S(2)}) collective-permute-start(bf16[512,256]{1,0:T(8,128)(2,1)S(1)} %get-tuple-element.21), channel_id=1, source_target_pairs={{0,16},{8,24},{16,0},{24,8},{1,17},{9,25},{17,1},{25,9},{2,18},{10... | collective-permute-start | bytes 786440 | tf_op jit(solution)/shard_map/ppermute | solution.py:34
  133.8 4.3 %collective-permute-start.7 = (bf16[512,256]{1,0:T(8,128)(2,1)S(1)}, bf16[512,256]{1,0:T(8,128)(2,1)S(1)}, u32[]{:S(2)}, u32[]{:S(2)}) collective-permute-start(bf16[512,256]{1,0:T(8,128)(2,1)S(1)} %get-tuple-element.21), channel_id=1, source_target_pairs={{0,24},{8,0},{16,8},{24,16},{1,25},{9,1},{17,9},{25,17},{2,26},{10... | collective-permute-start | bytes 786440 | tf_op jit(solution)/shard_map/ppermute | solution.py:34
  138.3 4.5 %collective-permute-done.6 = bf16[512,256]{1,0:T(8,128)(2,1)S(1)} collective-permute-done((bf16[512,256]{1,0:T(8,128)(2,1)S(1)}, bf16[512,256]{1,0:T(8,128)(2,1)S(1)}, u32[]{:S(2)}, u32[]{:S(2)}) %collective-permute-start.6) | collective-permute-done | bytes 262176 | tf_op jit(solution)/shard_map/ppermute | solution.py:34
  142.9 4.1 %collective-permute-done.7 = bf16[512,256]{1,0:T(8,128)(2,1)S(1)} collective-permute-done((bf16[512,256]{1,0:T(8,128)(2,1)S(1)}, bf16[512,256]{1,0:T(8,128)(2,1)S(1)}, u32[]{:S(2)}, u32[]{:S(2)}) %collective-permute-start.7) | collective-permute-done | bytes 262176 | tf_op jit(solution)/shard_map/ppermute | solution.py:34
  147.5 3.0 %fusion.18 = bf16[256,768]{1,0:T(8,128)(2,1)S(1)} fusion(bf16[2048,1792]{1,0:T(8,128)(2,1)} %all-gather.2.cloned.1.call-done, bf16[128,2048]{1,0:T(8,128)(2,1)S(1)} %collective-permute-done.4, bf16[128,2048]{1,0:T(8,128)(2,1)S(1)} %bitcast.47), kind=kOutput, calls=%fused_computation.15 | convolution fusion | flops 807993344 | bytes 4587520 | tf_op jit(solution)/shard_map/dot_general | solution.py:248
  151.6 1.5 fusion.6
  153.1 2.8 %collective-permute-start.8 = (bf16[128,2048]{1,0:T(8,128)(2,1)S(1)}, bf16[128,2048]{1,0:T(8,128)(2,1)S(1)}, u32[]{:S(2)}, u32[]{:S(2)}) collective-permute-start(bf16[128,2048]{1,0:T(8,128)(2,1)S(1)} %fusion.6), channel_id=1, source_target_pairs={{0,1},{1,0},{2,3},{3,2},{4,5},{5,4},{6,7},{7,6},{8,9},{9,8},{10,11... | collective-permute-start | bytes 1572872 | tf_op jit(solution)/shard_map/ppermute | solution.py:54
  157.5 11.6 %all_to_all.32 = bf16[4,32,2048]{2,1,0:T(8,128)(2,1)S(1)} all-to-all(bf16[4,32,2048]{2,1,0:T(8,128)(2,1)S(1)} %bitcast.41), channel_id=1, replica_groups=mesh['zh'=4,'zl'=4,'y'=4,'x'=4,'c'=2] {'x'}, dimensions={0} | all-to-all | bytes 1048576 | tf_op jit(solution)/shard_map/all_to_all | solution.py:59
  169.5 10.7 %all_to_all.33 = bf16[4,32,2048]{2,1,0:T(8,128)(2,1)S(1)} all-to-all(bf16[4,32,2048]{2,1,0:T(8,128)(2,1)S(1)} %broadcast_in_dim.69), channel_id=1, replica_groups=mesh['zh'=4,'zl'=4,'y'=4,'x'=4,'c'=2] {'x'}, dimensions={0} | all-to-all | bytes 1048576 | tf_op jit(solution)/shard_map/all_to_all | solution.py:20
  180.2 4.0 %collective-permute-start.9 = (bf16[128,2048]{1,0:T(8,128)(2,1)S(1)}, bf16[128,2048]{1,0:T(8,128)(2,1)S(1)}, u32[]{:S(2)}, u32[]{:S(2)}) collective-permute-start(bf16[128,2048]{1,0:T(8,128)(2,1)S(1)} %bitcast.38), channel_id=1, source_target_pairs={{0,1},{1,0},{2,3},{3,2},{4,5},{5,4},{6,7},{7,6},{8,9},{9,8},{10,11... | collective-permute-start | bytes 1572872 | tf_op jit(solution)/shard_map/ppermute | solution.py:65
  (77 shorter events, 21.5 us)
Async XLA Ops:
  6.5 141.0 %all-gather.2.cloned.1.call-start = ((), (), s32[]{:S(2)}) async-start(), calls=%async_computation.6 | async-start | bytes 7798784 | tf_op jit(solution)/shard_map/all_gather | solution.py:47
  18.9 54.3 %copy-start.2 = (bf16[2048]{0:T(1024)(128)(2,1)S(1)}, bf16[2048]{0:T(1024)(128)(2,1)}, u32[]{:S(2)}) copy-start(bf16[2048]{0:T(1024)(128)(2,1)} %param.16) | copy-start | bytes 12292
  18.9 54.4 %copy-start = (bf16[256,2048]{1,0:T(8,128)(2,1)S(1)}, bf16[256,2048]{1,0:T(8,128)(2,1)}, u32[]{:S(2)}) copy-start(bf16[256,2048]{1,0:T(8,128)(2,1)} %param.15) | copy-start | bytes 3145732
  59.8 16.4 %collective-permute-start = (bf16[512,128]{1,0:T(8,128)(2,1)}, bf16[512,128]{1,0:T(8,128)(2,1)}, u32[]{:S(2)}, u32[]{:S(2)}) collective-permute-start(bf16[512,128]{1,0:T(8,128)(2,1)} %slice.36), channel_id=1, source_target_pairs={{0,8},{8,16},{16,24},{24,0},{1,9},{9,17},{17,25},{25,1},{2,10},{10... | collective-permute-start | bytes 393224 | tf_op jit(solution)/shard_map/ppermute | solution.py:34
  62.3 14.9 %collective-permute-start.1 = (bf16[512,128]{1,0:T(8,128)(2,1)}, bf16[512,128]{1,0:T(8,128)(2,1)}, u32[]{:S(2)}, u32[]{:S(2)}) collective-permute-start(bf16[512,128]{1,0:T(8,128)(2,1)} %slice.36), channel_id=1, source_target_pairs={{0,16},{8,24},{16,0},{24,8},{1,17},{9,25},{17,1},{25,9},{2,18},{10... | collective-permute-start | bytes 393224 | tf_op jit(solution)/shard_map/ppermute | solution.py:34
  65.6 12.5 %collective-permute-start.2 = (bf16[512,128]{1,0:T(8,128)(2,1)}, bf16[512,128]{1,0:T(8,128)(2,1)}, u32[]{:S(2)}, u32[]{:S(2)}) collective-permute-start(bf16[512,128]{1,0:T(8,128)(2,1)} %slice.36), channel_id=1, source_target_pairs={{0,24},{8,0},{16,8},{24,16},{1,25},{9,1},{17,9},{25,17},{2,26},{10... | collective-permute-start | bytes 393224 | tf_op jit(solution)/shard_map/ppermute | solution.py:34
  69.6 5.4 %copy-start.6 = (bf16[4,128]{1,0:T(4,128)(2,1)S(1)}, bf16[4,128]{1,0:T(4,128)(2,1)}, u32[]{:S(2)}) copy-start(bf16[4,128]{1,0:T(4,128)(2,1)} %param.19) | copy-start | bytes 3076
  69.6 6.0 %copy-start.3 = (bf16[2048]{0:T(1024)(128)(2,1)S(1)}, bf16[2048]{0:T(1024)(128)(2,1)}, u32[]{:S(2)}) copy-start(bf16[2048]{0:T(1024)(128)(2,1)} %param.25) | copy-start | bytes 12292
  69.6 6.0 %copy-start.4 = (bf16[2048]{0:T(1024)(128)(2,1)S(1)}, bf16[2048]{0:T(1024)(128)(2,1)}, u32[]{:S(2)}) copy-start(bf16[2048]{0:T(1024)(128)(2,1)} %param.26) | copy-start | bytes 12292
  69.6 6.6 %copy-start.5 = (bf16[2048]{0:T(1024)(128)(2,1)S(1)}, bf16[2048]{0:T(1024)(128)(2,1)}, u32[]{:S(2)}) copy-start(bf16[2048]{0:T(1024)(128)(2,1)} %param.29) | copy-start | bytes 12292
  69.6 14.8 %all-to-all-start = ((bf16[4,512,256]{2,1,0:T(8,128)(2,1)}), bf16[4,512,256]{2,1,0:T(8,128)(2,1)S(1)}, u32[]{:S(2)}, u32[]{:S(2)}) async-start(bf16[4,512,256]{2,1,0:T(8,128)(2,1)} %broadcast_in_dim.64), calls=%async_computation | async-start | bytes 2097152 | tf_op jit(solution)/shard_map/all_to_all | solution.py:20
  89.4 12.4 %collective-permute-start.3 = (bf16[128,2048]{1,0:T(8,128)(2,1)S(1)}, bf16[128,2048]{1,0:T(8,128)(2,1)S(1)}, u32[]{:S(2)}, u32[]{:S(2)}) collective-permute-start(bf16[128,2048]{1,0:T(8,128)(2,1)S(1)} %convolution_convert_fusion), channel_id=1, source_target_pairs={{0,1},{1,0},{2,3},{3,2},{4,5},{5,4},{6,7},{7,6},{8,9},{9,8},{10,11... | collective-permute-start | bytes 1572872 | tf_op jit(solution)/shard_map/ppermute | solution.py:54
  100.3 14.6 %copy-start.1 = (f32[2048]{0:T(1024)S(1)}, f32[2048]{0:T(1024)}, u32[]{:S(2)}) copy-start(f32[2048]{0:T(1024)} %convert_element_type.88) | copy-start | bytes 24580
  115.8 11.0 %all-to-all-start.2 = ((bf16[4,32,2048]{2,1,0:T(8,128)(2,1)}), bf16[4,32,2048]{2,1,0:T(8,128)(2,1)S(1)}, u32[]{:S(2)}, u32[]{:S(2)}) async-start(bf16[4,32,2048]{2,1,0:T(8,128)(2,1)} %broadcast_in_dim.66), calls=%async_computation.2 | async-start | bytes 1048576 | tf_op jit(solution)/shard_map/all_to_all | solution.py:20
  119.3 19.0 %collective-permute-start.5 = (bf16[512,256]{1,0:T(8,128)(2,1)S(1)}, bf16[512,256]{1,0:T(8,128)(2,1)S(1)}, u32[]{:S(2)}, u32[]{:S(2)}) collective-permute-start(bf16[512,256]{1,0:T(8,128)(2,1)S(1)} %get-tuple-element.21), channel_id=1, source_target_pairs={{0,8},{8,16},{16,24},{24,0},{1,9},{9,17},{17,25},{25,1},{2,10},{10... | collective-permute-start | bytes 786440 | tf_op jit(solution)/shard_map/ppermute | solution.py:34
  126.8 20.2 %collective-permute-start.4 = (bf16[128,2048]{1,0:T(8,128)(2,1)S(1)}, bf16[128,2048]{1,0:T(8,128)(2,1)S(1)}, u32[]{:S(2)}, u32[]{:S(2)}) collective-permute-start(bf16[128,2048]{1,0:T(8,128)(2,1)S(1)} %bitcast.45), channel_id=1, source_target_pairs={{0,1},{1,0},{2,3},{3,2},{4,5},{5,4},{6,7},{7,6},{8,9},{9,8},{10,11... | collective-permute-start | bytes 1572872 | tf_op jit(solution)/shard_map/ppermute | solution.py:243
  131.6 11.2 %collective-permute-start.6 = (bf16[512,256]{1,0:T(8,128)(2,1)S(1)}, bf16[512,256]{1,0:T(8,128)(2,1)S(1)}, u32[]{:S(2)}, u32[]{:S(2)}) collective-permute-start(bf16[512,256]{1,0:T(8,128)(2,1)S(1)} %get-tuple-element.21), channel_id=1, source_target_pairs={{0,16},{8,24},{16,0},{24,8},{1,17},{9,25},{17,1},{25,9},{2,18},{10... | collective-permute-start | bytes 786440 | tf_op jit(solution)/shard_map/ppermute | solution.py:34
  133.8 13.2 %collective-permute-start.7 = (bf16[512,256]{1,0:T(8,128)(2,1)S(1)}, bf16[512,256]{1,0:T(8,128)(2,1)S(1)}, u32[]{:S(2)}, u32[]{:S(2)}) collective-permute-start(bf16[512,256]{1,0:T(8,128)(2,1)S(1)} %get-tuple-element.21), channel_id=1, source_target_pairs={{0,24},{8,0},{16,8},{24,16},{1,25},{9,1},{17,9},{25,17},{2,26},{10... | collective-permute-start | bytes 786440 | tf_op jit(solution)/shard_map/ppermute | solution.py:34
  147.5 4.0 %copy-start.7 = (bf16[2048,1792]{1,0:T(8,128)(2,1)S(1)}, bf16[2048,1792]{1,0:T(8,128)(2,1)}, u32[]{:S(2)}) copy-start(bf16[2048,1792]{1,0:T(8,128)(2,1)} %all-gather.2.cloned.1.call-done) | copy-start | bytes 22020100
  153.1 4.3 %collective-permute-start.8 = (bf16[128,2048]{1,0:T(8,128)(2,1)S(1)}, bf16[128,2048]{1,0:T(8,128)(2,1)S(1)}, u32[]{:S(2)}, u32[]{:S(2)}) collective-permute-start(bf16[128,2048]{1,0:T(8,128)(2,1)S(1)} %fusion.6), channel_id=1, source_target_pairs={{0,1},{1,0},{2,3},{3,2},{4,5},{5,4},{6,7},{7,6},{8,9},{9,8},{10,11... | collective-permute-start | bytes 1572872 | tf_op jit(solution)/shard_map/ppermute | solution.py:54
  180.2 5.5 %collective-permute-start.9 = (bf16[128,2048]{1,0:T(8,128)(2,1)S(1)}, bf16[128,2048]{1,0:T(8,128)(2,1)S(1)}, u32[]{:S(2)}, u32[]{:S(2)}) collective-permute-start(bf16[128,2048]{1,0:T(8,128)(2,1)S(1)} %bitcast.38), channel_id=1, source_target_pairs={{0,1},{1,0},{2,3},{3,2},{4,5},{5,4},{6,7},{7,6},{8,9},{9,8},{10,11... | collective-permute-start | bytes 1572872 | tf_op jit(solution)/shard_map/ppermute | solution.py:65
Sparse Core Ops, SparseCore 0:
  19.1 103.5 all-gather.1

commit v6 on v4

--- a/solution.py
+++ b/solution.py
@@ -63,8 +63,11 @@
 def all_rows(part):
     half = spread(part, "x").reshape(-1, part.shape[-1])
     other = lax.ppermute(half, "c", CORES)
-    mine = lax.broadcasted_iota(jnp.int32, (2, 1, 1), 0) == lax.axis_index("c")
-    return jnp.where(mine, half[None], other[None]).reshape(-1, part.shape[-1])
+    core = lax.axis_index("c")
+    mine = lax.broadcasted_iota(jnp.int32, (2, 1, 1), 0) == core
+    out = jnp.where(mine, half[None], jnp.zeros_like(half)[None]).reshape(-1, part.shape[-1])
+    place = (1 - core).astype(jnp.uint32) * half.shape[0]
+    return lax.dynamic_update_slice_in_dim(lax.optimization_barrier(out), other, place, axis=0)
 
 
 def root_norm(values, gain):

time: 187 us -> 187 us (level)
  no operation moved by 1% of the time
where the time goes in v6:
time: 187 us; the launch traced here: 186 us
  blocking collectives  85.2 us (46%)
  starting transfers between devices  38.1 us (20%)
  waiting for transfers between devices  23.3 us (12%)
  between operations  13.8 us (7%)
  matrix products  9.64 us (5%)
  other arithmetic  7.29 us (4%)
  local copies, waits for them, and re-layouts  5.76 us (3%)
  Pallas kernels  2.75 us (1%)
    all_gather x1, blocking collectives, per_device(): lax.all_gather(jnp.concatenate((recurrent_branch_weight, output_gate_weig...  38.9 us
    all_to_all x2, blocking collectives, summed_rows(): lax.all_to_all(quarters, 'x', split_axis=0, concat_axis=0, tiled=True)  24.1 us
    all_to_all x2, blocking collectives, spread(): return lax.all_to_all(copies, axis, split_axis=0, concat_axis=0, tiled=True)  22.2 us
    all_to_all x2, waiting for transfers between devices, spread(): return lax.all_to_all(copies, axis, split_axis=0, concat_axis=0, tiled=True)  13.9 us
    ppermute x2, starting transfers between devices, summed_rows(): sent = lax.ppermute(rows_of(others).astype(jnp.bfloat16), 'c', CORES)  13.5 us
    ppermute x3, starting transfers between devices, sent_round(): pieces.append(lax.ppermute(array, axis, ring))  8.71 us
    ppermute x3, waiting for transfers between devices, sent_round(): pieces.append(lax.ppermute(array, axis, ring))  8.64 us
    all_to_all x2, starting transfers between devices, spread(): return lax.all_to_all(copies, axis, split_axis=0, concat_axis=0, tiled=True)  7.17 us
  transfers between devices with their start and end apart: 10, of which 6 were waited for; matrix products, arithmetic and copies ran while one was open for 7% of the time, Pallas kernels for 1%

profile of v6, /device:TPU:1, one launch (start us, length us, event | category | flops | bytes accessed | tf_op | source)
XLA Modules:
  0.0 185.8 jit_solution(15369039737779464077)
XLA Ops:
  7.5 11.5 %all_to_all.30 = bf16[4,32,1792]{2,1,0:T(8,128)(2,1)} all-to-all(bf16[4,32,1792]{2,1,0:T(8,128)(2,1)S(1)} %broadcast_in_dim.60), channel_id=1, replica_groups=mesh['zh'=4,'zl'=4,'y'=4,'x'=4,'c'=2] {'y'}, dimensions={0} | all-to-all | bytes 917504 | tf_op jit(solution)/shard_map/all_to_all | solution.py:20
  19.1 38.9 %all_gather.6 = bf16[512,640]{1,0:T(8,128)(2,1)S(1)} all-gather(bf16[32,640]{1,0:T(8,128)(2,1)S(1)} %pad_maximum_fusion.5), channel_id=1, replica_groups=mesh['zh'=4,'zl'=4,'y'=4,'x'=4,'c'=2] {'zh','zl'}, dimensions={0}, use_global_device_ids=true | all-gather | bytes 696320 | tf_op jit(solution)/shard_map/all_gather | solution.py:172
  58.0 1.4 broadcast_in_dim.58
  59.4 3.7 %all-to-all-start = ((bf16[4,512,384]{2,1,0:T(8,128)(2,1)}), bf16[4,512,384]{2,1,0:T(8,128)(2,1)S(1)}, u32[]{:S(2)}, u32[]{:S(2)}) async-start(bf16[4,512,384]{2,1,0:T(8,128)(2,1)} %broadcast_in_dim.58), calls=%async_computation | async-start | bytes 3145728 | tf_op jit(solution)/shard_map/all_to_all | solution.py:20
  63.5 1.3 fusion.11
  67.3 8.6 %all-to-all-done = bf16[4,512,384]{2,1,0:T(8,128)(2,1)S(1)} async-done(((bf16[4,512,384]{2,1,0:T(8,128)(2,1)}), bf16[4,512,384]{2,1,0:T(8,128)(2,1)S(1)}, u32[]{:S(2)}, u32[]{:S(2)}) %all-to-all-start) | async-done | bytes 1572896 | tf_op jit(solution)/shard_map/all_to_all | solution.py:20
  78.2 2.7 %shard_map.145 = bf16[256,128]{1,0:T(8,128)(2,1)} custom-call(bf16[256,256]{1,0:T(8,128)(2,1)} %convolution_convert_fusion.1.both, f32[4,128]{1,0:T(4,128)} %convert_element_type.89.taps, bf16[2,128,128]{2,1,0:T(8,128)(2,1)} %bitcast.41, bf16[2,128,128]{2,1,0:T(8,128)(2,1)} %bitcast.42, f32[2,128]{1,0:T(2,128)} %rate.1, f32[2,256,128]{2,1,0:T(8,128)} %extra.1), custom_call_target="tpu_custom_call" | custom-call | tf_op jit(solution)/shard_map/pallas_call | solution.py:196
  82.0 10.7 %collective-permute-start = (bf16[128,2048]{1,0:T(8,128)(2,1)S(1)}, bf16[128,2048]{1,0:T(8,128)(2,1)S(1)}, u32[]{:S(2)}, u32[]{:S(2)}) collective-permute-start(bf16[128,2048]{1,0:T(8,128)(2,1)S(1)} %convolution_convert_fusion), channel_id=1, source_target_pairs={{0,1},{1,0},{2,3},{3,2},{4,5},{5,4},{6,7},{7,6},{8,9},{9,8},{10,11... | collective-permute-start | bytes 1572872 | tf_op jit(solution)/shard_map/ppermute | solution.py:54
  94.4 12.5 %all_to_all.31 = bf16[4,32,2048]{2,1,0:T(8,128)(2,1)S(1)} all-to-all(bf16[4,32,2048]{2,1,0:T(8,128)(2,1)S(1)} %bitcast.30), channel_id=1, replica_groups=mesh['zh'=4,'zl'=4,'y'=4,'x'=4,'c'=2] {'x'}, dimensions={0} | all-to-all | bytes 1048576 | tf_op jit(solution)/shard_map/all_to_all | solution.py:59
  108.3 3.5 %all-to-all-start.2 = ((bf16[4,32,2048]{2,1,0:T(8,128)(2,1)}), bf16[4,32,2048]{2,1,0:T(8,128)(2,1)S(1)}, u32[]{:S(2)}, u32[]{:S(2)}) async-start(bf16[4,32,2048]{2,1,0:T(8,128)(2,1)} %broadcast_in_dim.59), calls=%async_computation.2 | async-start | bytes 1048576 | tf_op jit(solution)/shard_map/all_to_all | solution.py:20
  111.8 2.2 %collective-permute-start.2 = (bf16[512,256]{1,0:T(8,128)(2,1)S(1)}, bf16[512,256]{1,0:T(8,128)(2,1)S(1)}, u32[]{:S(2)}, u32[]{:S(2)}) collective-permute-start(bf16[512,256]{1,0:T(8,128)(2,1)S(1)} %slice.39), channel_id=1, source_target_pairs={{0,8},{8,16},{16,24},{24,0},{1,9},{9,17},{17,25},{25,1},{2,10},{10... | collective-permute-start | bytes 786440 | tf_op jit(solution)/shard_map/ppermute | solution.py:34
  114.0 5.3 %all-to-all-done.2 = bf16[4,32,2048]{2,1,0:T(8,128)(2,1)S(1)} async-done(((bf16[4,32,2048]{2,1,0:T(8,128)(2,1)}), bf16[4,32,2048]{2,1,0:T(8,128)(2,1)S(1)}, u32[]{:S(2)}, u32[]{:S(2)}) %all-to-all-start.2) | async-done | bytes 524320 | tf_op jit(solution)/shard_map/all_to_all | solution.py:20
  119.3 4.7 %collective-permute-start.1 = (bf16[128,2048]{1,0:T(8,128)(2,1)S(1)}, bf16[128,2048]{1,0:T(8,128)(2,1)S(1)}, u32[]{:S(2)}, u32[]{:S(2)}) collective-permute-start(bf16[128,2048]{1,0:T(8,128)(2,1)S(1)} %bitcast.35), channel_id=1, source_target_pairs={{0,1},{1,0},{2,3},{3,2},{4,5},{5,4},{6,7},{7,6},{8,9},{9,8},{10,11... | collective-permute-start | bytes 1572872 | tf_op jit(solution)/shard_map/ppermute | solution.py:241
  124.1 2.3 %collective-permute-start.3 = (bf16[512,256]{1,0:T(8,128)(2,1)S(1)}, bf16[512,256]{1,0:T(8,128)(2,1)S(1)}, u32[]{:S(2)}, u32[]{:S(2)}) collective-permute-start(bf16[512,256]{1,0:T(8,128)(2,1)S(1)} %slice.39), channel_id=1, source_target_pairs={{0,16},{8,24},{16,0},{24,8},{1,17},{9,25},{17,1},{25,9},{2,18},{10... | collective-permute-start | bytes 786440 | tf_op jit(solution)/shard_map/ppermute | solution.py:34
  126.4 4.2 %collective-permute-start.4 = (bf16[512,256]{1,0:T(8,128)(2,1)S(1)}, bf16[512,256]{1,0:T(8,128)(2,1)S(1)}, u32[]{:S(2)}, u32[]{:S(2)}) collective-permute-start(bf16[512,256]{1,0:T(8,128)(2,1)S(1)} %slice.39), channel_id=1, source_target_pairs={{0,24},{8,0},{16,8},{24,16},{1,25},{9,1},{17,9},{25,17},{2,26},{10... | collective-permute-start | bytes 786440 | tf_op jit(solution)/shard_map/ppermute | solution.py:34
  130.8 4.5 %collective-permute-done.3 = bf16[512,256]{1,0:T(8,128)(2,1)S(1)} collective-permute-done((bf16[512,256]{1,0:T(8,128)(2,1)S(1)}, bf16[512,256]{1,0:T(8,128)(2,1)S(1)}, u32[]{:S(2)}, u32[]{:S(2)}) %collective-permute-start.3) | collective-permute-done | bytes 262176 | tf_op jit(solution)/shard_map/ppermute | solution.py:34
  135.4 4.1 %collective-permute-done.4 = bf16[512,256]{1,0:T(8,128)(2,1)S(1)} collective-permute-done((bf16[512,256]{1,0:T(8,128)(2,1)S(1)}, bf16[512,256]{1,0:T(8,128)(2,1)S(1)}, u32[]{:S(2)}, u32[]{:S(2)}) %collective-permute-start.4) | collective-permute-done | bytes 262176 | tf_op jit(solution)/shard_map/ppermute | solution.py:34
  140.0 3.0 %fusion.18 = bf16[256,768]{1,0:T(8,128)(2,1)S(1)} fusion(bf16[2048,1792]{1,0:T(8,128)(2,1)} %all-gather.2.cloned.1.call-done, bf16[128,2048]{1,0:T(8,128)(2,1)S(1)} %collective-permute-done.1, bf16[128,2048]{1,0:T(8,128)(2,1)S(1)} %bitcast.37), kind=kOutput, calls=%fused_computation.15 | convolution fusion | flops 807993344 | bytes 4587520 | tf_op jit(solution)/shard_map/dot_general | solution.py:246
  144.0 1.5 fusion.6
  145.5 2.8 %collective-permute-start.5 = (bf16[128,2048]{1,0:T(8,128)(2,1)S(1)}, bf16[128,2048]{1,0:T(8,128)(2,1)S(1)}, u32[]{:S(2)}, u32[]{:S(2)}) collective-permute-start(bf16[128,2048]{1,0:T(8,128)(2,1)S(1)} %fusion.6), channel_id=1, source_target_pairs={{0,1},{1,0},{2,3},{3,2},{4,5},{5,4},{6,7},{7,6},{8,9},{9,8},{10,11... | collective-permute-start | bytes 1572872 | tf_op jit(solution)/shard_map/ppermute | solution.py:54
  148.3 1.5 fusion.2
  149.9 11.6 %all_to_all.32 = bf16[4,32,2048]{2,1,0:T(8,128)(2,1)S(1)} all-to-all(bf16[4,32,2048]{2,1,0:T(8,128)(2,1)S(1)} %bitcast.31), channel_id=1, replica_groups=mesh['zh'=4,'zl'=4,'y'=4,'x'=4,'c'=2] {'x'}, dimensions={0} | all-to-all | bytes 1048576 | tf_op jit(solution)/shard_map/all_to_all | solution.py:59
  161.9 10.7 %all_to_all.33 = bf16[4,32,2048]{2,1,0:T(8,128)(2,1)S(1)} all-to-all(bf16[4,32,2048]{2,1,0:T(8,128)(2,1)S(1)} %broadcast_in_dim.62), channel_id=1, replica_groups=mesh['zh'=4,'zl'=4,'y'=4,'x'=4,'c'=2] {'x'}, dimensions={0} | all-to-all | bytes 1048576 | tf_op jit(solution)/shard_map/all_to_all | solution.py:20
  172.6 4.0 %collective-permute-start.6 = (bf16[128,2048]{1,0:T(8,128)(2,1)S(1)}, bf16[128,2048]{1,0:T(8,128)(2,1)S(1)}, u32[]{:S(2)}, u32[]{:S(2)}) collective-permute-start(bf16[128,2048]{1,0:T(8,128)(2,1)S(1)} %bitcast.28), channel_id=1, source_target_pairs={{0,1},{1,0},{2,3},{3,2},{4,5},{5,4},{6,7},{7,6},{8,9},{9,8},{10,11... | collective-permute-start | bytes 1572872 | tf_op jit(solution)/shard_map/ppermute | solution.py:65
  (72 shorter events, 14.9 us)
Async XLA Ops:
  6.5 12.5 %slice-start = ((bf16[32,1024]{1,0:T(8,128)(2,1)}), bf16[32,256]{1,0:T(8,128)(2,1)S(1)}, s32[]{:S(2)}) async-start(bf16[32,1024]{1,0:T(8,128)(2,1)} %param.27), calls=%async_computation.7 | async-start | bytes 32768 | tf_op jit(solution)/shard_map/slice | solution.py:178
  6.5 12.5 %copy-start.3 = (bf16[128,32]{0,1:T(8,128)(2,1)S(1)}, bf16[128,32]{0,1:T(8,128)(2,1)}, u32[]{:S(2)}) copy-start(bf16[128,32]{0,1:T(8,128)(2,1)} %param.24) | copy-start | bytes 24580
  6.5 12.5 %copy-start.5 = (bf16[32,128]{1,0:T(8,128)(2,1)S(1)}, bf16[32,128]{1,0:T(8,128)(2,1)}, u32[]{:S(2)}) copy-start(bf16[32,128]{1,0:T(8,128)(2,1)} %param.17) | copy-start | bytes 24580
  6.5 12.5 %copy-start.4 = (bf16[32,128]{1,0:T(8,128)(2,1)S(1)}, bf16[32,128]{1,0:T(8,128)(2,1)}, u32[]{:S(2)}) copy-start(bf16[32,128]{1,0:T(8,128)(2,1)} %param.18) | copy-start | bytes 24580
  6.5 133.4 %all-gather.2.cloned.1.call-start = ((), (), s32[]{:S(2)}) async-start(), calls=%async_computation.6 | async-start | bytes 7798784 | tf_op jit(solution)/shard_map/all_gather | solution.py:47
  59.4 3.8 %copy-start.6 = (bf16[2048]{0:T(1024)(128)(2,1)S(1)}, bf16[2048]{0:T(1024)(128)(2,1)}, u32[]{:S(2)}) copy-start(bf16[2048]{0:T(1024)(128)(2,1)} %param.16) | copy-start | bytes 12292
  59.4 3.8 %copy-start = (bf16[256,2048]{1,0:T(8,128)(2,1)S(1)}, bf16[256,2048]{1,0:T(8,128)(2,1)}, u32[]{:S(2)}) copy-start(bf16[256,2048]{1,0:T(8,128)(2,1)} %param.15) | copy-start | bytes 3145732
  59.4 16.5 %all-to-all-start = ((bf16[4,512,384]{2,1,0:T(8,128)(2,1)}), bf16[4,512,384]{2,1,0:T(8,128)(2,1)S(1)}, u32[]{:S(2)}, u32[]{:S(2)}) async-start(bf16[4,512,384]{2,1,0:T(8,128)(2,1)} %broadcast_in_dim.58), calls=%async_computation | async-start | bytes 3145728 | tf_op jit(solution)/shard_map/all_to_all | solution.py:20
  63.1 1.7 copy-start.8
  63.1 2.3 %copy-start.7 = (bf16[2048]{0:T(1024)(128)(2,1)S(1)}, bf16[2048]{0:T(1024)(128)(2,1)}, u32[]{:S(2)}) copy-start(bf16[2048]{0:T(1024)(128)(2,1)} %param.25) | copy-start | bytes 12292
  75.9 1.2 copy-start.1
  82.0 12.2 %collective-permute-start = (bf16[128,2048]{1,0:T(8,128)(2,1)S(1)}, bf16[128,2048]{1,0:T(8,128)(2,1)S(1)}, u32[]{:S(2)}, u32[]{:S(2)}) collective-permute-start(bf16[128,2048]{1,0:T(8,128)(2,1)S(1)} %convolution_convert_fusion), channel_id=1, source_target_pairs={{0,1},{1,0},{2,3},{3,2},{4,5},{5,4},{6,7},{7,6},{8,9},{9,8},{10,11... | collective-permute-start | bytes 1572872 | tf_op jit(solution)/shard_map/ppermute | solution.py:54
  93.8 13.5 %copy-start.2 = (f32[2048]{0:T(1024)S(1)}, f32[2048]{0:T(1024)}, u32[]{:S(2)}) copy-start(f32[2048]{0:T(1024)} %convert_element_type.91) | copy-start | bytes 24580
  108.3 11.0 %all-to-all-start.2 = ((bf16[4,32,2048]{2,1,0:T(8,128)(2,1)}), bf16[4,32,2048]{2,1,0:T(8,128)(2,1)S(1)}, u32[]{:S(2)}, u32[]{:S(2)}) async-start(bf16[4,32,2048]{2,1,0:T(8,128)(2,1)} %broadcast_in_dim.59), calls=%async_computation.2 | async-start | bytes 1048576 | tf_op jit(solution)/shard_map/all_to_all | solution.py:20
  111.8 19.0 %collective-permute-start.2 = (bf16[512,256]{1,0:T(8,128)(2,1)S(1)}, bf16[512,256]{1,0:T(8,128)(2,1)S(1)}, u32[]{:S(2)}, u32[]{:S(2)}) collective-permute-start(bf16[512,256]{1,0:T(8,128)(2,1)S(1)} %slice.39), channel_id=1, source_target_pairs={{0,8},{8,16},{16,24},{24,0},{1,9},{9,17},{17,25},{25,1},{2,10},{10... | collective-permute-start | bytes 786440 | tf_op jit(solution)/shard_map/ppermute | solution.py:34
  119.3 20.1 %collective-permute-start.1 = (bf16[128,2048]{1,0:T(8,128)(2,1)S(1)}, bf16[128,2048]{1,0:T(8,128)(2,1)S(1)}, u32[]{:S(2)}, u32[]{:S(2)}) collective-permute-start(bf16[128,2048]{1,0:T(8,128)(2,1)S(1)} %bitcast.35), channel_id=1, source_target_pairs={{0,1},{1,0},{2,3},{3,2},{4,5},{5,4},{6,7},{7,6},{8,9},{9,8},{10,11... | collective-permute-start | bytes 1572872 | tf_op jit(solution)/shard_map/ppermute | solution.py:241
  124.1 11.2 %collective-permute-start.3 = (bf16[512,256]{1,0:T(8,128)(2,1)S(1)}, bf16[512,256]{1,0:T(8,128)(2,1)S(1)}, u32[]{:S(2)}, u32[]{:S(2)}) collective-permute-start(bf16[512,256]{1,0:T(8,128)(2,1)S(1)} %slice.39), channel_id=1, source_target_pairs={{0,16},{8,24},{16,0},{24,8},{1,17},{9,25},{17,1},{25,9},{2,18},{10... | collective-permute-start | bytes 786440 | tf_op jit(solution)/shard_map/ppermute | solution.py:34
  126.4 13.1 %collective-permute-start.4 = (bf16[512,256]{1,0:T(8,128)(2,1)S(1)}, bf16[512,256]{1,0:T(8,128)(2,1)S(1)}, u32[]{:S(2)}, u32[]{:S(2)}) collective-permute-start(bf16[512,256]{1,0:T(8,128)(2,1)S(1)} %slice.39), channel_id=1, source_target_pairs={{0,24},{8,0},{16,8},{24,16},{1,25},{9,1},{17,9},{25,17},{2,26},{10... | collective-permute-start | bytes 786440 | tf_op jit(solution)/shard_map/ppermute | solution.py:34
  140.0 4.0 %copy-start.9 = (bf16[2048,1792]{1,0:T(8,128)(2,1)S(1)}, bf16[2048,1792]{1,0:T(8,128)(2,1)}, u32[]{:S(2)}) copy-start(bf16[2048,1792]{1,0:T(8,128)(2,1)} %all-gather.2.cloned.1.call-done) | copy-start | bytes 22020100
  145.5 4.3 %collective-permute-start.5 = (bf16[128,2048]{1,0:T(8,128)(2,1)S(1)}, bf16[128,2048]{1,0:T(8,128)(2,1)S(1)}, u32[]{:S(2)}, u32[]{:S(2)}) collective-permute-start(bf16[128,2048]{1,0:T(8,128)(2,1)S(1)} %fusion.6), channel_id=1, source_target_pairs={{0,1},{1,0},{2,3},{3,2},{4,5},{5,4},{6,7},{7,6},{8,9},{9,8},{10,11... | collective-permute-start | bytes 1572872 | tf_op jit(solution)/shard_map/ppermute | solution.py:54
  172.6 5.5 %collective-permute-start.6 = (bf16[128,2048]{1,0:T(8,128)(2,1)S(1)}, bf16[128,2048]{1,0:T(8,128)(2,1)S(1)}, u32[]{:S(2)}, u32[]{:S(2)}) collective-permute-start(bf16[128,2048]{1,0:T(8,128)(2,1)S(1)} %bitcast.28), channel_id=1, source_target_pairs={{0,1},{1,0},{2,3},{3,2},{4,5},{5,4},{6,7},{7,6},{8,9},{9,8},{10,11... | collective-permute-start | bytes 1572872 | tf_op jit(solution)/shard_map/ppermute | solution.py:65
Sparse Core Ops, SparseCore 0:
  19.1 103.5 all-gather.1

commit v7 on v6

--- a/solution.py
+++ b/solution.py
@@ -118,8 +118,11 @@
     return jnp.where(jnp.abs(x) < 0.4, -x * series, 1.0 - jnp.exp(x))
 
 
-def hidden_kernel(both, taps, retention, admission, rate, extra, out):
+def hidden_kernel(normed, weights, taps, retention, admission, rate, extra, out):
     channels = out.shape[1]
+    both = jnp.dot(
+        normed[...], weights[:, : 2 * channels], preferred_element_type=jnp.float32
+    ).astype(jnp.bfloat16)
     signal = both[:, :channels].astype(jnp.float32)
     width_taps = taps.shape[0]
     total = jnp.zeros(signal.shape, jnp.float32)
@@ -190,13 +193,11 @@
     normed = lax.optimization_barrier(
         root_norm(tokens.astype(jnp.float32), recurrent_input_gain).astype(jnp.bfloat16)
     )
-    both = jnp.dot(
-        normed, mixer[:, : 2 * channels], preferred_element_type=jnp.float32
-    ).astype(jnp.bfloat16)
     hidden = pl.pallas_call(
-        hidden_kernel, out_shape=jax.ShapeDtypeStruct((both.shape[0], channels), jnp.bfloat16)
+        hidden_kernel, out_shape=jax.ShapeDtypeStruct((tokens.shape[0], channels), jnp.bfloat16)
     )(
-        both,
+        normed,
+        mixer,
         filter_taps.astype(jnp.float32),
         retention_gate_blocks.reshape(2, channels, channels),
         input_gate_blocks.reshape(2, channels, channels),

time: 187 us -> 187 us (level)
  transfers between devices with their start and end apart: 10 -> 10, of which waited for: 6 -> 6; matrix products, arithmetic and copies ran while one was open for 7% -> 7% of each run, Pallas kernels for 1% -> 2%
where the time goes in v7:
time: 187 us; the launch traced here: 186 us
  blocking collectives  85.2 us (46%)
  starting transfers between devices  38.1 us (20%)
  waiting for transfers between devices  24.6 us (13%)
  between operations  13.8 us (7%)
  matrix products  8.51 us (5%)
  local copies, waits for them, and re-layouts  6.05 us (3%)
  other arithmetic  6.03 us (3%)
  Pallas kernels  4.06 us (2%)
    all_gather x1, blocking collectives, per_device(): lax.all_gather(jnp.concatenate((recurrent_branch_weight, output_gate_weig...  38.9 us
    all_to_all x2, blocking collectives, summed_rows(): lax.all_to_all(quarters, 'x', split_axis=0, concat_axis=0, tiled=True)  24.1 us
    all_to_all x2, blocking collectives, spread(): return lax.all_to_all(copies, axis, split_axis=0, concat_axis=0, tiled=True)  22.2 us
    all_to_all x2, waiting for transfers between devices, spread(): return lax.all_to_all(copies, axis, split_axis=0, concat_axis=0, tiled=True)  15.1 us
    ppermute x2, starting transfers between devices, summed_rows(): sent = lax.ppermute(rows_of(others).astype(jnp.bfloat16), 'c', CORES)  13.5 us
    ppermute x3, waiting for transfers between devices, sent_round(): pieces.append(lax.ppermute(array, axis, ring))  8.67 us
    ppermute x3, starting transfers between devices, sent_round(): pieces.append(lax.ppermute(array, axis, ring))  8.66 us
    all_to_all x2, starting transfers between devices, spread(): return lax.all_to_all(copies, axis, split_axis=0, concat_axis=0, tiled=True)  7.16 us
  transfers between devices with their start and end apart: 10, of which 6 were waited for; matrix products, arithmetic and copies ran while one was open for 7% of the time, Pallas kernels for 2%

profile of v7, /device:TPU:1, one launch (start us, length us, event | category | flops | bytes accessed | tf_op | source)
XLA Modules:
  0.0 186.3 jit_solution(12132608257050518789)
XLA Ops:
  7.5 11.5 %all_to_all.30 = bf16[4,32,1792]{2,1,0:T(8,128)(2,1)} all-to-all(bf16[4,32,1792]{2,1,0:T(8,128)(2,1)S(1)} %broadcast_in_dim.60), channel_id=1, replica_groups=mesh['zh'=4,'zl'=4,'y'=4,'x'=4,'c'=2] {'y'}, dimensions={0} | all-to-all | bytes 917504 | tf_op jit(solution)/shard_map/all_to_all | solution.py:20
  19.1 38.9 %all_gather.6 = bf16[512,640]{1,0:T(8,128)(2,1)S(1)} all-gather(bf16[32,640]{1,0:T(8,128)(2,1)S(1)} %pad_maximum_fusion.5), channel_id=1, replica_groups=mesh['zh'=4,'zl'=4,'y'=4,'x'=4,'c'=2] {'zh','zl'}, dimensions={0}, use_global_device_ids=true | all-gather | bytes 696320 | tf_op jit(solution)/shard_map/all_gather | solution.py:175
  58.0 1.4 broadcast_in_dim.58
  59.4 3.7 %all-to-all-start = ((bf16[4,512,384]{2,1,0:T(8,128)(2,1)}), bf16[4,512,384]{2,1,0:T(8,128)(2,1)S(1)}, u32[]{:S(2)}, u32[]{:S(2)}) async-start(bf16[4,512,384]{2,1,0:T(8,128)(2,1)} %broadcast_in_dim.58), calls=%async_computation | async-start | bytes 3145728 | tf_op jit(solution)/shard_map/all_to_all | solution.py:20
  66.1 9.8 %all-to-all-done = bf16[4,512,384]{2,1,0:T(8,128)(2,1)S(1)} async-done(((bf16[4,512,384]{2,1,0:T(8,128)(2,1)}), bf16[4,512,384]{2,1,0:T(8,128)(2,1)S(1)}, u32[]{:S(2)}, u32[]{:S(2)}) %all-to-all-start) | async-done | bytes 1572896 | tf_op jit(solution)/shard_map/all_to_all | solution.py:20
  75.9 1.5 copy.17
  77.4 4.1 %shard_map.145 = bf16[256,128]{1,0:T(8,128)(2,1)} custom-call(bf16[256,2048]{1,0:T(8,128)(2,1)} %fusion.11.normed, bf16[2048,384]{1,0:T(8,128)(2,1)} %bitcast.23, f32[4,128]{1,0:T(4,128)} %convert_element_type.85.taps, bf16[2,128,128]{2,1,0:T(8,128)(2,1)} %bitcast.40, bf16[2,128,128]{2,1,0:T(8,128)(2,1)} %bitcast.41, f32[2,128]{1,0:T(2,128)} %rate.1, ...), custom_call_target="tpu_custom_call" | custom-call | tf_op jit(solution)/shard_map/pallas_call | solution.py:196
  82.5 10.7 %collective-permute-start = (bf16[128,2048]{1,0:T(8,128)(2,1)S(1)}, bf16[128,2048]{1,0:T(8,128)(2,1)S(1)}, u32[]{:S(2)}, u32[]{:S(2)}) collective-permute-start(bf16[128,2048]{1,0:T(8,128)(2,1)S(1)} %convolution_convert_fusion), channel_id=1, source_target_pairs={{0,1},{1,0},{2,3},{3,2},{4,5},{5,4},{6,7},{7,6},{8,9},{9,8},{10,11... | collective-permute-start | bytes 1572872 | tf_op jit(solution)/shard_map/ppermute | solution.py:54
  94.9 12.5 %all_to_all.31 = bf16[4,32,2048]{2,1,0:T(8,128)(2,1)S(1)} all-to-all(bf16[4,32,2048]{2,1,0:T(8,128)(2,1)S(1)} %bitcast.29), channel_id=1, replica_groups=mesh['zh'=4,'zl'=4,'y'=4,'x'=4,'c'=2] {'x'}, dimensions={0} | all-to-all | bytes 1048576 | tf_op jit(solution)/shard_map/all_to_all | solution.py:59
  108.8 3.5 %all-to-all-start.2 = ((bf16[4,32,2048]{2,1,0:T(8,128)(2,1)}), bf16[4,32,2048]{2,1,0:T(8,128)(2,1)S(1)}, u32[]{:S(2)}, u32[]{:S(2)}) async-start(bf16[4,32,2048]{2,1,0:T(8,128)(2,1)} %broadcast_in_dim.59), calls=%async_computation.2 | async-start | bytes 1048576 | tf_op jit(solution)/shard_map/all_to_all | solution.py:20
  112.3 2.2 %collective-permute-start.2 = (bf16[512,256]{1,0:T(8,128)(2,1)S(1)}, bf16[512,256]{1,0:T(8,128)(2,1)S(1)}, u32[]{:S(2)}, u32[]{:S(2)}) collective-permute-start(bf16[512,256]{1,0:T(8,128)(2,1)S(1)} %slice.35), channel_id=1, source_target_pairs={{0,8},{8,16},{16,24},{24,0},{1,9},{9,17},{17,25},{25,1},{2,10},{10... | collective-permute-start | bytes 786440 | tf_op jit(solution)/shard_map/ppermute | solution.py:34
  114.5 5.4 %all-to-all-done.2 = bf16[4,32,2048]{2,1,0:T(8,128)(2,1)S(1)} async-done(((bf16[4,32,2048]{2,1,0:T(8,128)(2,1)}), bf16[4,32,2048]{2,1,0:T(8,128)(2,1)S(1)}, u32[]{:S(2)}, u32[]{:S(2)}) %all-to-all-start.2) | async-done | bytes 524320 | tf_op jit(solution)/shard_map/all_to_all | solution.py:20
  119.8 4.8 %collective-permute-start.1 = (bf16[128,2048]{1,0:T(8,128)(2,1)S(1)}, bf16[128,2048]{1,0:T(8,128)(2,1)S(1)}, u32[]{:S(2)}, u32[]{:S(2)}) collective-permute-start(bf16[128,2048]{1,0:T(8,128)(2,1)S(1)} %bitcast.34), channel_id=1, source_target_pairs={{0,1},{1,0},{2,3},{3,2},{4,5},{5,4},{6,7},{7,6},{8,9},{9,8},{10,11... | collective-permute-start | bytes 1572872 | tf_op jit(solution)/shard_map/ppermute | solution.py:242
  124.6 2.2 %collective-permute-start.3 = (bf16[512,256]{1,0:T(8,128)(2,1)S(1)}, bf16[512,256]{1,0:T(8,128)(2,1)S(1)}, u32[]{:S(2)}, u32[]{:S(2)}) collective-permute-start(bf16[512,256]{1,0:T(8,128)(2,1)S(1)} %slice.35), channel_id=1, source_target_pairs={{0,16},{8,24},{16,0},{24,8},{1,17},{9,25},{17,1},{25,9},{2,18},{10... | collective-permute-start | bytes 786440 | tf_op jit(solution)/shard_map/ppermute | solution.py:34
  126.8 4.3 %collective-permute-start.4 = (bf16[512,256]{1,0:T(8,128)(2,1)S(1)}, bf16[512,256]{1,0:T(8,128)(2,1)S(1)}, u32[]{:S(2)}, u32[]{:S(2)}) collective-permute-start(bf16[512,256]{1,0:T(8,128)(2,1)S(1)} %slice.35), channel_id=1, source_target_pairs={{0,24},{8,0},{16,8},{24,16},{1,25},{9,1},{17,9},{25,17},{2,26},{10... | collective-permute-start | bytes 786440 | tf_op jit(solution)/shard_map/ppermute | solution.py:34
  131.3 4.6 %collective-permute-done.3 = bf16[512,256]{1,0:T(8,128)(2,1)S(1)} collective-permute-done((bf16[512,256]{1,0:T(8,128)(2,1)S(1)}, bf16[512,256]{1,0:T(8,128)(2,1)S(1)}, u32[]{:S(2)}, u32[]{:S(2)}) %collective-permute-start.3) | collective-permute-done | bytes 262176 | tf_op jit(solution)/shard_map/ppermute | solution.py:34
  135.8 4.1 %collective-permute-done.4 = bf16[512,256]{1,0:T(8,128)(2,1)S(1)} collective-permute-done((bf16[512,256]{1,0:T(8,128)(2,1)S(1)}, bf16[512,256]{1,0:T(8,128)(2,1)S(1)}, u32[]{:S(2)}, u32[]{:S(2)}) %collective-permute-start.4) | collective-permute-done | bytes 262176 | tf_op jit(solution)/shard_map/ppermute | solution.py:34
  140.5 3.0 %fusion.18 = bf16[256,768]{1,0:T(8,128)(2,1)S(1)} fusion(bf16[2048,1792]{1,0:T(8,128)(2,1)} %all-gather.2.cloned.1.call-done, bf16[128,2048]{1,0:T(8,128)(2,1)S(1)} %collective-permute-done.1, bf16[128,2048]{1,0:T(8,128)(2,1)S(1)} %bitcast.36), kind=kOutput, calls=%fused_computation.15 | convolution fusion | flops 807993344 | bytes 4587520 | tf_op jit(solution)/shard_map/dot_general | solution.py:247
  144.5 1.5 fusion.6
  146.0 2.8 %collective-permute-start.5 = (bf16[128,2048]{1,0:T(8,128)(2,1)S(1)}, bf16[128,2048]{1,0:T(8,128)(2,1)S(1)}, u32[]{:S(2)}, u32[]{:S(2)}) collective-permute-start(bf16[128,2048]{1,0:T(8,128)(2,1)S(1)} %fusion.6), channel_id=1, source_target_pairs={{0,1},{1,0},{2,3},{3,2},{4,5},{5,4},{6,7},{7,6},{8,9},{9,8},{10,11... | collective-permute-start | bytes 1572872 | tf_op jit(solution)/shard_map/ppermute | solution.py:54
  148.8 1.5 fusion.2
  150.4 11.6 %all_to_all.32 = bf16[4,32,2048]{2,1,0:T(8,128)(2,1)S(1)} all-to-all(bf16[4,32,2048]{2,1,0:T(8,128)(2,1)S(1)} %bitcast.30), channel_id=1, replica_groups=mesh['zh'=4,'zl'=4,'y'=4,'x'=4,'c'=2] {'x'}, dimensions={0} | all-to-all | bytes 1048576 | tf_op jit(solution)/shard_map/all_to_all | solution.py:59
  162.4 10.7 %all_to_all.33 = bf16[4,32,2048]{2,1,0:T(8,128)(2,1)S(1)} all-to-all(bf16[4,32,2048]{2,1,0:T(8,128)(2,1)S(1)} %broadcast_in_dim.62), channel_id=1, replica_groups=mesh['zh'=4,'zl'=4,'y'=4,'x'=4,'c'=2] {'x'}, dimensions={0} | all-to-all | bytes 1048576 | tf_op jit(solution)/shard_map/all_to_all | solution.py:20
  173.2 4.0 %collective-permute-start.6 = (bf16[128,2048]{1,0:T(8,128)(2,1)S(1)}, bf16[128,2048]{1,0:T(8,128)(2,1)S(1)}, u32[]{:S(2)}, u32[]{:S(2)}) collective-permute-start(bf16[128,2048]{1,0:T(8,128)(2,1)S(1)} %bitcast.27), channel_id=1, source_target_pairs={{0,1},{1,0},{2,3},{3,2},{4,5},{5,4},{6,7},{7,6},{8,9},{9,8},{10,11... | collective-permute-start | bytes 1572872 | tf_op jit(solution)/shard_map/ppermute | solution.py:65
  (71 shorter events, 12.6 us)
Async XLA Ops:
  6.5 12.5 %slice-start = ((bf16[32,1024]{1,0:T(8,128)(2,1)}), bf16[32,256]{1,0:T(8,128)(2,1)S(1)}, s32[]{:S(2)}) async-start(bf16[32,1024]{1,0:T(8,128)(2,1)} %param.27), calls=%async_computation.7 | async-start | bytes 32768 | tf_op jit(solution)/shard_map/slice | solution.py:181
  6.5 12.5 %copy-start.2 = (bf16[128,32]{0,1:T(8,128)(2,1)S(1)}, bf16[128,32]{0,1:T(8,128)(2,1)}, u32[]{:S(2)}) copy-start(bf16[128,32]{0,1:T(8,128)(2,1)} %param.24) | copy-start | bytes 24580
  6.5 12.5 %copy-start.4 = (bf16[32,128]{1,0:T(8,128)(2,1)S(1)}, bf16[32,128]{1,0:T(8,128)(2,1)}, u32[]{:S(2)}) copy-start(bf16[32,128]{1,0:T(8,128)(2,1)} %param.17) | copy-start | bytes 24580
  6.5 12.5 %copy-start.3 = (bf16[32,128]{1,0:T(8,128)(2,1)S(1)}, bf16[32,128]{1,0:T(8,128)(2,1)}, u32[]{:S(2)}) copy-start(bf16[32,128]{1,0:T(8,128)(2,1)} %param.18) | copy-start | bytes 24580
  6.5 133.9 %all-gather.2.cloned.1.call-start = ((), (), s32[]{:S(2)}) async-start(), calls=%async_computation.6 | async-start | bytes 7798784 | tf_op jit(solution)/shard_map/all_gather | solution.py:47
  59.4 3.8 %copy-start.5 = (bf16[2048]{0:T(1024)(128)(2,1)S(1)}, bf16[2048]{0:T(1024)(128)(2,1)}, u32[]{:S(2)}) copy-start(bf16[2048]{0:T(1024)(128)(2,1)} %param.16) | copy-start | bytes 12292
  59.4 3.8 %copy-start.1 = (bf16[256,2048]{1,0:T(8,128)(2,1)S(1)}, bf16[256,2048]{1,0:T(8,128)(2,1)}, u32[]{:S(2)}) copy-start(bf16[256,2048]{1,0:T(8,128)(2,1)} %param.15) | copy-start | bytes 3145732
  59.4 16.5 %all-to-all-start = ((bf16[4,512,384]{2,1,0:T(8,128)(2,1)}), bf16[4,512,384]{2,1,0:T(8,128)(2,1)S(1)}, u32[]{:S(2)}, u32[]{:S(2)}) async-start(bf16[4,512,384]{2,1,0:T(8,128)(2,1)} %broadcast_in_dim.58), calls=%async_computation | async-start | bytes 3145728 | tf_op jit(solution)/shard_map/all_to_all | solution.py:20
  63.1 3.0 %copy-start.6 = (bf16[2048]{0:T(1024)(128)(2,1)S(1)}, bf16[2048]{0:T(1024)(128)(2,1)}, u32[]{:S(2)}) copy-start(bf16[2048]{0:T(1024)(128)(2,1)} %param.25) | copy-start | bytes 12292
  63.1 3.0 %copy-start.7 = (bf16[2048]{0:T(1024)(128)(2,1)S(1)}, bf16[2048]{0:T(1024)(128)(2,1)}, u32[]{:S(2)}) copy-start(bf16[2048]{0:T(1024)(128)(2,1)} %param.26) | copy-start | bytes 12292
  63.1 3.0 %copy-start.8 = (bf16[2048]{0:T(1024)(128)(2,1)S(1)}, bf16[2048]{0:T(1024)(128)(2,1)}, u32[]{:S(2)}) copy-start(bf16[2048]{0:T(1024)(128)(2,1)} %param.29) | copy-start | bytes 12292
  77.4 4.1 %copy-start = (bf16[16,4,32,384]{3,2,1,0:T(8,128)(2,1)S(1)}, bf16[16,4,32,384]{3,2,1,0:T(8,128)(2,1)}, u32[]{:S(2)}) copy-start(bf16[16,4,32,384]{3,2,1,0:T(8,128)(2,1)} %copy.17) | copy-start | bytes 4718596
  82.5 12.3 %collective-permute-start = (bf16[128,2048]{1,0:T(8,128)(2,1)S(1)}, bf16[128,2048]{1,0:T(8,128)(2,1)S(1)}, u32[]{:S(2)}, u32[]{:S(2)}) collective-permute-start(bf16[128,2048]{1,0:T(8,128)(2,1)S(1)} %convolution_convert_fusion), channel_id=1, source_target_pairs={{0,1},{1,0},{2,3},{3,2},{4,5},{5,4},{6,7},{7,6},{8,9},{9,8},{10,11... | collective-permute-start | bytes 1572872 | tf_op jit(solution)/shard_map/ppermute | solution.py:54
  108.8 11.0 %all-to-all-start.2 = ((bf16[4,32,2048]{2,1,0:T(8,128)(2,1)}), bf16[4,32,2048]{2,1,0:T(8,128)(2,1)S(1)}, u32[]{:S(2)}, u32[]{:S(2)}) async-start(bf16[4,32,2048]{2,1,0:T(8,128)(2,1)} %broadcast_in_dim.59), calls=%async_computation.2 | async-start | bytes 1048576 | tf_op jit(solution)/shard_map/all_to_all | solution.py:20
  112.3 19.0 %collective-permute-start.2 = (bf16[512,256]{1,0:T(8,128)(2,1)S(1)}, bf16[512,256]{1,0:T(8,128)(2,1)S(1)}, u32[]{:S(2)}, u32[]{:S(2)}) collective-permute-start(bf16[512,256]{1,0:T(8,128)(2,1)S(1)} %slice.35), channel_id=1, source_target_pairs={{0,8},{8,16},{16,24},{24,0},{1,9},{9,17},{17,25},{25,1},{2,10},{10... | collective-permute-start | bytes 786440 | tf_op jit(solution)/shard_map/ppermute | solution.py:34
  119.8 20.2 %collective-permute-start.1 = (bf16[128,2048]{1,0:T(8,128)(2,1)S(1)}, bf16[128,2048]{1,0:T(8,128)(2,1)S(1)}, u32[]{:S(2)}, u32[]{:S(2)}) collective-permute-start(bf16[128,2048]{1,0:T(8,128)(2,1)S(1)} %bitcast.34), channel_id=1, source_target_pairs={{0,1},{1,0},{2,3},{3,2},{4,5},{5,4},{6,7},{7,6},{8,9},{9,8},{10,11... | collective-permute-start | bytes 1572872 | tf_op jit(solution)/shard_map/ppermute | solution.py:242
  124.6 11.2 %collective-permute-start.3 = (bf16[512,256]{1,0:T(8,128)(2,1)S(1)}, bf16[512,256]{1,0:T(8,128)(2,1)S(1)}, u32[]{:S(2)}, u32[]{:S(2)}) collective-permute-start(bf16[512,256]{1,0:T(8,128)(2,1)S(1)} %slice.35), channel_id=1, source_target_pairs={{0,16},{8,24},{16,0},{24,8},{1,17},{9,25},{17,1},{25,9},{2,18},{10... | collective-permute-start | bytes 786440 | tf_op jit(solution)/shard_map/ppermute | solution.py:34
  126.8 13.2 %collective-permute-start.4 = (bf16[512,256]{1,0:T(8,128)(2,1)S(1)}, bf16[512,256]{1,0:T(8,128)(2,1)S(1)}, u32[]{:S(2)}, u32[]{:S(2)}) collective-permute-start(bf16[512,256]{1,0:T(8,128)(2,1)S(1)} %slice.35), channel_id=1, source_target_pairs={{0,24},{8,0},{16,8},{24,16},{1,25},{9,1},{17,9},{25,17},{2,26},{10... | collective-permute-start | bytes 786440 | tf_op jit(solution)/shard_map/ppermute | solution.py:34
  140.5 4.0 %copy-start.9 = (bf16[2048,1792]{1,0:T(8,128)(2,1)S(1)}, bf16[2048,1792]{1,0:T(8,128)(2,1)}, u32[]{:S(2)}) copy-start(bf16[2048,1792]{1,0:T(8,128)(2,1)} %all-gather.2.cloned.1.call-done) | copy-start | bytes 22020100
  146.0 4.3 %collective-permute-start.5 = (bf16[128,2048]{1,0:T(8,128)(2,1)S(1)}, bf16[128,2048]{1,0:T(8,128)(2,1)S(1)}, u32[]{:S(2)}, u32[]{:S(2)}) collective-permute-start(bf16[128,2048]{1,0:T(8,128)(2,1)S(1)} %fusion.6), channel_id=1, source_target_pairs={{0,1},{1,0},{2,3},{3,2},{4,5},{5,4},{6,7},{7,6},{8,9},{9,8},{10,11... | collective-permute-start | bytes 1572872 | tf_op jit(solution)/shard_map/ppermute | solution.py:54
  173.2 5.5 %collective-permute-start.6 = (bf16[128,2048]{1,0:T(8,128)(2,1)S(1)}, bf16[128,2048]{1,0:T(8,128)(2,1)S(1)}, u32[]{:S(2)}, u32[]{:S(2)}) collective-permute-start(bf16[128,2048]{1,0:T(8,128)(2,1)S(1)} %bitcast.27), channel_id=1, source_target_pairs={{0,1},{1,0},{2,3},{3,2},{4,5},{5,4},{6,7},{7,6},{8,9},{9,8},{10,11... | collective-permute-start | bytes 1572872 | tf_op jit(solution)/shard_map/ppermute | solution.py:65
Sparse Core Ops, SparseCore 0:
  19.1 103.5 all-gather.1
